TPU v7x, 128 devices: a whole 4x4x4 slice. The times are simulated.
128 devices in a mesh: ep: 32 (over z, y, core), tp: 4 (over x).
Axes of the slice: x: 4, y: 4, z: 4, core: 2. Of those that a mesh axis runs over, the one named last changes fastest.
Arguments:
- tokens: bfloat16 [1536, 2048], P('ep'), may hold values from -6 to 6
- mix_gain: float32 [2048], replicated, may hold values from 0.1 to 1.9
- w_query: bfloat16 [2048, 1024], P(None, 'tp'), may hold values from -0.125 to 0.125
- w_key: bfloat16 [2048, 1024], P(None, 'tp'), may hold values from -0.125 to 0.125
- w_value: bfloat16 [2048, 1024], P(None, 'tp'), may hold values from -0.125 to 0.125
- w_outgate: bfloat16 [2048, 1024], P(None, 'tp'), may hold values from -0.125 to 0.125
- w_ingate: bfloat16 [2048, 8], P(None, 'tp'), may hold values from -0.125 to 0.125
- w_forget: bfloat16 [2048, 8], P(None, 'tp'), may hold values from -0.125 to 0.125
- in_bias: float32 [8], P('tp'), may hold values from -2 to 1
- forget_bias: float32 [8], P('tp'), may hold values from -1 to 4
- w_mix_out: bfloat16 [1024, 2048], replicated, may hold values from -0.1875 to 0.1875
- cell_state: float32 [1536, 8, 128, 128], P('ep', 'tp'), may hold values from -0.5 to 0.5
- norm_state: float32 [1536, 8, 128], P('ep', 'tp'), may hold values from -0.5 to 0.5
- max_state: float32 [1536, 8], P('ep', 'tp'), may hold values from -1 to 2
- moe_gain: float32 [2048], replicated, may hold values from 0.1 to 1.9
- route_ids: int32 [1536, 2], P('ep'), may hold values from 0 to 31, as said below
- route_weights: float32 [1536, 2], P('ep'), may hold values from 0.2 to 1
- expert_gate: bfloat16 [32, 2048, 1024], P('ep', None, 'tp'), may hold values from -0.125 to 0.125
- expert_up: bfloat16 [32, 2048, 1024], P('ep', None, 'tp'), may hold values from -0.125 to 0.125
- expert_down: bfloat16 [32, 1024, 2048], P('ep', 'tp'), may hold values from -0.1875 to 0.1875
- branch_gate: bfloat16 [2048], replicated, may hold values from -0.125 to 0.125
- dense_gate: bfloat16 [2048, 8192], P(None, ('ep', 'tp')), may hold values from -0.125 to 0.125
- dense_up: bfloat16 [2048, 8192], P(None, ('ep', 'tp')), may hold values from -0.125 to 0.125
- dense_down: bfloat16 [8192, 2048], P(('ep', 'tp')), may hold values from -0.25 to 0.25
Outputs:
- layer_out: bfloat16 [1536, 2048], P('ep', 'tp')
- new_cell: float32 [1536, 8, 128, 128], P('ep', 'tp')
- new_norm: float32 [1536, 8, 128], P('ep', 'tp')
- new_max: float32 [1536, 8], P('ep', 'tp')
Inputs may be any that keep to these rules, and one draw needn't show every extreme that they name: `route_ids`: each row names two different experts of one group of 8 consecutive ids. Within the rows of one device no id appears more than 6 times, and some id appears exactly 6 times.
All inputs are finite; a program needn't handle non-finite values.
Results may differ from a plain program's by a relative error of at most 0.009.
The roundings to bfloat16 on the way count: a program that leaves them out, or rounds other values in their place, can miss the bound.
Values may be sent and summed in bfloat16 or wider, within the bound.
No kernel may reach another device: no remote copies, remote signals or barrier semaphores. Data moves between devices by JAX's collectives and lax.ppermute only.
A program may use at most 128 MiB of HBM per device.

v0:
```python
import jax
import jax.numpy as jnp
from jax import lax
from jax.sharding import PartitionSpec as P

EPS = 1e-06


def in_order(parts, dim):
    parts = jnp.moveaxis(parts, 0, dim)
    dims = parts.shape
    return parts.reshape(*dims[:dim], dims[dim] * dims[dim + 1], *dims[dim + 2 :])


def sent_to_all(array, axis):
    copies = jnp.broadcast_to(array, (lax.axis_size(axis), *array.shape))
    return lax.all_to_all(copies, axis, split_axis=0, concat_axis=0, tiled=True)


def collect(array, axis, dim):
    return in_order(sent_to_all(array, axis), dim)


def turned_gather(arrays, axis, dims):
    turned = [jnp.moveaxis(a, dim, 0) for a, dim in zip(arrays, dims)]
    both = jnp.concatenate([t.reshape(len(t), -1) for t in turned], axis=1)
    filled, at, done = (lax.all_gather(both, axis, axis=0, tiled=True), 0, [])
    for t, dim in zip(turned, dims):
        piece = filled[:, at : at + t[0].size].reshape(-1, *t.shape[1:])
        done.append(jnp.moveaxis(piece, 0, dim))
        at += t[0].size
    return tuple(done)


def split_up(array, dim, size):
    dims = array.shape
    parts = array.reshape(*dims[:dim], size, dims[dim] // size, *dims[dim + 1 :])
    return jnp.moveaxis(parts, dim, 0)


def summed_on_arrival(array, axis, dim):
    parts = split_up(array, dim, lax.axis_size(axis))
    arrived = lax.all_to_all(parts, axis, split_axis=0, concat_axis=0, tiled=True)
    return arrived.astype(jnp.float32).sum(axis=0)


def norm_rows(rows_in, gain_vec):
    as_float = rows_in.astype(jnp.float32)
    scaled = as_float * lax.rsqrt(jnp.mean(as_float * as_float, axis=-1, keepdims=True) + EPS)
    return (scaled * gain_vec).astype(jnp.bfloat16)


def swiglu(tok_rows, gate_w, up_w):
    gate_proj = jnp.dot(tok_rows, gate_w, preferred_element_type=jnp.float32)
    up_proj = jnp.dot(tok_rows, up_w, preferred_element_type=jnp.float32)
    return (jax.nn.silu(gate_proj) * up_proj).astype(jnp.bfloat16)


def branch_weight(tok_rows, branch_gate):
    return jax.nn.sigmoid(jnp.dot(tok_rows, branch_gate, preferred_element_type=jnp.float32))


def cell_step(
    normed,
    w_query,
    w_key,
    w_value,
    w_outgate,
    w_ingate,
    w_forget,
    in_bias,
    forget_bias,
    cell_state,
    norm_state,
    max_state,
):
    row_count, head_count = max_state.shape
    head_size = cell_state.shape[2]

    def project(weight):
        return jnp.dot(normed, weight, preferred_element_type=jnp.float32)

    queries = project(w_query).reshape(row_count, head_count, head_size)
    key_vecs = project(w_key).reshape(row_count, head_count, head_size) * head_size ** (-0.5)
    values = project(w_value).reshape(row_count, head_count, head_size)
    outgate = project(w_outgate)
    in_pre = project(w_ingate) + in_bias
    log_forget = jax.nn.log_sigmoid(project(w_forget) + forget_bias)
    new_max = jnp.maximum(log_forget + max_state, in_pre)
    carry_factor = jnp.exp(log_forget + max_state - new_max)
    write_factor = jnp.exp(in_pre - new_max)
    written = write_factor[..., None] * key_vecs
    new_cell = (
        carry_factor[..., None, None] * cell_state + written[..., :, None] * values[..., None, :]
    )
    new_norm = carry_factor[..., None] * norm_state + written
    numerator = jnp.einsum("bhd,bhde->bhe", queries, new_cell, precision=lax.Precision.HIGHEST)
    denominator = jnp.sum(queries * new_norm, axis=-1)
    cell_out = numerator / jnp.maximum(jnp.abs(denominator), jnp.exp(-new_max))[..., None]
    mixed_heads = (
        jax.nn.sigmoid(outgate) * cell_out.reshape(row_count, head_count * head_size)
    ).astype(jnp.bfloat16)
    return (mixed_heads, new_cell, new_norm, new_max)


def local(
    tokens,
    mix_gain,
    w_query,
    w_key,
    w_value,
    w_outgate,
    w_ingate,
    w_forget,
    in_bias,
    forget_bias,
    w_mix_out,
    cell_state,
    norm_state,
    max_state,
    moe_gain,
    route_ids,
    route_weights,
    expert_gate,
    expert_up,
    expert_down,
    branch_gate,
    dense_gate,
    dense_up,
    dense_down,
):
    seq_dev, model_width = tokens.shape
    tp_count = lax.axis_size("tp")
    ep_count = lax.axis_size("ep")
    col_width = model_width // tp_count
    normed = norm_rows(tokens, mix_gain)
    mixed_heads, new_cell, new_norm, new_max = cell_step(
        normed,
        w_query,
        w_key,
        w_value,
        w_outgate,
        w_ingate,
        w_forget,
        in_bias,
        forget_bias,
        cell_state,
        norm_state,
        max_state,
    )
    all_heads = collect(mixed_heads, "tp", 1)
    mixed_proj = jnp.dot(all_heads, w_mix_out, preferred_element_type=jnp.float32)
    residual = (tokens.astype(jnp.float32) + mixed_proj).astype(jnp.bfloat16)
    moe_in = norm_rows(residual, moe_gain)
    gathered = lax.all_gather(moe_in, "ep", axis=0, tiled=True)
    gate_block, up_block = turned_gather((dense_gate, dense_up), "tp", (1, 1))
    down_block = lax.all_to_all(dense_down, "tp", split_axis=1, concat_axis=0, tiled=True)
    hidden = swiglu(gathered, gate_block, up_block)
    partial_value = jnp.dot(hidden, down_block, preferred_element_type=jnp.float32)
    dense_out = summed_on_arrival(
        (partial_value * branch_weight(gathered, branch_gate)[:, None]).astype(jnp.bfloat16),
        "ep",
        0,
    )
    local_experts = expert_gate.shape[0]
    experts = ep_count * local_experts
    capacity = max(2, 4 * seq_dev // experts)
    top_count = route_ids.shape[1]
    flat_ids = route_ids.reshape(-1)
    position = jnp.arange(flat_ids.shape[0], dtype=jnp.int32)
    earlier = (flat_ids[:, None] == flat_ids[None, :]) & (position[None, :] < position[:, None])
    slot_rank = jnp.sum(earlier.astype(jnp.int32), axis=1)
    slot_index = flat_ids * capacity + slot_rank
    owner_row = position // top_count
    slots_all = jnp.arange(experts * capacity, dtype=jnp.int32)
    matches = slots_all[:, None] == slot_index[None, :]
    source_row = jnp.sum(jnp.where(matches, owner_row[None, :] + 1, 0), axis=1) - 1
    source_row = jnp.where(source_row < 0, seq_dev, source_row)
    padded = jnp.concatenate([moe_in, jnp.zeros((1, model_width), jnp.bfloat16)], axis=0)
    dispatch = jnp.take(padded, source_row, axis=0).reshape(
        ep_count, local_experts, capacity, model_width
    )
    received = lax.all_to_all(dispatch, "ep", split_axis=0, concat_axis=0, tiled=True)
    gate_proj = jnp.einsum(
        "secd,edf->secf", received, expert_gate, preferred_element_type=jnp.float32
    )
    up_proj = jnp.einsum("secd,edf->secf", received, expert_up, preferred_element_type=jnp.float32)
    hidden = (jax.nn.silu(gate_proj) * up_proj).astype(jnp.bfloat16)
    full_out = jnp.einsum("secf,efd->secd", hidden, expert_down, preferred_element_type=jnp.float32)
    summed = summed_on_arrival(full_out.astype(jnp.bfloat16), "tp", 3)
    returned = lax.all_to_all(
        summed.astype(jnp.bfloat16), "ep", split_axis=0, concat_axis=0, tiled=True
    ).astype(summed.dtype)
    returned = returned.reshape(experts * capacity, col_width)
    picked = jnp.take(returned, slot_index, axis=0) * route_weights.reshape(-1)[:, None]
    moe_out = jnp.sum(picked.reshape(seq_dev, top_count, col_width), axis=1)
    own_cols = lax.dynamic_slice_in_dim(
        residual, lax.axis_index("tp") * col_width, col_width, 1
    ).astype(jnp.float32)
    layer_out = (own_cols + moe_out + dense_out).astype(jnp.bfloat16)
    return (layer_out, new_cell, new_norm, new_max)


def solution(mesh):
    in_specs = (
        P("ep", None),
        P(),
        P(None, "tp"),
        P(None, "tp"),
        P(None, "tp"),
        P(None, "tp"),
        P(None, "tp"),
        P(None, "tp"),
        P("tp"),
        P("tp"),
        P(),
        P("ep", "tp", None, None),
        P("ep", "tp", None),
        P("ep", "tp"),
        P(),
        P("ep", None),
        P("ep", None),
        P("ep", None, "tp"),
        P("ep", None, "tp"),
        P("ep", "tp", None),
        P(),
        P(None, ("ep", "tp")),
        P(None, ("ep", "tp")),
        P(("ep", "tp"), None),
    )
    out_specs = (P("ep", "tp"), P("ep", "tp", None, None), P("ep", "tp", None), P("ep", "tp"))
    return jax.shard_map(local, mesh=mesh, in_specs=in_specs, out_specs=out_specs, check_vma=False)
```

profile of v0, /device:TPU:0, one launch (start us, length us, event | category | flops | bytes accessed | tf_op | source)
XLA Modules:
  0.0 159.9 jit_solution(14502547936491669466)
XLA Ops:
  7.3 2.0 %pad_maximum_fusion = bf16[64,4096]{1,0:T(8,128)(2,1)} fusion(bf16[64,2048]{1,0:T(8,128)(2,1)} %bitcast.109, bf16[64,2048]{1,0:T(8,128)(2,1)} %bitcast.110), kind=kLoop, calls=%fused_computation.41 | loop fusion | flops 1048576 | bytes 1048576 | tf_op jit(solution)/shard_map/concatenate | solution.py:26
  9.4 1.1 fusion.32
  10.4 1.7 %fusion.54 = f32[48,256]{1,0:T(8,128)S(1)} fusion(bf16[2048,256]{1,0:T(8,128)(2,1)} %param.26, bf16[48,2048]{1,0:T(8,128)(2,1)} %param.24, f32[2048]{0:T(1024)} %param.25, f32[48]{0:T(128)S(1)} %add_rsqrt_fusion.1), kind=kOutput, calls=%fused_computation.101 | convolution fusion | flops 50724864 | bytes 1302720 | tf_op jit(solution)/shard_map/dot_general | solution.py:81
  12.1 0.6 reshape.212
  12.8 1.2 convolution_add_fusion.1
  14.0 1.2 subtract_exponential_fusion
  15.3 0.7 copy.85
  16.1 1.0 fusion.50
  17.2 0.3 fusion.48
  17.5 1.6 %multiply_reduce_fusion.1 = (f32[48,2]{1,0:T(8,128)S(1)}, f32[48,2,128]{2,1,0:T(2,128)}, f32[48,2,128]{2,1,0:T(2,128)S(1)}) fusion(f32[48,2,128]{2,1,0:T(2,128)} %reshape.212, f32[48,2,128]{2,1,0:T(2,128)} %param.36, f32[48,2]{1,0:T(8,128)S(1)} %copy.84, f32[48,2,128]{2,1,0:T(2,128)S(1)} %reshape.213, f32[48,2]{1,0:T(8,128)} %copy.85), kind=kLoop, calls=%fused_computation.63 | loop fusion | flops 61344 | bytes 246912 | tf_op jit(solution)/shard_map/reduce_sum | solution.py:98
  19.3 4.6 %multiply_add_fusion = f32[48,2,128,128]{3,2,1,0:T(8,128)S(1)} fusion(f32[48,2,128,128]{3,2,1,0:T(8,128)} %param.35, f32[48,2,128]{2,1,0:T(2,128)S(1)} %mul.166, f32[48,2,128]{2,1,0:T(2,128)S(1)} %get-tuple-element.6, f32[48,2]{1,0:T(8,128)S(1)} %copy.84), kind=kLoop, calls=%fused_computation.2 | loop fusion | flops 4718592 | bytes 12681600 | tf_op jit(solution)/shard_map/add | solution.py:94
  24.0 5.5 %fusion.57 = f32[48,2,1,128]{3,2,1,0:T(1,128)S(1)} fusion(f32[48,2,128,1]{2,3,1,0:T(1,128)S(1)} %bitcast.111, f32[48,2,128,128]{3,2,1,0:T(8,128)S(1)} %multiply_add_fusion), kind=kOutput, calls=%fused_computation.102 | convolution fusion | flops 18874368 | bytes 6389760 | tf_op jit(solution)/shard_map/bhd,bhde->bhe/dot_general | solution.py:97
  29.5 0.1 broadcast_divide_fusion
  29.6 0.4 fusion.10
  30.0 11.2 %all_to_all.44 = bf16[4,48,256]{2,1,0:T(8,128)(2,1)S(1)} all-to-all(bf16[4,48,256]{2,1,0:T(8,128)(2,1)S(1)} %broadcast_in_dim.37), channel_id=1, replica_groups=mesh['ep'=32,'tp'=4] {'tp'}, dimensions={0} | all-to-all | bytes 196608 | tf_op jit(solution)/shard_map/all_to_all | solution.py:17
  41.2 1.0 fusion.29
  42.2 0.8 fusion.31
  43.1 0.1 reshape.216
  43.2 0.2 convert_reduce_fusion.1
  43.4 0.1 select_reduce_fusion
  43.7 0.9 concatenate.6
  44.6 1.1 gather_fusion
  45.8 0.3 gather.13
  46.1 0.2 select_bitcast_fusion
  46.3 28.2 %all_to_all.45 = bf16[32,1,6,2048]{3,2,1,0:T(8,128)(2,1)S(1)} all-to-all(bf16[32,1,6,2048]{3,2,1,0:T(8,128)(2,1)S(1)} %select_bitcast_fusion), channel_id=1, replica_groups=mesh['ep'=32,'tp'=4] {'ep'}, dimensions={0} | all-to-all | bytes 1572864 | tf_op jit(solution)/shard_map/all_to_all | solution.py:183
  74.5 0.7 convolution_bitcast_fusion.1
  75.1 2.3 %convolution_convert_fusion = bf16[32,6,2048]{2,0,1:T(8,128)(2,1)S(1)} fusion(bf16[1,256,2048]{2,1,0:T(8,128)(2,1)S(1)} %copy-done, bf16[1,2048,256]{2,1,0:T(8,128)(2,1)} %param.42, bf16[32,1,6,2048]{3,2,1,0:T(8,128)(2,1)S(1)} %all_to_all.45, f32[32,1,6,256]{3,0,2,1:T(8,128)S(1)} %convolution_bitcast_fusion.1), kind=kOutput, calls=%fused_computation.8 | convolution fusion | flops 403341312 | bytes 3866624 | tf_op jit(solution)/shard_map/secf,efd->secd/dot_general | solution.py:189
  77.4 1.0 copy.120
  78.5 3.5 %all-to-all-start.2 = ((bf16[4,32,1,6,512]{4,1,3,2,0:T(8,128)(2,1)}), bf16[4,32,1,6,512]{4,1,3,2,0:T(8,128)(2,1)S(1)}, u32[]{:S(2)}, u32[]{:S(2)}) async-start(bf16[4,32,1,6,512]{4,1,3,2,0:T(8,128)(2,1)} %bitcast.100), calls=%async_computation.2 | async-start | bytes 1572864 | tf_op jit(solution)/shard_map/all_to_all | solution.py:43
  82.0 0.7 copy.121
  82.7 12.2 %all-to-all-done.2 = bf16[4,32,1,6,512]{4,1,3,2,0:T(8,128)(2,1)S(1)} async-done(((bf16[4,32,1,6,512]{4,1,3,2,0:T(8,128)(2,1)}), bf16[4,32,1,6,512]{4,1,3,2,0:T(8,128)(2,1)S(1)}, u32[]{:S(2)}, u32[]{:S(2)}) %all-to-all-start.2) | async-done | bytes 786464 | tf_op jit(solution)/shard_map/all_to_all | solution.py:43
  94.9 3.6 %all-to-all-start.4 = ((bf16[64,4,512]{2,0,1:T(8,128)(2,1)}), bf16[64,4,512]{2,0,1:T(8,128)(2,1)S(1)}, u32[]{:S(2)}, u32[]{:S(2)}) async-start(bf16[64,4,512]{2,0,1:T(8,128)(2,1)} %bitcast.101), calls=%async_computation.4 | async-start | bytes 524288 | tf_op jit(solution)/shard_map/all_to_all | solution.py:157
  98.5 0.1 reduce_sum.87
  98.6 0.8 copy.97
  99.5 1.2 all-gather.3.cloned.1.call-done
  100.7 6.2 %fusion.14 = f32[1536,256]{1,0:T(8,128)} fusion(bf16[1536,2048]{1,0:T(8,128)(2,1)} %all-gather.3.cloned.1.call-done, bf16[256,4096]{1,0:T(8,128)(2,1)} %all-gather.5.cloned.1.call-done), kind=kOutput, calls=%fused_computation.27 | convolution fusion | flops 1610612736 | bytes 8912896 | tf_op jit(solution)/shard_map/dot_general | solution.py:54
  106.9 1.7 %convolution_reduce_fusion = f32[1536]{0:T(1024)S(1)} fusion(bf16[1536,2048]{1,0:T(8,128)(2,1)S(1)} %copy-done.2, bf16[2048,1]{0,1:T(2,128)(2,1)S(1)} %reshape.249), kind=kOutput, calls=%fused_computation.22 | convolution fusion | flops 6291456 | bytes 6301696 | tf_op jit(solution)/shard_map/dot_general | solution.py:60
  108.7 4.7 %all-to-all-start.3 = ((bf16[32,1,6,512]{3,2,1,0:T(8,128)(2,1)}), bf16[32,1,6,512]{3,2,1,0:T(8,128)(2,1)S(1)}, u32[]{:S(2)}, u32[]{:S(2)}) async-start(bf16[32,1,6,512]{3,2,1,0:T(8,128)(2,1)} %copy.97), calls=%async_computation.3 | async-start | bytes 524288 | tf_op jit(solution)/shard_map/all_to_all | solution.py:191
  113.4 7.5 %fusion = bf16[1536,512]{1,0:T(8,128)(2,1)} fusion(bf16[256,512]{1,0:T(8,128)(2,1)S(1)} %bitcast.108, f32[1536]{0:T(1024)S(1)} %add_divide_fusion, bf16[1536,2048]{1,0:T(8,128)(2,1)} %all-gather.3.cloned.1.call-done, f32[1536,256]{1,0:T(8,128)} %fusion.14, bf16[256,4096]{1,0:T(8,128)(2,1)} %all-gather.5.cloned.1.call-done), kind=kOutput, calls=%fused_computation.5 | convolution fusion | flops 2017198080 | bytes 10754048 | tf_op jit(solution)/shard_map/dot_general | solution.py:159
  120.9 1.2 all-to-all-done.3
  122.1 6.1 %all-to-all-start.5 = ((bf16[32,48,512]{2,1,0:T(8,128)(2,1)}), bf16[32,48,512]{2,1,0:T(8,128)(2,1)S(1)}, u32[]{:S(2)}, u32[]{:S(2)}) async-start(bf16[32,48,512]{2,1,0:T(8,128)(2,1)} %bitcast.102), calls=%async_computation.5 | async-start | bytes 3145728 | tf_op jit(solution)/shard_map/all_to_all | solution.py:43
  128.3 0.1 reduce_sum.84
  128.5 0.1 mul.185
  129.0 0.7 gather_fusion.1
  129.8 0.3 multiply_reduce_fusion
  130.2 22.0 %all-to-all-done.5 = bf16[32,48,512]{2,1,0:T(8,128)(2,1)S(1)} async-done(((bf16[32,48,512]{2,1,0:T(8,128)(2,1)}), bf16[32,48,512]{2,1,0:T(8,128)(2,1)S(1)}, u32[]{:S(2)}, u32[]{:S(2)}) %all-to-all-start.5) | async-done | bytes 1572896 | tf_op jit(solution)/shard_map/all_to_all | solution.py:43
  152.2 0.2 convert_reduce_fusion
  152.4 0.6 add_convert_fusion
  (69 shorter events, 1.4 us)
Async XLA Ops:
  7.2 68.0 %copy-start = (bf16[1,256,2048]{2,1,0:T(8,128)(2,1)S(1)}, bf16[1,256,2048]{2,1,0:T(8,128)(2,1)}, u32[]{:S(2)}) copy-start(bf16[1,256,2048]{2,1,0:T(8,128)(2,1)} %param.43) | copy-start | bytes 3145732
  7.2 8.9 %copy-start.3 = (bf16[48,2048]{1,0:T(8,128)(2,1)S(1)}, bf16[48,2048]{1,0:T(8,128)(2,1)}, u32[]{:S(2)}) copy-start(bf16[48,2048]{1,0:T(8,128)(2,1)} %param.24) | copy-start | bytes 589828
  7.2 9.9 %copy-start.9 = (f32[2048]{0:T(1024)S(1)}, f32[2048]{0:T(1024)}, u32[]{:S(2)}) copy-start(f32[2048]{0:T(1024)} %param.25) | copy-start | bytes 24580
  7.2 8.9 %copy-start.5 = (bf16[2048,256]{1,0:T(8,128)(2,1)S(1)}, bf16[2048,256]{1,0:T(8,128)(2,1)}, u32[]{:S(2)}) copy-start(bf16[2048,256]{1,0:T(8,128)(2,1)} %param.27) | copy-start | bytes 3145732
  7.2 9.9 %copy-start.6 = (bf16[2048,256]{1,0:T(8,128)(2,1)S(1)}, bf16[2048,256]{1,0:T(8,128)(2,1)}, u32[]{:S(2)}) copy-start(bf16[2048,256]{1,0:T(8,128)(2,1)} %param.28) | copy-start | bytes 3145732
  7.2 92.2 %all-gather.5.cloned.1.call-start = ((), (), s32[]{:S(2)}) async-start(), calls=%async_computation.7 | async-start | bytes 2621440 | tf_op jit(solution)/shard_map/all_gather | solution.py:27
  9.3 91.4 %all-gather.3.cloned.1.call-start = ((), (), s32[]{:S(2)}) async-start(), calls=%async_computation.6 | async-start | bytes 6488064 | tf_op jit(solution)/shard_map/all_gather | solution.py:155
  15.2 8.7 %copy-start.13 = (f32[48,2]{0,1:T(2,128)}, f32[48,2]{0,1:T(2,128)S(1)}, u32[]{:S(2)}) copy-start(f32[48,2]{0,1:T(2,128)S(1)} %get-tuple-element.8) | copy-start | bytes 1156
  24.0 18.2 %copy-start.1 = (f32[48,2,128,128]{3,2,1,0:T(8,128)}, f32[48,2,128,128]{3,2,1,0:T(8,128)S(1)}, u32[]{:S(2)}) copy-start(f32[48,2,128,128]{3,2,1,0:T(8,128)S(1)} %multiply_add_fusion) | copy-start | bytes 18874372
  24.0 5.6 %copy-start.7 = (bf16[2048,256]{1,0:T(8,128)(2,1)S(1)}, bf16[2048,256]{1,0:T(8,128)(2,1)}, u32[]{:S(2)}) copy-start(bf16[2048,256]{1,0:T(8,128)(2,1)} %param.29) | copy-start | bytes 3145732
  24.0 17.2 %copy-start.4 = (bf16[1024,2048]{1,0:T(8,128)(2,1)S(1)}, bf16[1024,2048]{1,0:T(8,128)(2,1)}, u32[]{:S(2)}) copy-start(bf16[1024,2048]{1,0:T(8,128)(2,1)} %param.34) | copy-start | bytes 12582916
  29.5 12.7 %copy-start.11 = (f32[2048]{0:T(1024)S(1)}, f32[2048]{0:T(1024)}, u32[]{:S(2)}) copy-start(f32[2048]{0:T(1024)} %param.38) | copy-start | bytes 24580
  29.5 13.5 %copy-start.10 = (s32[48,2]{0,1:T(2,128)S(1)}, s32[48,2]{0,1:T(2,128)}, u32[]{:S(2)}) copy-start(s32[48,2]{0,1:T(2,128)} %param.39) | copy-start | bytes 1156
  46.1 28.4 %copy-start.15 = (bf16[1,2048,256]{2,1,0:T(8,128)(2,1)S(1)}, bf16[1,2048,256]{2,1,0:T(8,128)(2,1)}, u32[]{:S(2)}) copy-start(bf16[1,2048,256]{2,1,0:T(8,128)(2,1)} %param.41) | copy-start | bytes 3145732
  74.4 7.5 %copy-start.12 = (bf16[2048]{0:T(1024)(128)(2,1)S(1)}, bf16[2048]{0:T(1024)(128)(2,1)}, u32[]{:S(2)}) copy-start(bf16[2048]{0:T(1024)(128)(2,1)} %param.44) | copy-start | bytes 12292
  74.4 7.6 %copy-start.8 = (bf16[64,2048]{1,0:T(8,128)(2,1)S(1)}, bf16[64,2048]{1,0:T(8,128)(2,1)}, u32[]{:S(2)}) copy-start(bf16[64,2048]{1,0:T(8,128)(2,1)} %param.47) | copy-start | bytes 786436
  78.5 16.4 %all-to-all-start.2 = ((bf16[4,32,1,6,512]{4,1,3,2,0:T(8,128)(2,1)}), bf16[4,32,1,6,512]{4,1,3,2,0:T(8,128)(2,1)S(1)}, u32[]{:S(2)}, u32[]{:S(2)}) async-start(bf16[4,32,1,6,512]{4,1,3,2,0:T(8,128)(2,1)} %bitcast.100), calls=%async_computation.2 | async-start | bytes 1572864 | tf_op jit(solution)/shard_map/all_to_all | solution.py:43
  94.9 13.8 %all-to-all-start.4 = ((bf16[64,4,512]{2,0,1:T(8,128)(2,1)}), bf16[64,4,512]{2,0,1:T(8,128)(2,1)S(1)}, u32[]{:S(2)}, u32[]{:S(2)}) async-start(bf16[64,4,512]{2,0,1:T(8,128)(2,1)} %bitcast.101), calls=%async_computation.4 | async-start | bytes 524288 | tf_op jit(solution)/shard_map/all_to_all | solution.py:157
  100.7 6.3 %copy-start.2 = (bf16[1536,2048]{1,0:T(8,128)(2,1)S(1)}, bf16[1536,2048]{1,0:T(8,128)(2,1)}, u32[]{:S(2)}) copy-start(bf16[1536,2048]{1,0:T(8,128)(2,1)} %all-gather.3.cloned.1.call-done) | copy-start | bytes 18874372
  108.7 13.4 %all-to-all-start.3 = ((bf16[32,1,6,512]{3,2,1,0:T(8,128)(2,1)}), bf16[32,1,6,512]{3,2,1,0:T(8,128)(2,1)S(1)}, u32[]{:S(2)}, u32[]{:S(2)}) async-start(bf16[32,1,6,512]{3,2,1,0:T(8,128)(2,1)} %copy.97), calls=%async_computation.3 | async-start | bytes 524288 | tf_op jit(solution)/shard_map/all_to_all | solution.py:191
  113.4 15.5 %copy-start.14 = (f32[48,2]{0,1:T(2,128)S(1)}, f32[48,2]{0,1:T(2,128)}, u32[]{:S(2)}) copy-start(f32[48,2]{0,1:T(2,128)} %param.40) | copy-start | bytes 1156
  122.1 30.1 %all-to-all-start.5 = ((bf16[32,48,512]{2,1,0:T(8,128)(2,1)}), bf16[32,48,512]{2,1,0:T(8,128)(2,1)S(1)}, u32[]{:S(2)}, u32[]{:S(2)}) async-start(bf16[32,48,512]{2,1,0:T(8,128)(2,1)} %bitcast.102), calls=%async_computation.5 | async-start | bytes 3145728 | tf_op jit(solution)/shard_map/all_to_all | solution.py:43
Sparse Core Ops, SparseCore 0:
  9.7 34.2 all-gather.4
  46.3 54.3 all-gather.2
where the time goes:
time: 161 us; the launch traced here: 160 us
  blocking collectives  39.3 us (24%)
  waiting for transfers between devices  36.7 us (23%)
  matrix products  30.8 us (19%)
  starting transfers between devices  17.9 us (11%)
  between operations  14.5 us (9%)
  other arithmetic  12.2 us (8%)
  local copies, waits for them, and re-layouts  8.49 us (5%)
    all_to_all x2, waiting for transfers between devices, summed_on_arrival(): lax.all_to_all(parts, axis, split_axis=0, concat_axis=0, tiled=True)  34.2 us
    all_to_all x1, blocking collectives, local(): lax.all_to_all(dispatch, 'ep', split_axis=0, concat_axis=0, tiled=True)  28.2 us
    all_to_all x1, blocking collectives, sent_to_all(): return lax.all_to_all(copies, axis, split_axis=0, concat_axis=0, tiled=True)  11.2 us
    all_to_all x2, starting transfers between devices, summed_on_arrival(): lax.all_to_all(parts, axis, split_axis=0, concat_axis=0, tiled=True)  9.63 us
    dot_general x1, matrix products, local(): jnp.dot(hidden, down_block, preferred_element_type=jnp.float32)  7.52 us
    dot_general x1, matrix products, swiglu(): gate_proj = jnp.dot(tok_rows, gate_w, preferred_element_type=jnp.float32)  6.25 us
    dot_general x6, matrix products, project(): return jnp.dot(normed, weight, preferred_element_type=jnp.float32)  5.85 us
    dot_general x1, matrix products, cell_step(): jnp.einsum('bhd,bhde->bhe', queries, new_cell, precision=lax.Precision.HI...  5.45 us
  transfers between devices with their start and end apart: 6, of which 4 were waited for; matrix products, arithmetic and copies ran while one was open for 30% of the time, Pallas kernels for 0%

commit v1 on v0

v1 whole, which is shorter than its diff:
```python
import jax
import jax.numpy as jnp
from jax import lax
from jax.experimental import pallas as pl
from jax.experimental.pallas import tpu as pltpu
from jax.sharding import Mesh
from jax.sharding import PartitionSpec as P


EPS = 1e-06
BF = jnp.bfloat16
F32 = jnp.float32
EP = ("q", "c")
ALL = ("q", "c", "x")
CORES = 2
VMEM = pl.BlockSpec(memory_space=pltpu.VMEM)
SMEM = pl.BlockSpec(memory_space=pltpu.SMEM)
ANY = pl.BlockSpec(memory_space=pl.ANY)


def params(mib=60):
    return pltpu.CompilerParams(vmem_limit_bytes=mib * 1024 * 1024)


def far_memory(array):
    return pltpu.with_memory_space_constraint(array, pltpu.HBM)


def near_memory(array):
    return pltpu.with_memory_space_constraint(array, pltpu.VMEM)


def nt_dot(left, right):
    return lax.dot_general(left, right, (((1,), (1,)), ((), ())), preferred_element_type=F32)


def normed_rows(rows_in, gain_vec):
    as_float = rows_in.astype(F32)
    mean = jnp.mean(as_float * as_float, axis=-1, keepdims=True)
    return (as_float * lax.rsqrt(mean + EPS) * gain_vec).astype(BF)


def log_sigmoid(x):
    return -(jnp.maximum(-x, 0.0) + jnp.log1p(jnp.exp(-jnp.abs(x))))


def gate_factors(in_pre, forget_pre, max_state):
    log_forget = log_sigmoid(forget_pre)
    new_max = jnp.maximum(log_forget + max_state, in_pre)
    return jnp.exp(log_forget + max_state - new_max), jnp.exp(in_pre - new_max), new_max


def padded_transpose(block):
    rows, cols = block.shape
    if rows < 128:
        block = jnp.concatenate([block, jnp.zeros((128 - rows, cols), block.dtype)], axis=0)
    return block.T


def front_kernel(
    tok, gain, wq, wk, wv, wo, w_in, w_fg, in_bias, fg_bias, cell, norm, mx,
    heads_o, carry_o, written_o, value_o, norm_o, max_o,
    wbuf, cbuf, num, wsem, csem,
):
    rows, head_count, hd = cbuf.shape[:3]
    chunks = csem.shape[0]
    per = rows // chunks
    weights = (wq, wk, wv, wo)
    loads = [pltpu.make_async_copy(w, wbuf.at[i], wsem.at[i]) for i, w in enumerate(weights)]
    parts = [
        pltpu.make_async_copy(cell.at[pl.ds(j * per, per)], cbuf.at[pl.ds(j * per, per)], csem.at[j])
        for j in range(chunks)
    ]
    for copy in loads + parts:
        copy.start()
    normed = normed_rows(tok[...], gain[...])
    in_row = nt_dot(w_in[...], normed)
    fg_row = nt_dot(w_fg[...], normed)
    factors = []
    for h in range(head_count):
        found = gate_factors(
            in_row[h : h + 1] + in_bias[h], fg_row[h : h + 1] + fg_bias[h], mx[h : h + 1]
        )
        max_o[h : h + 1] = found[2]
        factors += found
    factors.append(jnp.zeros((8 - len(factors), rows), F32))
    same = lax.broadcasted_iota(jnp.int32, (rows, rows), 0) == lax.broadcasted_iota(
        jnp.int32, (rows, rows), 1
    )
    columns = lax.dot_general(
        same.astype(F32),
        jnp.concatenate(factors, axis=0),
        (((1,), (1,)), ((), ())),
        preferred_element_type=F32,
        precision=lax.Precision.HIGHEST,
    )

    def project(i):
        loads[i].wait()
        return jnp.dot(normed, wbuf[i], preferred_element_type=F32)

    queries = project(0)
    keys = project(1) * hd ** (-0.5)
    values = project(2)
    outgate = project(3)
    turned = [padded_transpose(queries[:, h * hd : (h + 1) * hd]) for h in range(head_count)]
    for j in range(chunks):
        parts[j].wait()
        for b in range(j * per, (j + 1) * per):
            for h in range(head_count):
                num[h, b : b + 1] = jnp.sum(
                    turned[h][:, b : b + 1] * cbuf[b, h], axis=0, keepdims=True
                )
    for h in range(head_count):
        cols = slice(h * hd, (h + 1) * hd)
        carry, write, new_max = (columns[:, 3 * h + k : 3 * h + k + 1] for k in range(3))
        query, value = queries[:, cols], values[:, cols]
        written = write * keys[:, cols]
        at = pl.ds(h, rows, stride=head_count)
        new_norm = carry * norm[at, :] + written
        norm_o[at, :] = new_norm
        written_o[at, :] = written
        value_o[at, :] = value
        carry_o[at, :] = jnp.broadcast_to(carry, (rows, hd))
        numerator = carry * num[h] + jnp.sum(query * written, axis=-1, keepdims=True) * value
        denominator = jnp.sum(query * new_norm, axis=-1, keepdims=True)
        cell_out = numerator / jnp.maximum(jnp.abs(denominator), jnp.exp(-new_max))
        gated = (jax.nn.sigmoid(outgate[:, cols]) * cell_out).astype(BF)
        heads_o[:, cols] = gated


def update_kernel(carry, written, value, cell, out):
    turned = padded_transpose(written[...])
    for p in range(cell.shape[0]):
        out[p] = carry[p : p + 1] * cell[p] + turned[:, p : p + 1] * value[p : p + 1]


def over(index, divisor):
    factor, shift = {6: (10923, 16), 24: (43691, 20)}[divisor]
    return (index * factor) >> shift


def route_kernel(place, ids, select_o, slots_o):
    seqs = ids.shape[1]
    lanes = select_o.shape[1]
    row = lax.broadcasted_iota(jnp.int32, (seqs, seqs), 0)
    col = lax.broadcasted_iota(jnp.int32, (seqs, seqs), 1)
    first, second = ids[0:1], ids[1:2]
    here = lax.broadcasted_iota(jnp.int32, (seqs, lanes), 0)
    there = lax.broadcasted_iota(jnp.int32, (seqs, lanes), 1)
    slot_rows = []
    slots = jnp.zeros((seqs, lanes), jnp.int32)
    for k, own in enumerate((first, second)):
        column = jnp.sum(jnp.where(row == col, own, 0), axis=1, keepdims=True)
        same = ((column == first) | (column == second)) & (col < row)
        slot = column * 6 + jnp.sum(jnp.where(same, 1, 0), axis=1, keepdims=True)
        slots = jnp.where(there == k, slot, slots)
        slot_rows.append(
            jnp.sum(jnp.where((there & 63) == here, slot + 1, 0), axis=0, keepdims=True) - 1
        )
    slots_o[...] = slots
    size = select_o.shape[0]
    line = lax.broadcasted_iota(jnp.int32, (size, 1), 0)
    lane = lax.broadcasted_iota(jnp.int32, (1, lanes), 1)
    e = over(line, 24)
    inner = line - 24 * e
    part = over(inner, 6)
    entry = inner - 6 * part
    side, is_moe = part >> 1, part & 1
    dense_row = jnp.where(is_moe == 0, (place[0] * CORES + (e & 1)) * 6 + entry, -1)
    slot = jnp.where(is_moe == 1, e * 6 + entry, -2)
    hit = (dense_row == (lane & 63)) | (slot == slot_rows[0]) | (slot == slot_rows[1])
    select_o[...] = jnp.where(hit & (side == lane >> 6), 1.0, 0.0).astype(BF)


def plan_kernel(slots, picks_o, gather_o, spread_o):
    seqs = slots.shape[0]
    lanes = picks_o.shape[1]
    lane = lax.broadcasted_iota(jnp.int32, (1, lanes), 1)
    source = over(lane, 24)
    inner = lane - 24 * source
    part = over(inner, 6)
    entry = inner - 6 * part
    side, is_moe = part >> 1, part & 1
    from_x, from_c, from_e = source & 3, (source >> 2) & 1, source >> 2
    dense_row = jnp.where(is_moe == 0, (from_x * CORES + from_c) * 6 + entry, -1)
    slot = jnp.where(is_moe == 1, from_e * 6 + entry, -1)
    row = lax.broadcasted_iota(jnp.int32, (seqs, 1), 0)
    for k in range(3):
        if k == 0:
            hit = jnp.where(dense_row == row, 1.0, 0.0)
        else:
            hit = jnp.where(slot == slots[:, k - 1 : k], 1.0, 0.0)
        for h in range(2):
            at = (2 * k + h) * seqs
            picks_o[at : at + seqs] = jnp.where(side == h, hit, 0.0).astype(BF)
    size = gather_o.shape[0]
    col = lax.broadcasted_iota(jnp.int32, (1, size), 1)
    e = over(col, 24)
    inner = col - 24 * e
    part = over(inner, 6)
    grouped = part * (size // 4) + e * 6 + inner - 6 * part
    row = lax.broadcasted_iota(jnp.int32, (size, 1), 0)
    gather_o[...] = jnp.where(grouped == row, 1.0, 0.0).astype(BF)
    e = over(row, 24)
    inner = row - 24 * e
    part = over(inner, 6)
    grouped = part * (size // 4) + e * 6 + inner - 6 * part
    spread_o[...] = jnp.where(grouped == col, 1.0, 0.0).astype(BF)


def mix_kernel(
    place, heads, heads_l, heads_r, heads_f, w_mix, tok, gain, branch, select,
    send_o, own_o, weight_o,
    wbuf, sems,
):
    width = heads.shape[1]
    turns = (0, 3, 1, 2)
    loads = []
    for i, turn in enumerate(turns):
        start = pl.multiple_of(((place[0] + turn) & 3) * width, width)
        loads.append(pltpu.make_async_copy(w_mix.at[pl.ds(start, width)], wbuf.at[i], sems.at[i]))
        loads[i].start()
    mixed_proj = None
    for i, block in enumerate((heads, heads_l, heads_r, heads_f)):
        loads[i].wait()
        part = jnp.dot(block[...], wbuf[i], preferred_element_type=F32)
        mixed_proj = part if mixed_proj is None else mixed_proj + part
    residual = (tok[...].astype(F32) + mixed_proj).astype(BF)
    moe_in = normed_rows(residual, gain[...])
    half = send_o.shape[1]
    gap = jnp.zeros((select.shape[1] // 2 - moe_in.shape[0], half), BF)
    stacked = jnp.concatenate([moe_in[:, :half], gap, moe_in[:, half:], gap], axis=0)
    send_o[...] = jnp.dot(select[...], stacked, preferred_element_type=F32).astype(BF)
    cols = own_o.shape[1]
    own = residual[:, :cols]
    for k in range(1, residual.shape[1] // cols):
        own = jnp.where(place[0] == k, residual[:, k * cols : (k + 1) * cols], own)
    own_o[...] = own
    logit = jnp.sum(moe_in.astype(F32) * branch[...].astype(F32), axis=-1, keepdims=True)
    weight_o[...] = jnp.broadcast_to(jax.nn.sigmoid(logit), weight_o.shape)


def ffn_kernel(
    abuf, gather, spread, e_gate, e_up, e_down, *rest
):
    gates, boths = rest[:8], rest[8:16]
    out, gabuf, spbuf, egbuf, eubuf, edbuf, gbuf, ubuf, dbuf, xbuf, obuf, sems, osems = rest[16:]
    units = gates[0].shape[0]
    pairs = [
        (gather, gabuf), (e_gate, egbuf), (e_up, eubuf), (e_down, edbuf),
    ]
    for b in range(8):
        rows = pl.ds(b * units, units)
        pairs.append((gates[b], gbuf.at[rows]))
        pairs.append((boths[b].at[pl.ds(0, units)], ubuf.at[rows]))
        pairs.append((boths[b].at[pl.ds(units, units)], dbuf.at[rows]))
    pairs.append((spread, spbuf))
    loads = [pltpu.make_async_copy(src, dst, sems.at[i]) for i, (src, dst) in enumerate(pairs)]
    for copy in loads:
        copy.start()
    loads[0].wait()
    size, half = abuf.shape[0] // 4, abuf.shape[1]
    for part in range(4):
        piece = jnp.dot(
            gabuf[part * size : (part + 1) * size], abuf[...], preferred_element_type=F32
        )
        xbuf[part % 2, :, (part // 2) * half : (part // 2 + 1) * half] = piece.astype(BF)
    tok = xbuf[1]
    loads[1].wait()
    loads[2].wait()
    gate_proj = jnp.dot(tok, egbuf[0], preferred_element_type=F32)
    up_proj = jnp.dot(tok, eubuf[0], preferred_element_type=F32)
    hidden = (jax.nn.silu(gate_proj) * up_proj).astype(BF)
    loads[3].wait()
    expert_out = jnp.dot(hidden, edbuf[0], preferred_element_type=F32).astype(BF)
    tok = xbuf[0]
    total = None
    for side in range(2):
        for copy in loads[4 + 12 * side : 16 + 12 * side]:
            copy.wait()
        rows = slice(side * 4 * units, (side + 1) * 4 * units)
        hidden = (jax.nn.silu(nt_dot(tok, gbuf[rows])) * nt_dot(tok, ubuf[rows])).astype(BF)
        part = jnp.dot(hidden, dbuf[rows], preferred_element_type=F32)
        total = part if total is None else total + part
    total = total.astype(BF)
    loads[-1].wait()
    peers, quarter = obuf.shape[0], obuf.shape[3]
    stores = []
    for s in range(peers):
        sides = []
        for h in range(2):
            at = (2 * s + h) * quarter
            sides += [total[:, at : at + quarter], expert_out[:, at : at + quarter]]
        block = jnp.dot(spbuf[...], jnp.concatenate(sides, axis=0), preferred_element_type=F32)
        obuf[s] = block.reshape(obuf.shape[1:]).astype(BF)
        stores.append(pltpu.make_async_copy(obuf.at[s], out.at[:, s], osems.at[s]))
        stores[s].start()
    for copy in stores:
        copy.wait()


def final_kernel(picks, returned, own, weight, route_w, out):
    sums = jnp.dot(picks[...], returned[...], preferred_element_type=F32)
    seqs, quarter = own.shape[0], returned.shape[1]
    for h in range(2):
        dense, first, second = (
            sums[(2 * k + h) * seqs : (2 * k + h + 1) * seqs] for k in range(3)
        )
        cols = slice(h * quarter, (h + 1) * quarter)
        total = own[:, cols].astype(F32) + (route_w[:, :1] * first + route_w[:, 1:2] * second)
        out[:, cols] = (total + weight[:, :1] * dense).astype(BF)


def shape(*dims, dtype=F32):
    return jax.ShapeDtypeStruct(dims, dtype)


def local(
    tokens,
    mix_gain,
    w_query,
    w_key,
    w_value,
    w_outgate,
    w_ingate,
    w_forget,
    in_bias,
    forget_bias,
    w_mix_out,
    cell_state,
    norm_state,
    max_state,
    moe_gain,
    route_ids,
    route_weights,
    expert_gate,
    expert_up,
    expert_down,
    branch_gate,
    dense_gate,
    dense_up,
    dense_down,
):
    seqs, width = tokens.shape
    tp_count = lax.axis_size("x")
    chips = lax.axis_size("q")
    ep_count = chips * CORES
    place = lax.axis_index("x")
    cols = width // tp_count
    half = width // 2
    head_count, hd = cell_state.shape[1:3]
    pair_rows = seqs * head_count
    groups = tp_count * CORES
    share = seqs // groups
    capacity = max(2, 4 * seqs // ep_count)
    swap = [(0, 1), (1, 0)]

    right = [(i, (i + 1) % tp_count) for i in range(tp_count)]
    left = [(i, (i - 1) % tp_count) for i in range(tp_count)]
    across = [(i, (i + 2) % tp_count) for i in range(tp_count)]

    gate = dense_gate.T
    gate_l = lax.ppermute(gate, "x", right)
    gate_r = lax.ppermute(gate, "x", left)
    both = jnp.concatenate([dense_up.T, dense_down], axis=0)
    front_bytes = w_query.size * 4 * 2 + cell_state.size * 4
    heads, carry, written, value, new_norm, new_max = pl.pallas_call(
        front_kernel,
        in_specs=[VMEM, VMEM, ANY, ANY, ANY, ANY, VMEM, VMEM, SMEM, SMEM, ANY, VMEM, VMEM],
        out_specs=[VMEM] * 6,
        out_shape=[
            shape(seqs, head_count * hd, dtype=BF),
            shape(pair_rows, hd),
            shape(pair_rows, hd),
            shape(pair_rows, hd),
            shape(pair_rows, hd),
            shape(head_count, seqs),
        ],
        scratch_shapes=[
            pltpu.VMEM((4, *w_query.shape), BF),
            pltpu.VMEM(cell_state.shape, F32),
            pltpu.VMEM((head_count, seqs, hd), F32),
            pltpu.SemaphoreType.DMA((4,)),
            pltpu.SemaphoreType.DMA((6,)),
        ],
        compiler_params=params(),
        cost_estimate=pl.CostEstimate(
            flops=2 * seqs * width * 4 * head_count * hd, transcendentals=0, bytes_accessed=front_bytes
        ),
        name="front",
    )(
        tokens,
        mix_gain.reshape(1, width),
        far_memory(w_query),
        far_memory(w_key),
        far_memory(w_value),
        far_memory(w_outgate),
        w_ingate.T,
        w_forget.T,
        in_bias,
        forget_bias,
        far_memory(cell_state),
        norm_state.reshape(pair_rows, hd),
        max_state.T,
    )
    heads_l = lax.ppermute(heads, "x", right)
    heads_r = lax.ppermute(heads, "x", left)
    heads_f = lax.ppermute(heads, "x", across)
    both_l = lax.ppermute(both, "x", right)
    both_r = lax.ppermute(both, "x", left)
    gate_f = lax.ppermute(gate_l, "x", right)
    both_f = lax.ppermute(both_r, "x", left)
    gates, boths = [gate, gate_l, gate_r, gate_f], [both, both_l, both_r, both_f]
    gates += [lax.ppermute(w, "c", swap) for w in gates[:3]]
    boths += [lax.ppermute(w, "c", swap) for w in boths[:3]]
    gates.append(lax.ppermute(gate_f, "c", swap))
    boths.append(lax.ppermute(both_f, "c", swap))

    chunk_rows = 2 * (share + capacity)
    total_rows = ep_count * chunk_rows
    select, slots = pl.pallas_call(
        route_kernel,
        in_specs=[SMEM, VMEM],
        out_specs=[VMEM] * 2,
        out_shape=[
            shape(total_rows, 128, dtype=BF),
            shape(seqs, 128, dtype=jnp.int32),
        ],
        compiler_params=params(),
        name="route",
    )(place.reshape(1), route_ids.T)

    send, own, weight = pl.pallas_call(
        mix_kernel,
        in_specs=[SMEM] + [VMEM] * 4 + [ANY] + [VMEM] * 4,
        out_specs=[VMEM] * 3,
        out_shape=[
            pltpu.HBM((ep_count * chunk_rows, half), BF),
            shape(seqs, cols, dtype=BF),
            shape(seqs, 128),
        ],
        scratch_shapes=[
            pltpu.VMEM((tp_count, w_mix_out.shape[0] // tp_count, width), BF),
            pltpu.SemaphoreType.DMA((tp_count,)),
        ],
        compiler_params=params(40),
        cost_estimate=pl.CostEstimate(
            flops=2 * seqs * width * w_mix_out.shape[0], transcendentals=0, bytes_accessed=w_mix_out.size * 2
        ),
        name="mix",
    )(
        place.reshape(1),
        near_memory(heads),
        near_memory(heads_l),
        near_memory(heads_r),
        near_memory(heads_f),
        *(far_memory(a) for a in (w_mix_out, tokens, moe_gain.reshape(1, width))),
        *(far_memory(a) for a in (branch_gate.reshape(1, width), select)),
    )
    arrived = lax.all_to_all(
        send.reshape(ep_count, chunk_rows, half), EP, split_axis=0, concat_axis=0, tiled=True
    )
    sources = ep_count * tp_count
    quarter = cols // 2
    picks, gather, spread = pl.pallas_call(
        plan_kernel,
        in_specs=[VMEM],
        out_specs=[VMEM] * 3,
        out_shape=[
            pltpu.HBM((6 * seqs, sources * chunk_rows), BF),
            pltpu.HBM((total_rows, total_rows), BF),
            pltpu.HBM((total_rows, total_rows), BF),
        ],
        compiler_params=params(),
        name="plan",
    )(slots)
    many = ep_count * share
    units = gate.shape[0]
    back = pl.pallas_call(
        ffn_kernel,
        in_specs=[VMEM] + [ANY] * 21,
        out_specs=ANY,
        out_shape=pltpu.HBM((ep_count, tp_count, chunk_rows, quarter), BF),
        scratch_shapes=[
            pltpu.VMEM((total_rows, total_rows), BF),
            pltpu.VMEM((total_rows, total_rows), BF),
            pltpu.VMEM(expert_gate.shape, BF),
            pltpu.VMEM(expert_up.shape, BF),
            pltpu.VMEM(expert_down.shape, BF),
            pltpu.VMEM((8 * units, width), BF),
            pltpu.VMEM((8 * units, width), BF),
            pltpu.VMEM((8 * units, width), BF),
            pltpu.VMEM((2, many, width), BF),
            pltpu.VMEM((tp_count, ep_count, chunk_rows, quarter), BF),
            pltpu.SemaphoreType.DMA((29,)),
            pltpu.SemaphoreType.DMA((tp_count,)),
        ],
        compiler_params=params(46),
        cost_estimate=pl.CostEstimate(
            flops=6 * many * width * (8 * units + expert_down.shape[1]),
            transcendentals=0,
            bytes_accessed=6 * width * (8 * units + expert_down.shape[1]),
        ),
        name="ffn",
    )(near_memory(arrived.reshape(total_rows, half)), *(far_memory(a) for a in (
        gather, spread, expert_gate, expert_up, expert_down,
        *gates, *boths,
    )))
    returned = lax.all_to_all(
        back.reshape(sources, chunk_rows, quarter), ALL, split_axis=0, concat_axis=0, tiled=True
    )
    pairs = 16
    flat = pl.BlockSpec((pairs, hd), lambda i: (i, 0))
    cube = pl.BlockSpec((pairs, hd, hd), lambda i: (i, 0, 0))
    new_cell = pl.pallas_call(
        update_kernel,
        grid=(pair_rows // pairs,),
        in_specs=[flat, flat, flat, cube],
        out_specs=cube,
        out_shape=pltpu.HBM((pair_rows, hd, hd), F32),
        compiler_params=params(),
        cost_estimate=pl.CostEstimate(
            flops=3 * cell_state.size, transcendentals=0, bytes_accessed=8 * cell_state.size
        ),
        name="update",
    )(carry, written, value, far_memory(cell_state.reshape(pair_rows, hd, hd)))
    layer_out = pl.pallas_call(
        final_kernel,
        in_specs=[VMEM] * 5,
        out_specs=VMEM,
        out_shape=shape(seqs, cols, dtype=BF),
        compiler_params=params(40),
        name="final",
    )(
        far_memory(picks),
        near_memory(returned.reshape(sources * chunk_rows, quarter)),
        *(far_memory(a) for a in (own, weight, route_weights)),
    )
    return (
        layer_out,
        new_cell.reshape(cell_state.shape),
        new_norm.reshape(norm_state.shape),
        new_max.T,
    )


def solution(mesh):
    ep_count, tp_count = mesh.shape["ep"], mesh.shape["tp"]
    mesh = Mesh(mesh.devices.reshape(ep_count // CORES, CORES, tp_count), ALL)
    in_specs = (
        P(EP, None),
        P(),
        P(None, "x"),
        P(None, "x"),
        P(None, "x"),
        P(None, "x"),
        P(None, "x"),
        P(None, "x"),
        P("x"),
        P("x"),
        P(),
        P(EP, "x", None, None),
        P(EP, "x", None),
        P(EP, "x"),
        P(),
        P(EP, None),
        P(EP, None),
        P(EP, None, "x"),
        P(EP, None, "x"),
        P(EP, "x", None),
        P(),
        P(None, ALL),
        P(None, ALL),
        P(ALL, None),
    )
    out_specs = (P(EP, "x"), P(EP, "x", None, None), P(EP, "x", None), P(EP, "x"))
    return jax.shard_map(local, mesh=mesh, in_specs=in_specs, out_specs=out_specs, check_vma=False)
```

time: 161 us -> 115 us (0.71)
  blocking collectives: 39.3 us -> 0 us
  Pallas kernels: 0 us -> 38.1 us
  matrix products: 30.8 us -> 0 us
  between operations: 14.5 us -> 0.85 us
  starting transfers between devices: 17.9 us -> 29.3 us
  other arithmetic: 12.2 us -> 1.07 us
  local copies, waits for them, and re-layouts: 8.49 us -> 4.08 us
  waiting for transfers between devices: 36.7 us -> 39.4 us
    all_to_all x2 -> x0, blocking collectives: 39.3 us -> none  [the longest x1 28.2 us: local(): lax.all_to_all(dispatch, 'ep', split_axis=0, concat_axis=0, tiled=True)]
    pallas_call x0 -> x7, Pallas kernels: none -> 38.1 us  [the longest x1 8.58 us: local(): pl.pallas_call(ffn_kernel, in_specs=[VMEM] + [ANY] * 21, out_specs=ANY, o...]
    dot_general x13 -> x0, matrix products: 30.8 us -> none  [the longest x1 7.52 us: local(): jnp.dot(hidden, down_block, preferred_element_type=jnp.float32)]
    ppermute x0 -> x17, waiting for transfers between devices: none -> 23.9 us  [the longest x1 15.6 us: local(): gate_f = lax.ppermute(gate_l, 'x', right)]
    all_to_all x4 -> x2, waiting for transfers between devices: 35.4 us -> 15.5 us  [the longest x1 15.5 us: local(): lax.all_to_all(back.reshape(sources, chunk_rows, quarter), ALL, split_axi...]
    ppermute x0 -> x17, starting transfers between devices: none -> 13.4 us  [the longest x1 3.22 us: local(): heads_r = lax.ppermute(heads, 'x', left)]
    add x2 -> x0, other arithmetic: 4.61 us -> none  [the longest x1 4.6 us: cell_step(): carry_factor[..., None, None] * cell_state]
    reduce_sum x7 -> x0, other arithmetic: 3.69 us -> none  [the longest x1 1.62 us: cell_step(): denominator = jnp.sum(queries * new_norm, axis=-1)]
  transfers between devices with their start and end apart: 6 -> 19, of which waited for: 4 -> 5; matrix products, arithmetic and copies ran while one was open for 30% -> 1% of each run, Pallas kernels for 0% -> 24%
where the time goes in v1:
time: 115 us; the launch traced here: 113 us
  waiting for transfers between devices  39.4 us (34%)
  Pallas kernels  38.1 us (33%)
  starting transfers between devices  29.3 us (25%)
  local copies, waits for them, and re-layouts  4.08 us (4%)
    ppermute x1, waiting for transfers between devices, local(): gate_f = lax.ppermute(gate_l, 'x', right)  15.6 us
    all_to_all x1, waiting for transfers between devices, local(): lax.all_to_all(back.reshape(sources, chunk_rows, quarter), ALL, split_axi...  15.5 us
    pallas_call x1, Pallas kernels, local(): pl.pallas_call(ffn_kernel, in_specs=[VMEM] + [ANY] * 21, out_specs=ANY, o...  8.58 us
    all_to_all x1, starting transfers between devices, local(): lax.all_to_all(send.reshape(ep_count, chunk_rows, half), EP, split_axis=0...  8.46 us
    pallas_call x1, Pallas kernels, local(): pl.pallas_call(update_kernel, grid=(pair_rows // pairs,), in_specs=[flat,...  8.25 us
    all_to_all x1, starting transfers between devices, local(): lax.all_to_all(back.reshape(sources, chunk_rows, quarter), ALL, split_axi...  7.51 us
    pallas_call x1, Pallas kernels, local(): pl.pallas_call(front_kernel, in_specs=[VMEM, VMEM, ANY, ANY, ANY, ANY, VM...  7.49 us
    pallas_call x1, Pallas kernels, local(): pl.pallas_call(mix_kernel, in_specs=[SMEM] + [VMEM] * 4 + [ANY] + [VMEM]...  5.37 us
  transfers between devices with their start and end apart: 19, of which 5 were waited for; matrix products, arithmetic and copies ran while one was open for 1% of the time, Pallas kernels for 24%

profile of v1, /device:TPU:0, one launch (start us, length us, event | category | flops | bytes accessed | tf_op | source)
XLA Modules:
  0.0 112.9 jit_solution(3681286722035820193)
XLA Ops:
  0.6 1.1 pad_maximum_fusion.rest_8_
  1.7 2.9 %collective-permute-start.11 = (bf16[128,2048]{1,0:T(8,128)(2,1)S(1)}, bf16[128,2048]{1,0:T(8,128)(2,1)S(1)}, u32[]{:S(2)}, u32[]{:S(2)}) collective-permute-start(bf16[128,2048]{1,0:T(8,128)(2,1)S(1)} %pad_maximum_fusion.rest_8_), channel_id=1, source_target_pairs={{0,3},{1,0},{2,1},{3,2},{4,7},{5,4},{6,5},{7,6},{8,11},{9,8},{10,9... | collective-permute-start | bytes 1572872 | tf_op jit(solution)/shard_map/ppermute | solution.py:411
  4.7 7.5 %front.1 = (bf16[48,256]{1,0:T(8,128)(2,1)}, f32[96,128]{1,0:T(8,128)}, f32[96,128]{1,0:T(8,128)}, f32[96,128]{1,0:T(8,128)}, f32[96,128]{1,0:T(8,128)}, /*index=5*/f32[2,48]{1,0:T(2,128)}) custom-call(bf16[48,2048]{1,0:T(8,128)(2,1)} %tok.3, f32[1,2048]{1,0:T(1,128)} %bitcast.30, bf16[2048,256]{1,0:T(8,128)(2,1)} %wq.1, bf16[2048,256]{1,0:T(8,128)(2,1)} %wk.1, ...), custom_call_target="tpu_custom_call" | custom-call | flops 201326592 | bytes 10485760 | tf_op jit(solution)/shard_map/front/pallas_call | solution.py:368
  12.2 0.1 collective-permute-start
  12.2 3.2 %collective-permute-start.1 = (bf16[48,256]{1,0:T(8,128)(2,1)}, bf16[48,256]{1,0:T(8,128)(2,1)S(1)}, u32[]{:S(2)}, u32[]{:S(2)}) collective-permute-start(bf16[48,256]{1,0:T(8,128)(2,1)} %get-tuple-element.20.heads), channel_id=1, source_target_pairs={{0,3},{1,0},{2,1},{3,2},{4,7},{5,4},{6,5},{7,6},{8,11},{9,8},{10,9... | collective-permute-start | bytes 73736 | tf_op jit(solution)/shard_map/ppermute | solution.py:408
  15.5 0.0 collective-permute-start.2
  15.5 0.6 reshape.49.branch
  16.1 2.2 %route.1 = (bf16[768,128]{1,0:T(8,128)(2,1)}, s32[48,128]{1,0:T(8,128)}) custom-call(s32[1]{0:T(128)} %bitcast.place, s32[2,48]{1,0:T(2,128)} %bitcast.36), custom_call_target="tpu_custom_call" | custom-call | tf_op jit(solution)/shard_map/route/pallas_call | solution.py:422
  18.3 0.0 collective-permute-done.heads_l
  18.3 0.0 collective-permute-done.1.heads_r
  18.3 2.7 %collective-permute-done.2.heads_f = bf16[48,256]{1,0:T(8,128)(2,1)S(1)} collective-permute-done((bf16[48,256]{1,0:T(8,128)(2,1)}, bf16[48,256]{1,0:T(8,128)(2,1)S(1)}, u32[]{:S(2)}, u32[]{:S(2)}) %collective-permute-start.2) | collective-permute-done | bytes 24608 | tf_op jit(solution)/shard_map/ppermute | solution.py:409
  21.0 0.7 copy-done.2
  21.7 5.4 %mix.1 = (bf16[768,1024]{1,0:T(8,128)(2,1)}, bf16[48,512]{1,0:T(8,128)(2,1)S(1)}, f32[48,128]{1,0:T(8,128)S(1)}) custom-call(s32[1]{0:T(128)} %bitcast.place, bf16[48,256]{1,0:T(8,128)(2,1)S(1)} %copy-done.2, bf16[48,256]{1,0:T(8,128)(2,1)S(1)} %collective-permute-done.heads_l, bf16[48,256]{1,0:T(8,128)(2,1)S(1)} %collective-permute-done.1.heads_r, ...), custom_call_target="tpu_custom_call" | custom-call | flops 201326592 | bytes 4194304 | tf_op jit(solution)/shard_map/mix/pallas_call | solution.py:434
  27.1 0.6 copy-done
  27.8 0.6 copy-done.1
  28.4 8.5 %all-to-all-start = ((bf16[32,24,1024]{2,1,0:T(8,128)(2,1)}), bf16[32,24,1024]{2,1,0:T(8,128)(2,1)S(1)}, u32[]{:S(2)}, u32[]{:S(2)}) async-start(bf16[32,24,1024]{2,1,0:T(8,128)(2,1)} %bitcast.23), calls=%async_computation | async-start | bytes 3145728 | tf_op jit(solution)/shard_map/all_to_all | solution.py:461
  36.9 0.1 collective-permute-start.3
  36.9 0.8 collective-permute-start.10
  37.7 2.6 %collective-permute-start.4 = (bf16[64,2048]{1,0:T(8,128)(2,1)S(1)}, bf16[64,2048]{1,0:T(8,128)(2,1)S(1)}, u32[]{:S(2)}, u32[]{:S(2)}) collective-permute-start(bf16[64,2048]{1,0:T(8,128)(2,1)S(1)} %bitcast.26), channel_id=1, source_target_pairs={{0,3},{1,0},{2,1},{3,2},{4,7},{5,4},{6,5},{7,6},{8,11},{9,8},{10,9... | collective-permute-start | bytes 786440 | tf_op jit(solution)/shard_map/ppermute | solution.py:365
  40.3 0.0 collective-permute-done.11.rest_10_
  40.3 1.9 %collective-permute-start.12 = (bf16[128,2048]{1,0:T(8,128)(2,1)S(1)}, bf16[128,2048]{1,0:T(8,128)(2,1)}, u32[]{:S(2)}, u32[]{:S(2)}) collective-permute-start(bf16[128,2048]{1,0:T(8,128)(2,1)S(1)} %collective-permute-done.11.rest_10_), channel_id=1, source_target_pairs={{0,3},{1,0},{2,1},{3,2},{4,7},{5,4},{6,5},{7,6},{8,11},{9,8},{10,9... | collective-permute-start | bytes 1572872 | tf_op jit(solution)/shard_map/ppermute | solution.py:413
  42.2 0.0 collective-permute-start.6
  42.2 5.1 %collective-permute-done.3.rest_1_ = bf16[64,2048]{1,0:T(8,128)(2,1)S(1)} collective-permute-done((bf16[64,2048]{1,0:T(8,128)(2,1)S(1)}, bf16[64,2048]{1,0:T(8,128)(2,1)S(1)}, u32[]{:S(2)}, u32[]{:S(2)}) %collective-permute-start.3) | collective-permute-done | bytes 262176 | tf_op jit(solution)/shard_map/ppermute | solution.py:364
  47.3 0.0 collective-permute-start.5
  47.3 0.0 collective-permute-done.4.rest_2_
  47.3 0.1 collective-permute-start.7
  47.4 0.0 collective-permute-done.6.rest_4_
  47.5 0.5 collective-permute-start.13
  48.0 15.6 %collective-permute-done.5.rest_3_ = bf16[64,2048]{1,0:T(8,128)(2,1)} collective-permute-done((bf16[64,2048]{1,0:T(8,128)(2,1)S(1)}, bf16[64,2048]{1,0:T(8,128)(2,1)}, u32[]{:S(2)}, u32[]{:S(2)}) %collective-permute-start.5) | collective-permute-done | bytes 262176 | tf_op jit(solution)/shard_map/ppermute | solution.py:412
  63.6 0.0 collective-permute-start.8
  63.6 0.0 collective-permute-done.10.rest_9_
  63.6 0.5 collective-permute-start.14
  64.1 0.0 collective-permute-done.7.rest_5_
  64.1 0.1 collective-permute-start.15
  64.2 0.0 collective-permute-done.12.rest_11_
  64.2 0.4 collective-permute-start.16
  64.6 0.5 collective-permute-done.8.rest_6_
  65.1 0.1 collective-permute-start.9
  65.3 3.5 %plan.1 = (bf16[288,3072]{1,0:T(8,128)(2,1)}, bf16[768,768]{1,0:T(8,128)(2,1)}, bf16[768,768]{1,0:T(8,128)(2,1)}) custom-call(s32[48,128]{1,0:T(8,128)} %get-tuple-element.18.slots), custom_call_target="tpu_custom_call" | custom-call | tf_op jit(solution)/shard_map/plan/pallas_call | solution.py:466
  68.8 0.0 collective-permute-done.14.rest_13_
  68.8 0.8 copy-done.6
  69.6 8.6 %ffn.1 = bf16[32,4,24,256]{3,2,1,0:T(8,128)(2,1)} custom-call(bf16[768,1024]{1,0:T(8,128)(2,1)S(1)} %bitcast.18, bf16[768,768]{1,0:T(8,128)(2,1)} %get-tuple-element.23.gather, bf16[768,768]{1,0:T(8,128)(2,1)} %get-tuple-element.24.spread, bf16[1,2048,256]{2,1,0:T(8,128)(2,1)} %e_gate.1, bf16[1,2048,256]{2,1,0:T(8,128)(2,1)} %e_up.1, ...), custom_call_target="tpu_custom_call" | custom-call | flops 1811939328 | bytes 9437184 | tf_op jit(solution)/shard_map/ffn/pallas_call | solution.py:480
  78.2 0.0 copy-start.14
  78.2 7.5 %all-to-all-start.1 = ((bf16[128,24,256]{2,1,0:T(8,128)(2,1)}), bf16[128,24,256]{2,1,0:T(8,128)(2,1)S(1)}, u32[]{:S(2)}, u32[]{:S(2)}) async-start(bf16[128,24,256]{2,1,0:T(8,128)(2,1)} %bitcast.22), calls=%async_computation.1 | async-start | bytes 3145728 | tf_op jit(solution)/shard_map/all_to_all | solution.py:510
  85.7 0.7 copy.28.route_w
  86.4 8.3 %update.1 = f32[96,128,128]{2,1,0:T(8,128)} custom-call(f32[96,128]{1,0:T(8,128)} %get-tuple-element.27.carry, f32[96,128]{1,0:T(8,128)} %get-tuple-element.28.written, f32[96,128]{1,0:T(8,128)} %get-tuple-element.29.value, f32[96,128,128]{2,1,0:T(8,128)} %bitcast.20), custom_call_target="tpu_custom_call" | custom-call | flops 4718592 | bytes 12582912 | tf_op jit(solution)/shard_map/update/pallas_call | solution.py:516
  94.7 15.5 %all-to-all-done.1 = bf16[128,24,256]{2,1,0:T(8,128)(2,1)S(1)} async-done(((bf16[128,24,256]{2,1,0:T(8,128)(2,1)}), bf16[128,24,256]{2,1,0:T(8,128)(2,1)S(1)}, u32[]{:S(2)}, u32[]{:S(2)}) %all-to-all-start.1) | async-done | bytes 1572896 | tf_op jit(solution)/shard_map/all_to_all | solution.py:510
  110.1 2.8 %final.1 = bf16[48,512]{1,0:T(8,128)(2,1)} custom-call(bf16[288,3072]{1,0:T(8,128)(2,1)} %get-tuple-element.19.picks, bf16[3072,256]{1,0:T(8,128)(2,1)S(1)} %bitcast.19, bf16[48,512]{1,0:T(8,128)(2,1)} %copy-done, f32[48,128]{1,0:T(8,128)} %copy-done.1, f32[48,2]{1,0:T(8,128)} %copy.28.route_w), custom_call_target="tpu_custom_call" | custom-call | tf_op jit(solution)/shard_map/final/pallas_call | solution.py:528
  (30 shorter events, 0.1 us)
Async XLA Ops:
  1.7 45.7 %copy-start.3 = (bf16[128,2048]{1,0:T(8,128)(2,1)}, bf16[128,2048]{1,0:T(8,128)(2,1)S(1)}, u32[]{:S(2)}) copy-start(bf16[128,2048]{1,0:T(8,128)(2,1)S(1)} %pad_maximum_fusion.rest_8_) | copy-start | bytes 1572868
  1.7 38.5 %collective-permute-start.11 = (bf16[128,2048]{1,0:T(8,128)(2,1)S(1)}, bf16[128,2048]{1,0:T(8,128)(2,1)S(1)}, u32[]{:S(2)}, u32[]{:S(2)}) collective-permute-start(bf16[128,2048]{1,0:T(8,128)(2,1)S(1)} %pad_maximum_fusion.rest_8_), channel_id=1, source_target_pairs={{0,3},{1,0},{2,1},{3,2},{4,7},{5,4},{6,5},{7,6},{8,11},{9,8},{10,9... | collective-permute-start | bytes 1572872 | tf_op jit(solution)/shard_map/ppermute | solution.py:411
  4.7 10.8 %copy-start.13 = (bf16[2048]{0:T(1024)(128)(2,1)S(1)}, bf16[2048]{0:T(1024)(128)(2,1)}, u32[]{:S(2)}) copy-start(bf16[2048]{0:T(1024)(128)(2,1)} %param.44) | copy-start | bytes 12292
  12.2 6.1 %collective-permute-start = (bf16[48,256]{1,0:T(8,128)(2,1)}, bf16[48,256]{1,0:T(8,128)(2,1)S(1)}, u32[]{:S(2)}, u32[]{:S(2)}) collective-permute-start(bf16[48,256]{1,0:T(8,128)(2,1)} %get-tuple-element.20.heads), channel_id=1, source_target_pairs={{0,1},{1,2},{2,3},{3,0},{4,5},{5,6},{6,7},{7,4},{8,9},{9,10},{10,1... | collective-permute-start | bytes 73736 | tf_op jit(solution)/shard_map/ppermute | solution.py:407
  12.2 6.0 %collective-permute-start.1 = (bf16[48,256]{1,0:T(8,128)(2,1)}, bf16[48,256]{1,0:T(8,128)(2,1)S(1)}, u32[]{:S(2)}, u32[]{:S(2)}) collective-permute-start(bf16[48,256]{1,0:T(8,128)(2,1)} %get-tuple-element.20.heads), channel_id=1, source_target_pairs={{0,3},{1,0},{2,1},{3,2},{4,7},{5,4},{6,5},{7,6},{8,11},{9,8},{10,9... | collective-permute-start | bytes 73736 | tf_op jit(solution)/shard_map/ppermute | solution.py:408
  15.5 5.5 %collective-permute-start.2 = (bf16[48,256]{1,0:T(8,128)(2,1)}, bf16[48,256]{1,0:T(8,128)(2,1)S(1)}, u32[]{:S(2)}, u32[]{:S(2)}) collective-permute-start(bf16[48,256]{1,0:T(8,128)(2,1)} %get-tuple-element.20.heads), channel_id=1, source_target_pairs={{0,2},{1,3},{2,0},{3,1},{4,6},{5,7},{6,4},{7,5},{8,10},{9,11},{10,... | collective-permute-start | bytes 73736 | tf_op jit(solution)/shard_map/ppermute | solution.py:409
  21.0 0.7 copy-start.2
  27.1 0.6 copy-start
  27.7 0.6 copy-start.1
  28.4 8.5 %copy-start.7 = (bf16[2048,64]{0,1:T(8,128)(2,1)S(1)}, bf16[2048,64]{0,1:T(8,128)(2,1)}, u32[]{:S(2)}) copy-start(bf16[2048,64]{0,1:T(8,128)(2,1)} %param.45) | copy-start | bytes 786436
  28.4 41.2 %all-to-all-start = ((bf16[32,24,1024]{2,1,0:T(8,128)(2,1)}), bf16[32,24,1024]{2,1,0:T(8,128)(2,1)S(1)}, u32[]{:S(2)}, u32[]{:S(2)}) async-start(bf16[32,24,1024]{2,1,0:T(8,128)(2,1)} %bitcast.23), calls=%async_computation | async-start | bytes 3145728 | tf_op jit(solution)/shard_map/all_to_all | solution.py:461
  36.9 10.5 %collective-permute-start.3 = (bf16[64,2048]{1,0:T(8,128)(2,1)S(1)}, bf16[64,2048]{1,0:T(8,128)(2,1)S(1)}, u32[]{:S(2)}, u32[]{:S(2)}) collective-permute-start(bf16[64,2048]{1,0:T(8,128)(2,1)S(1)} %bitcast.25), channel_id=1, source_target_pairs={{0,1},{1,2},{2,3},{3,0},{4,5},{5,6},{6,7},{7,4},{8,9},{9,10},{10,1... | collective-permute-start | bytes 786440 | tf_op jit(solution)/shard_map/ppermute | solution.py:364
  36.9 26.6 %collective-permute-start.10 = (bf16[128,2048]{1,0:T(8,128)(2,1)S(1)}, bf16[128,2048]{1,0:T(8,128)(2,1)S(1)}, u32[]{:S(2)}, u32[]{:S(2)}) collective-permute-start(bf16[128,2048]{1,0:T(8,128)(2,1)S(1)} %pad_maximum_fusion.rest_8_), channel_id=1, source_target_pairs={{0,1},{1,2},{2,3},{3,0},{4,5},{5,6},{6,7},{7,4},{8,9},{9,10},{10,1... | collective-permute-start | bytes 1572872 | tf_op jit(solution)/shard_map/ppermute | solution.py:410
  37.7 9.6 %collective-permute-start.4 = (bf16[64,2048]{1,0:T(8,128)(2,1)S(1)}, bf16[64,2048]{1,0:T(8,128)(2,1)S(1)}, u32[]{:S(2)}, u32[]{:S(2)}) collective-permute-start(bf16[64,2048]{1,0:T(8,128)(2,1)S(1)} %bitcast.26), channel_id=1, source_target_pairs={{0,3},{1,0},{2,1},{3,2},{4,7},{5,4},{6,5},{7,6},{8,11},{9,8},{10,9... | collective-permute-start | bytes 786440 | tf_op jit(solution)/shard_map/ppermute | solution.py:365
  40.3 29.3 %copy-start.4 = (bf16[128,2048]{1,0:T(8,128)(2,1)}, bf16[128,2048]{1,0:T(8,128)(2,1)S(1)}, u32[]{:S(2)}) copy-start(bf16[128,2048]{1,0:T(8,128)(2,1)S(1)} %collective-permute-done.11.rest_10_) | copy-start | bytes 1572868
  40.3 24.0 %collective-permute-start.12 = (bf16[128,2048]{1,0:T(8,128)(2,1)S(1)}, bf16[128,2048]{1,0:T(8,128)(2,1)}, u32[]{:S(2)}, u32[]{:S(2)}) collective-permute-start(bf16[128,2048]{1,0:T(8,128)(2,1)S(1)} %collective-permute-done.11.rest_10_), channel_id=1, source_target_pairs={{0,3},{1,0},{2,1},{3,2},{4,7},{5,4},{6,5},{7,6},{8,11},{9,8},{10,9... | collective-permute-start | bytes 1572872 | tf_op jit(solution)/shard_map/ppermute | solution.py:413
  42.2 5.2 %collective-permute-start.6 = (bf16[64,2048]{1,0:T(8,128)(2,1)S(1)}, bf16[64,2048]{1,0:T(8,128)(2,1)S(1)}, u32[]{:S(2)}, u32[]{:S(2)}) collective-permute-start(bf16[64,2048]{1,0:T(8,128)(2,1)S(1)} %bitcast.27), channel_id=1, source_target_pairs={{0,4},{4,0},{1,5},{5,1},{2,6},{6,2},{3,7},{7,3},{8,12},{12,8},{9,1... | collective-permute-start | bytes 786440 | tf_op jit(solution)/shard_map/ppermute | solution.py:415
  47.3 16.9 %copy-start.8 = (bf16[64,2048]{1,0:T(8,128)(2,1)}, bf16[64,2048]{1,0:T(8,128)(2,1)S(1)}, u32[]{:S(2)}) copy-start(bf16[64,2048]{1,0:T(8,128)(2,1)S(1)} %collective-permute-done.3.rest_1_) | copy-start | bytes 786436
  47.3 16.3 %collective-permute-start.5 = (bf16[64,2048]{1,0:T(8,128)(2,1)S(1)}, bf16[64,2048]{1,0:T(8,128)(2,1)}, u32[]{:S(2)}, u32[]{:S(2)}) collective-permute-start(bf16[64,2048]{1,0:T(8,128)(2,1)S(1)} %collective-permute-done.3.rest_1_), channel_id=1, source_target_pairs={{0,1},{1,2},{2,3},{3,0},{4,5},{5,6},{6,7},{7,4},{8,9},{9,10},{10,1... | collective-permute-start | bytes 786440 | tf_op jit(solution)/shard_map/ppermute | solution.py:412
  47.3 17.3 %copy-start.9 = (bf16[64,2048]{1,0:T(8,128)(2,1)}, bf16[64,2048]{1,0:T(8,128)(2,1)S(1)}, u32[]{:S(2)}) copy-start(bf16[64,2048]{1,0:T(8,128)(2,1)S(1)} %collective-permute-done.4.rest_2_) | copy-start | bytes 786436
  47.3 16.8 %collective-permute-start.7 = (bf16[64,2048]{1,0:T(8,128)(2,1)S(1)}, bf16[64,2048]{1,0:T(8,128)(2,1)S(1)}, u32[]{:S(2)}, u32[]{:S(2)}) collective-permute-start(bf16[64,2048]{1,0:T(8,128)(2,1)S(1)} %collective-permute-done.3.rest_1_), channel_id=1, source_target_pairs={{0,4},{4,0},{1,5},{5,1},{2,6},{6,2},{3,7},{7,3},{8,12},{12,8},{9,1... | collective-permute-start | bytes 786440 | tf_op jit(solution)/shard_map/ppermute | solution.py:415
  47.5 17.7 %copy-start.10 = (bf16[64,2048]{1,0:T(8,128)(2,1)}, bf16[64,2048]{1,0:T(8,128)(2,1)S(1)}, u32[]{:S(2)}) copy-start(bf16[64,2048]{1,0:T(8,128)(2,1)S(1)} %collective-permute-done.6.rest_4_) | copy-start | bytes 786436
  47.5 21.3 %collective-permute-start.13 = (bf16[128,2048]{1,0:T(8,128)(2,1)S(1)}, bf16[128,2048]{1,0:T(8,128)(2,1)S(1)}, u32[]{:S(2)}, u32[]{:S(2)}) collective-permute-start(bf16[128,2048]{1,0:T(8,128)(2,1)S(1)} %pad_maximum_fusion.rest_8_), channel_id=1, source_target_pairs={{0,4},{4,0},{1,5},{5,1},{2,6},{6,2},{3,7},{7,3},{8,12},{12,8},{9,1... | collective-permute-start | bytes 1572872 | tf_op jit(solution)/shard_map/ppermute | solution.py:416
  63.6 1.5 %collective-permute-start.8 = (bf16[64,2048]{1,0:T(8,128)(2,1)S(1)}, bf16[64,2048]{1,0:T(8,128)(2,1)S(1)}, u32[]{:S(2)}, u32[]{:S(2)}) collective-permute-start(bf16[64,2048]{1,0:T(8,128)(2,1)S(1)} %collective-permute-done.4.rest_2_), channel_id=1, source_target_pairs={{0,4},{4,0},{1,5},{5,1},{2,6},{6,2},{3,7},{7,3},{8,12},{12,8},{9,1... | collective-permute-start | bytes 786440 | tf_op jit(solution)/shard_map/ppermute | solution.py:415
  63.6 6.0 %copy-start.5 = (bf16[128,2048]{1,0:T(8,128)(2,1)}, bf16[128,2048]{1,0:T(8,128)(2,1)S(1)}, u32[]{:S(2)}) copy-start(bf16[128,2048]{1,0:T(8,128)(2,1)S(1)} %collective-permute-done.10.rest_9_) | copy-start | bytes 1572868
  63.6 5.2 %collective-permute-start.14 = (bf16[128,2048]{1,0:T(8,128)(2,1)S(1)}, bf16[128,2048]{1,0:T(8,128)(2,1)}, u32[]{:S(2)}, u32[]{:S(2)}) collective-permute-start(bf16[128,2048]{1,0:T(8,128)(2,1)S(1)} %collective-permute-done.10.rest_9_), channel_id=1, source_target_pairs={{0,4},{4,0},{1,5},{5,1},{2,6},{6,2},{3,7},{7,3},{8,12},{12,8},{9,1... | collective-permute-start | bytes 1572872 | tf_op jit(solution)/shard_map/ppermute | solution.py:416
  64.1 1.2 %copy-start.11 = (bf16[64,2048]{1,0:T(8,128)(2,1)}, bf16[64,2048]{1,0:T(8,128)(2,1)S(1)}, u32[]{:S(2)}) copy-start(bf16[64,2048]{1,0:T(8,128)(2,1)S(1)} %collective-permute-done.7.rest_5_) | copy-start | bytes 786436
  64.1 5.4 %collective-permute-start.15 = (bf16[128,2048]{1,0:T(8,128)(2,1)S(1)}, bf16[128,2048]{1,0:T(8,128)(2,1)}, u32[]{:S(2)}, u32[]{:S(2)}) collective-permute-start(bf16[128,2048]{1,0:T(8,128)(2,1)S(1)} %collective-permute-done.11.rest_10_), channel_id=1, source_target_pairs={{0,4},{4,0},{1,5},{5,1},{2,6},{6,2},{3,7},{7,3},{8,12},{12,8},{9,1... | collective-permute-start | bytes 1572872 | tf_op jit(solution)/shard_map/ppermute | solution.py:416
  64.2 5.3 %collective-permute-start.16 = (bf16[128,2048]{1,0:T(8,128)(2,1)}, bf16[128,2048]{1,0:T(8,128)(2,1)}, u32[]{:S(2)}, u32[]{:S(2)}) collective-permute-start(bf16[128,2048]{1,0:T(8,128)(2,1)} %collective-permute-done.12.rest_11_), channel_id=1, source_target_pairs={{0,4},{4,0},{1,5},{5,1},{2,6},{6,2},{3,7},{7,3},{8,12},{12,8},{9,1... | collective-permute-start | bytes 1572872 | tf_op jit(solution)/shard_map/ppermute | solution.py:418
  65.1 4.4 %copy-start.12 = (bf16[64,2048]{1,0:T(8,128)(2,1)}, bf16[64,2048]{1,0:T(8,128)(2,1)S(1)}, u32[]{:S(2)}) copy-start(bf16[64,2048]{1,0:T(8,128)(2,1)S(1)} %collective-permute-done.8.rest_6_) | copy-start | bytes 786436
  65.1 3.6 %collective-permute-start.9 = (bf16[64,2048]{1,0:T(8,128)(2,1)}, bf16[64,2048]{1,0:T(8,128)(2,1)}, u32[]{:S(2)}, u32[]{:S(2)}) collective-permute-start(bf16[64,2048]{1,0:T(8,128)(2,1)} %collective-permute-done.5.rest_3_), channel_id=1, source_target_pairs={{0,4},{4,0},{1,5},{5,1},{2,6},{6,2},{3,7},{7,3},{8,12},{12,8},{9,1... | collective-permute-start | bytes 786440 | tf_op jit(solution)/shard_map/ppermute | solution.py:417
  68.8 0.8 copy-start.6
  78.2 7.5 %copy-start.14 = (f32[48,2]{0,1:T(2,128)S(1)}, f32[48,2]{0,1:T(2,128)}, u32[]{:S(2)}) copy-start(f32[48,2]{0,1:T(2,128)} %param.40) | copy-start | bytes 1156
  78.2 31.9 %all-to-all-start.1 = ((bf16[128,24,256]{2,1,0:T(8,128)(2,1)}), bf16[128,24,256]{2,1,0:T(8,128)(2,1)S(1)}, u32[]{:S(2)}, u32[]{:S(2)}) async-start(bf16[128,24,256]{2,1,0:T(8,128)(2,1)} %bitcast.22), calls=%async_computation.1 | async-start | bytes 3145728 | tf_op jit(solution)/shard_map/all_to_all | solution.py:510

commit v2 on v1

v2 whole, which is shorter than its diff:
```python
import jax
import jax.numpy as jnp
from jax import lax
from jax.experimental import pallas as pl
from jax.experimental.pallas import tpu as pltpu
from jax.sharding import Mesh
from jax.sharding import PartitionSpec as P


EPS = 1e-06
BF = jnp.bfloat16
F32 = jnp.float32
EP = ("q", "c")
ALL = ("q", "c", "x")
CORES = 2
VMEM = pl.BlockSpec(memory_space=pltpu.VMEM)
SMEM = pl.BlockSpec(memory_space=pltpu.SMEM)
ANY = pl.BlockSpec(memory_space=pl.ANY)


def params(mib=60):
    return pltpu.CompilerParams(vmem_limit_bytes=mib * 1024 * 1024)


def far_memory(array):
    return pltpu.with_memory_space_constraint(array, pltpu.HBM)


def near_memory(array):
    return pltpu.with_memory_space_constraint(array, pltpu.VMEM)


def nt_dot(left, right):
    return lax.dot_general(left, right, (((1,), (1,)), ((), ())), preferred_element_type=F32)


def normed_rows(rows_in, gain_vec):
    as_float = rows_in.astype(F32)
    mean = jnp.mean(as_float * as_float, axis=-1, keepdims=True)
    return (as_float * lax.rsqrt(mean + EPS) * gain_vec).astype(BF)


def log_sigmoid(x):
    return -(jnp.maximum(-x, 0.0) + jnp.log1p(jnp.exp(-jnp.abs(x))))


def gate_factors(in_pre, forget_pre, max_state):
    log_forget = log_sigmoid(forget_pre)
    new_max = jnp.maximum(log_forget + max_state, in_pre)
    return jnp.exp(log_forget + max_state - new_max), jnp.exp(in_pre - new_max), new_max


def padded_transpose(block):
    rows, cols = block.shape
    if rows < 128:
        block = jnp.concatenate([block, jnp.zeros((128 - rows, cols), block.dtype)], axis=0)
    return block.T


def start_all(pairs, sems):
    copies = [pltpu.make_async_copy(src, dst, sems.at[i]) for i, (src, dst) in enumerate(pairs)]
    for copy in copies:
        copy.start()
    return copies


def over(index, divisor):
    factor, shift = {6: (10923, 16), 24: (43691, 20)}[divisor]
    return (index * factor) >> shift


def route_tables(place, ids, select_o, slots_o):
    seqs = ids.shape[1]
    lanes = select_o.shape[1]
    row = lax.broadcasted_iota(jnp.int32, (seqs, seqs), 0)
    col = lax.broadcasted_iota(jnp.int32, (seqs, seqs), 1)
    first, second = ids[0:1], ids[1:2]
    here = lax.broadcasted_iota(jnp.int32, (seqs, lanes), 0)
    there = lax.broadcasted_iota(jnp.int32, (seqs, lanes), 1)
    slot_rows = []
    slots = jnp.zeros((seqs, lanes), jnp.int32)
    for k, own in enumerate((first, second)):
        column = jnp.sum(jnp.where(row == col, own, 0), axis=1, keepdims=True)
        same = ((column == first) | (column == second)) & (col < row)
        slot = column * 6 + jnp.sum(jnp.where(same, 1, 0), axis=1, keepdims=True)
        slots = jnp.where(there == k, slot, slots)
        slot_rows.append(
            jnp.sum(jnp.where((there & 63) == here, slot + 1, 0), axis=0, keepdims=True) - 1
        )
    slots_o[...] = slots
    line = lax.broadcasted_iota(jnp.int32, (24, lanes), 0)
    lane = lax.broadcasted_iota(jnp.int32, (24, lanes), 1)
    part = over(line, 6)
    entry = line - 6 * part
    right_side = part >> 1 == lane >> 6
    is_moe = part & 1 == 1
    wanted = jnp.where(right_side & is_moe, entry, -999)
    shared = [
        right_side & (part & 1 == 0) & ((place * CORES + c) * 6 + entry == lane & 63)
        for c in range(CORES)
    ]
    for e in range(0, select_o.shape[0] // 24, 2):
        hits = []
        for c in range(2):
            first, second = (rows - 6 * (e + c) for rows in slot_rows)
            hit = shared[c] | (wanted == first) | (wanted == second)
            hits.append(jnp.where(hit, 1.0, 0.0))
        select_o[e * 24 : (e + 2) * 24] = jnp.concatenate(hits, axis=0).astype(BF)


def front_kernel(
    place, ids_h, tok_h, gain_h, w_in_h, w_fg_h, in_bias_h, fg_bias_h, norm_h, mx_h,
    wq, wk, wv, wo, cell, w_mix_h, moe_gain_h,
    heads_o, carry_h, written_h, value_h, norm_out_h, max_h, slots_h, select_o, w_mix, tok, moe_gain,
    ids, slots, gain, w_in, w_fg, in_bias, fg_bias, norm, mx, wbuf, cbuf, num,
    carry_o, written_o, value_o, norm_o, max_o, hot, isem, wsem, csem, osem,
):
    rows, head_count, hd = cbuf.shape[:3]
    chunks = csem.shape[0]
    per = rows // chunks
    small = start_all(
        [
            (tok_h, tok), (gain_h, gain), (w_in_h, w_in), (w_fg_h, w_fg),
            (in_bias_h, in_bias), (fg_bias_h, fg_bias), (norm_h, norm), (mx_h, mx),
            (ids_h, ids), (moe_gain_h, moe_gain),
        ],
        isem,
    )
    loads = [
        pltpu.make_async_copy(w, wbuf.at[i], wsem.at[i]) for i, w in enumerate((wq, wk, wv, wo))
    ]
    parts = [
        pltpu.make_async_copy(cell.at[pl.ds(j * per, per)], cbuf.at[pl.ds(j * per, per)], csem.at[j])
        for j in range(chunks)
    ]
    later = pltpu.make_async_copy(w_mix_h, w_mix, wsem.at[4])
    for copy in (loads[0], *parts, *loads[1:], later):
        copy.start()
    small[8].wait()
    route_tables(place[0], ids, select_o, slots)
    line = lax.broadcasted_iota(jnp.int32, hot.shape, 0) & 63
    hot[...] = jnp.where(line == lax.broadcasted_iota(jnp.int32, hot.shape, 1) >> 7, 1.0, 0.0).astype(BF)
    small[0].wait()
    small[1].wait()
    normed = normed_rows(tok[...], gain[...])
    for copy in small[2:8] + small[9:]:
        copy.wait()
    loads[0].wait()
    queries = jnp.dot(normed, wbuf[0], preferred_element_type=F32)
    high = queries.astype(BF).astype(F32)
    gap = jnp.zeros((64 - rows, head_count * hd), F32)
    stacked = jnp.concatenate([high, gap, queries - high, gap], axis=0)
    turned = jnp.concatenate(
        [stacked[:, h * hd : (h + 1) * hd].T for h in range(head_count)], axis=0
    ).astype(BF)

    def read_out(j):
        parts[j].wait()
        for b in range(j * per, (j + 1) * per, 2):
            spread = jnp.dot(turned, hot[:, b * hd : (b + 2) * hd], preferred_element_type=F32)
            for k in range(2):
                for h in range(head_count):
                    num[h, b + k : b + k + 1] = jnp.sum(
                        spread[h * hd : (h + 1) * hd, k * hd : (k + 1) * hd] * cbuf[b + k, h],
                        axis=0,
                        keepdims=True,
                    )

    read_out(0)
    in_row = nt_dot(w_in[...], normed)
    fg_row = nt_dot(w_fg[...], normed)
    factors = []
    for h in range(head_count):
        found = gate_factors(
            in_row[h : h + 1] + in_bias[h], fg_row[h : h + 1] + fg_bias[h], mx[h : h + 1]
        )
        max_o[h : h + 1] = found[2]
        factors += found
    factors.append(jnp.zeros((8 - len(factors), rows), F32))
    same = lax.broadcasted_iota(jnp.int32, (rows, rows), 0) == lax.broadcasted_iota(
        jnp.int32, (rows, rows), 1
    )
    columns = lax.dot_general(
        same.astype(F32),
        jnp.concatenate(factors, axis=0),
        (((1,), (1,)), ((), ())),
        preferred_element_type=F32,
        precision=lax.Precision.HIGHEST,
    )

    for j in range(1, chunks):
        read_out(j)

    def project(i):
        loads[i].wait()
        return jnp.dot(normed, wbuf[i], preferred_element_type=F32)

    keys = project(1) * hd ** (-0.5)
    values = project(2)
    kept = []
    for h in range(head_count):
        cols = slice(h * hd, (h + 1) * hd)
        carry, write, new_max = (columns[:, 3 * h + k : 3 * h + k + 1] for k in range(3))
        query, value = queries[:, cols], values[:, cols]
        written = write * keys[:, cols]
        at = pl.ds(h, rows, stride=head_count)
        new_norm = carry * norm[at, :] + written
        norm_o[at, :] = new_norm
        written_o[at, :] = written
        value_o[at, :] = value
        carry_o[at, :] = jnp.broadcast_to(carry, (rows, hd))
        denominator = jnp.sum(query * new_norm, axis=-1, keepdims=True)
        floor = jnp.maximum(jnp.abs(denominator), jnp.exp(-new_max))
        added = jnp.sum(query * written, axis=-1, keepdims=True) * value
        kept.append((carry, added, floor))
    stores = start_all(
        [
            (carry_o, carry_h), (written_o, written_h), (value_o, value_h),
            (norm_o, norm_out_h), (max_o, max_h), (slots, slots_h),
        ],
        osem,
    )
    opened = jax.nn.sigmoid(project(3))
    for h in range(head_count):
        cols = slice(h * hd, (h + 1) * hd)
        carry, added, floor = kept[h]
        heads_o[:, cols] = (opened[:, cols] * ((carry * num[h] + added) / floor)).astype(BF)
    for copy in stores:
        copy.wait()
    later.wait()


def update_kernel(carry, written, value, cell, out):
    turned = padded_transpose(written[...])
    for p in range(cell.shape[0]):
        out[p] = carry[p : p + 1] * cell[p] + turned[:, p : p + 1] * value[p : p + 1]


def plan_kernel(slots, moe_in, branch, picks_o, weight_o):
    logit = jnp.sum(moe_in[...].astype(F32) * branch[...].astype(F32), axis=-1, keepdims=True)
    weight_o[...] = jnp.broadcast_to(jax.nn.sigmoid(logit), weight_o.shape)
    seqs = slots.shape[0]
    lanes = picks_o.shape[1]
    lane = lax.broadcasted_iota(jnp.int32, (1, lanes), 1)
    source = over(lane, 24)
    inner = lane - 24 * source
    part = over(inner, 6)
    entry = inner - 6 * part
    side, is_moe = part >> 1, part & 1
    from_x, from_c, from_e = source & 3, (source >> 2) & 1, source >> 2
    dense_row = jnp.where(is_moe == 0, (from_x * CORES + from_c) * 6 + entry, -1)
    slot = jnp.where(is_moe == 1, from_e * 6 + entry, -1)
    row = lax.broadcasted_iota(jnp.int32, (seqs, 1), 0)
    for k in range(3):
        if k == 0:
            hit = jnp.where(dense_row == row, 1.0, 0.0)
        else:
            hit = jnp.where(slot == slots[:, k - 1 : k], 1.0, 0.0)
        for h in range(2):
            at = (2 * k + h) * seqs
            picks_o[at : at + seqs] = jnp.where(side == h, hit, 0.0).astype(BF)


def mix_kernel(
    place, heads, heads_l, heads_r, heads_f, w_mix, tok, gain, select,
    send_h, own_o, moe_o,
    send, sems,
):
    width = heads.shape[1]
    mixed_proj = None
    for turn, block in ((0, heads), (3, heads_l), (1, heads_r), (2, heads_f)):
        start = pl.multiple_of(((place[0] + turn) & 3) * width, width)
        part = jnp.dot(block[...], w_mix[pl.ds(start, width)], preferred_element_type=F32)
        mixed_proj = part if mixed_proj is None else mixed_proj + part
    residual = (tok[...].astype(F32) + mixed_proj).astype(BF)
    moe_in = normed_rows(residual, gain[...])
    half = send.shape[1]
    gap = jnp.zeros((select.shape[1] // 2 - moe_in.shape[0], half), BF)
    stacked = jnp.concatenate([moe_in[:, :half], gap, moe_in[:, half:], gap], axis=0)
    chunks = sems.shape[0]
    lines = send.shape[0] // chunks
    stores = []
    for j in range(chunks):
        at = pl.ds(j * lines, lines)
        send[at] = jnp.dot(select[at], stacked, preferred_element_type=F32).astype(BF)
        stores.append(pltpu.make_async_copy(send.at[at], send_h.at[at], sems.at[j]))
        stores[j].start()
    moe_o[...] = moe_in
    cols = own_o.shape[1]
    own = residual[:, :cols]
    for k in range(1, residual.shape[1] // cols):
        own = jnp.where(place[0] == k, residual[:, k * cols : (k + 1) * cols], own)
    own_o[...] = own
    for copy in stores:
        copy.wait()


def grouped_row(index, lines):
    source = over(index, 24)
    inner = index - 24 * source
    part = over(inner, 6)
    return part * lines + source * 6 + inner - 6 * part


def ffn_kernel(abuf, e_gate, e_up, e_down, *rest):
    packs, rest = rest[:10], rest[10:]
    out, egbuf, eubuf, edbuf, gbuf, ubuf, dbuf, xbuf, obuf, sems, osems = rest
    units = packs[0].shape[0] // 3
    mid = units // 2
    pairs = [(e_gate, egbuf), (e_up, eubuf), (e_down, edbuf)]
    for side in range(2):
        for b in range(3):
            pack, rows = packs[5 * side + b], pl.ds((4 * side + b) * units, units)
            pairs.append((pack.at[pl.ds(0, units)], gbuf.at[rows]))
            pairs.append((pack.at[pl.ds(units, units)], ubuf.at[rows]))
            pairs.append((pack.at[pl.ds(2 * units, units)], dbuf.at[rows]))
        head, tail, last = packs[5 * side + 3], packs[5 * side + 4], (4 * side + 3) * units
        pairs.append((head.at[pl.ds(0, units)], gbuf.at[pl.ds(last, units)]))
        pairs.append((head.at[pl.ds(units, mid)], ubuf.at[pl.ds(last, mid)]))
        pairs.append((tail.at[pl.ds(0, mid)], ubuf.at[pl.ds(last + mid, mid)]))
        pairs.append((tail.at[pl.ds(mid, units)], dbuf.at[pl.ds(last, units)]))
    loads = start_all(pairs, sems)
    size, half = abuf.shape
    block = 192
    groups = size // block
    lines = block // 4
    row = lax.broadcasted_iota(jnp.int32, (block, 1), 0)
    col = lax.broadcasted_iota(jnp.int32, (1, block), 1)
    gather = jnp.where(grouped_row(col, lines) == row, 1.0, 0.0).astype(BF)
    spread = jnp.where(grouped_row(row, lines) == col, 1.0, 0.0).astype(BF)
    for g in range(groups):
        sorted_rows = jnp.dot(
            gather, abuf[g * block : (g + 1) * block], preferred_element_type=F32
        ).astype(BF)
        for part in range(4):
            xbuf[
                part % 2,
                g * lines : (g + 1) * lines,
                (part // 2) * half : (part // 2 + 1) * half,
            ] = sorted_rows[part * lines : (part + 1) * lines]
    tok = xbuf[1]
    loads[0].wait()
    loads[1].wait()
    gate_proj = jnp.dot(tok, egbuf[0], preferred_element_type=F32)
    up_proj = jnp.dot(tok, eubuf[0], preferred_element_type=F32)
    hidden = (jax.nn.silu(gate_proj) * up_proj).astype(BF)
    loads[2].wait()
    expert_out = jnp.dot(hidden, edbuf[0], preferred_element_type=F32).astype(BF)
    tok = xbuf[0]
    total = None
    for side in range(2):
        for copy in loads[3 + 13 * side : 16 + 13 * side]:
            copy.wait()
        rows = slice(side * 4 * units, (side + 1) * 4 * units)
        hidden = (jax.nn.silu(nt_dot(tok, gbuf[rows])) * nt_dot(tok, ubuf[rows])).astype(BF)
        part = jnp.dot(hidden, dbuf[rows], preferred_element_type=F32)
        total = part if total is None else total + part
    total = total.astype(BF)
    peers, quarter = obuf.shape[0], obuf.shape[3]
    held = obuf.shape[1] // groups
    stores = []
    for s in range(peers):
        for g in range(groups):
            rows = slice(g * lines, (g + 1) * lines)
            sides = []
            for h in range(2):
                at = (2 * s + h) * quarter
                sides += [total[rows, at : at + quarter], expert_out[rows, at : at + quarter]]
            mixed = jnp.dot(spread, jnp.concatenate(sides, axis=0), preferred_element_type=F32)
            obuf[s, g * held : (g + 1) * held] = mixed.reshape(held, -1, quarter).astype(BF)
        stores.append(pltpu.make_async_copy(obuf.at[s], out.at[:, s], osems.at[s]))
        stores[s].start()
    for copy in stores:
        copy.wait()


def final_kernel(
    picks_h, returned, own_h, weight_h, route_h, out, picks, own, weight, route_w, sems
):
    loads = start_all(
        [(own_h, own), (weight_h, weight), (route_h, route_w), (picks_h, picks)], sems
    )
    for copy in loads:
        copy.wait()
    sums = jnp.dot(picks[...], returned[...], preferred_element_type=F32)
    seqs, quarter = own.shape[0], returned.shape[1]
    for h in range(2):
        dense, first, second = (
            sums[(2 * k + h) * seqs : (2 * k + h + 1) * seqs] for k in range(3)
        )
        cols = slice(h * quarter, (h + 1) * quarter)
        total = own[:, cols].astype(F32) + (route_w[:, :1] * first + route_w[:, 1:2] * second)
        out[:, cols] = (total + weight[:, :1] * dense).astype(BF)


def local(
    tokens,
    mix_gain,
    w_query,
    w_key,
    w_value,
    w_outgate,
    w_ingate,
    w_forget,
    in_bias,
    forget_bias,
    w_mix_out,
    cell_state,
    norm_state,
    max_state,
    moe_gain,
    route_ids,
    route_weights,
    expert_gate,
    expert_up,
    expert_down,
    branch_gate,
    dense_gate,
    dense_up,
    dense_down,
):
    seqs, width = tokens.shape
    tp_count = lax.axis_size("x")
    chips = lax.axis_size("q")
    ep_count = chips * CORES
    place = lax.axis_index("x")
    cols = width // tp_count
    half = width // 2
    head_count, hd = cell_state.shape[1:3]
    pair_rows = seqs * head_count
    groups = tp_count * CORES
    share = seqs // groups
    capacity = max(2, 4 * seqs // ep_count)
    swap = [(0, 1), (1, 0)]

    right = [(i, (i + 1) % tp_count) for i in range(tp_count)]
    left = [(i, (i - 1) % tp_count) for i in range(tp_count)]
    across = [(i, (i + 2) % tp_count) for i in range(tp_count)]

    top_count = route_ids.shape[1]
    chunk_rows = 2 * (share + capacity)
    total_rows = ep_count * chunk_rows
    pack = jnp.concatenate([dense_gate.T, dense_up.T, dense_down], axis=0)
    units = dense_down.shape[0]
    front_bytes = w_query.size * 4 * 2 + cell_state.size * 4
    (
        heads, carry, written, value, new_norm, new_max, slots, select, w_mix, tok, gain,
    ) = pl.pallas_call(
        front_kernel,
        in_specs=[SMEM] + [ANY] * 16,
        out_specs=[VMEM] + [ANY] * 6 + [VMEM] * 4,
        out_shape=[
            pltpu.VMEM((seqs, head_count * hd), BF),
            pltpu.HBM((pair_rows, hd), F32),
            pltpu.HBM((pair_rows, hd), F32),
            pltpu.HBM((pair_rows, hd), F32),
            pltpu.HBM((pair_rows, hd), F32),
            pltpu.HBM((head_count, seqs), F32),
            pltpu.HBM((seqs, 128), jnp.int32),
            pltpu.VMEM((total_rows, 128), BF),
            pltpu.VMEM(w_mix_out.shape, BF),
            pltpu.VMEM(tokens.shape, BF),
            pltpu.VMEM((1, width), F32),
        ],
        scratch_shapes=[
            pltpu.VMEM((top_count, seqs), jnp.int32),
            pltpu.VMEM((seqs, 128), jnp.int32),
            pltpu.VMEM((1, width), F32),
            pltpu.VMEM((head_count, width), BF),
            pltpu.VMEM((head_count, width), BF),
            pltpu.SMEM((head_count,), F32),
            pltpu.SMEM((head_count,), F32),
            pltpu.VMEM((pair_rows, hd), F32),
            pltpu.VMEM((head_count, seqs), F32),
            pltpu.VMEM((4, *w_query.shape), BF),
            pltpu.VMEM(cell_state.shape, F32),
            pltpu.VMEM((head_count, seqs, hd), F32),
            pltpu.VMEM((pair_rows, hd), F32),
            pltpu.VMEM((pair_rows, hd), F32),
            pltpu.VMEM((pair_rows, hd), F32),
            pltpu.VMEM((pair_rows, hd), F32),
            pltpu.VMEM((head_count, seqs), F32),
            pltpu.VMEM((128, seqs * hd), BF),
            pltpu.SemaphoreType.DMA((10,)),
            pltpu.SemaphoreType.DMA((5,)),
            pltpu.SemaphoreType.DMA((6,)),
            pltpu.SemaphoreType.DMA((6,)),
        ],
        compiler_params=params(40),
        cost_estimate=pl.CostEstimate(
            flops=2 * seqs * width * 4 * head_count * hd, transcendentals=0, bytes_accessed=front_bytes
        ),
        name="front",
    )(place.reshape(1), *(far_memory(a) for a in (
        route_ids.T,
        tokens,
        mix_gain.reshape(1, width),
        w_ingate.T,
        w_forget.T,
        in_bias,
        forget_bias,
        norm_state.reshape(pair_rows, hd),
        max_state.T,
        w_query,
        w_key,
        w_value,
        w_outgate,
        cell_state,
        w_mix_out,
        moe_gain.reshape(1, width),
    )))
    heads_l = lax.ppermute(heads, "x", right)
    heads_r = lax.ppermute(heads, "x", left)
    heads_f = lax.ppermute(heads, "x", across)
    pack_l = lax.ppermute(pack, "x", right)
    pack_r = lax.ppermute(pack, "x", left)
    cut = pack.shape[0] // 2
    head_f = lax.ppermute(pack_l[:cut], "x", right)
    tail_f = lax.ppermute(pack_r[cut:], "x", left)
    packs = [pack, pack_l, pack_r, head_f, tail_f]
    packs += [lax.ppermute(w, "c", swap) for w in packs]

    send, own, moe_in = pl.pallas_call(
        mix_kernel,
        in_specs=[SMEM] + [VMEM] * 8,
        out_specs=[ANY, VMEM, VMEM],
        out_shape=[
            pltpu.HBM((total_rows, half), BF),
            pltpu.HBM((seqs, cols), BF),
            pltpu.HBM((seqs, width), BF),
        ],
        scratch_shapes=[pltpu.VMEM((total_rows, half), BF), pltpu.SemaphoreType.DMA((4,))],
        compiler_params=params(30),
        cost_estimate=pl.CostEstimate(
            flops=2 * seqs * width * w_mix_out.shape[0], transcendentals=0, bytes_accessed=w_mix_out.size * 2
        ),
        name="mix",
    )(
        place.reshape(1),
        *(near_memory(a) for a in (heads, heads_l, heads_r, heads_f, w_mix, tok, gain, select)),
    )
    arrived = lax.all_to_all(
        send.reshape(ep_count, chunk_rows, half), EP, split_axis=0, concat_axis=0, tiled=True
    )
    sources = ep_count * tp_count
    quarter = cols // 2
    picks, weight = pl.pallas_call(
        plan_kernel,
        in_specs=[VMEM] * 3,
        out_specs=[VMEM] * 2,
        out_shape=[
            pltpu.HBM((6 * seqs, sources * chunk_rows), BF),
            pltpu.HBM((seqs, 128), F32),
        ],
        compiler_params=params(),
        name="plan",
    )(slots, moe_in, branch_gate.reshape(1, width))
    many = ep_count * share
    back = pl.pallas_call(
        ffn_kernel,
        in_specs=[VMEM] + [ANY] * 13,
        out_specs=ANY,
        out_shape=pltpu.HBM((ep_count, tp_count, chunk_rows, quarter), BF),
        scratch_shapes=[
            pltpu.VMEM(expert_gate.shape, BF),
            pltpu.VMEM(expert_up.shape, BF),
            pltpu.VMEM(expert_down.shape, BF),
            pltpu.VMEM((8 * units, width), BF),
            pltpu.VMEM((8 * units, width), BF),
            pltpu.VMEM((8 * units, width), BF),
            pltpu.VMEM((2, many, width), BF),
            pltpu.VMEM((tp_count, ep_count, chunk_rows, quarter), BF),
            pltpu.SemaphoreType.DMA((29,)),
            pltpu.SemaphoreType.DMA((tp_count,)),
        ],
        compiler_params=params(46),
        cost_estimate=pl.CostEstimate(
            flops=6 * many * width * (8 * units + expert_down.shape[1]),
            transcendentals=0,
            bytes_accessed=6 * width * (8 * units + expert_down.shape[1]),
        ),
        name="ffn",
    )(near_memory(arrived.reshape(total_rows, half)), *(far_memory(a) for a in (
        expert_gate, expert_up, expert_down,
        *packs,
    )))
    returned = lax.all_to_all(
        back.reshape(sources, chunk_rows, quarter), ALL, split_axis=0, concat_axis=0, tiled=True
    )
    pairs = 16
    flat = pl.BlockSpec((pairs, hd), lambda i: (i, 0))
    cube = pl.BlockSpec((pairs, hd, hd), lambda i: (i, 0, 0))
    new_cell = pl.pallas_call(
        update_kernel,
        grid=(pair_rows // pairs,),
        in_specs=[flat, flat, flat, cube],
        out_specs=cube,
        out_shape=pltpu.HBM((pair_rows, hd, hd), F32),
        compiler_params=params(),
        cost_estimate=pl.CostEstimate(
            flops=3 * cell_state.size, transcendentals=0, bytes_accessed=8 * cell_state.size
        ),
        name="update",
    )(carry, written, value, far_memory(cell_state.reshape(pair_rows, hd, hd)))
    layer_out = pl.pallas_call(
        final_kernel,
        in_specs=[ANY, VMEM, ANY, ANY, ANY],
        out_specs=VMEM,
        out_shape=pltpu.HBM((seqs, cols), BF),
        scratch_shapes=[
            pltpu.VMEM((6 * seqs, sources * chunk_rows), BF),
            pltpu.VMEM((seqs, cols), BF),
            pltpu.VMEM((seqs, 128), F32),
            pltpu.VMEM(route_weights.shape, F32),
            pltpu.SemaphoreType.DMA((4,)),
        ],
        compiler_params=params(40),
        name="final",
    )(
        far_memory(picks),
        near_memory(returned.reshape(sources * chunk_rows, quarter)),
        *(far_memory(a) for a in (own, weight, route_weights)),
    )
    return (
        layer_out,
        new_cell.reshape(cell_state.shape),
        new_norm.reshape(norm_state.shape),
        new_max.T,
    )


def solution(mesh):
    ep_count, tp_count = mesh.shape["ep"], mesh.shape["tp"]
    mesh = Mesh(mesh.devices.reshape(ep_count // CORES, CORES, tp_count), ALL)
    in_specs = (
        P(EP, None),
        P(),
        P(None, "x"),
        P(None, "x"),
        P(None, "x"),
        P(None, "x"),
        P(None, "x"),
        P(None, "x"),
        P("x"),
        P("x"),
        P(),
        P(EP, "x", None, None),
        P(EP, "x", None),
        P(EP, "x"),
        P(),
        P(EP, None),
        P(EP, None),
        P(EP, None, "x"),
        P(EP, None, "x"),
        P(EP, "x", None),
        P(),
        P(None, ALL),
        P(None, ALL),
        P(ALL, None),
    )
    out_specs = (P(EP, "x"), P(EP, "x", None, None), P(EP, "x", None), P(EP, "x"))
    return jax.shard_map(local, mesh=mesh, in_specs=in_specs, out_specs=out_specs, check_vma=False)
```

time: 115 us -> 100 us (0.87)
  Pallas kernels: 38.1 us -> 31.6 us
  starting transfers between devices: 29.3 us -> 24.6 us
  local copies, waits for them, and re-layouts: 4.08 us -> 2.37 us
    ppermute x14 -> x9, waiting for transfers between devices: 21.2 us -> 8.49 us  [the longest x1 7.62 us: local(): head_f = lax.ppermute(pack_l[:cut], 'x', right)]
    all_to_all x1, waiting for transfers between devices: 0.01 us -> 10.1 us  [local(): lax.all_to_all(send.reshape(ep_count, chunk_rows, half), EP, split_axis=0...]
    pallas_call x6 -> x5, Pallas kernels: 29.9 us -> 23.3 us  [the longest x1 7.78 us: local(): pl.pallas_call(front_kernel, in_specs=[SMEM] + [ANY] * 16, out_specs=[VME...]
    ppermute x1, waiting for transfers between devices: 0.01 us -> 5.89 us  [local(): heads_l = lax.ppermute(heads, 'x', right)]
    all_to_all x1, waiting for transfers between devices: 15.5 us -> 12.1 us  [local(): lax.all_to_all(back.reshape(sources, chunk_rows, quarter), ALL, split_axi...]
    all_to_all x1, starting transfers between devices: 7.51 us -> 4.66 us  [local(): lax.all_to_all(back.reshape(sources, chunk_rows, quarter), ALL, split_axi...]
    unnamed x31 -> x11, local copies, waits for them, and re-layouts: 3.47 us -> 0.73 us
    ppermute x14 -> x9, starting transfers between devices: 10.1 us -> 7.55 us  [the longest x1 2.16 us: local(): tail_f = lax.ppermute(pack_r[cut:], 'x', left)]
  transfers between devices with their start and end apart: 19 -> 14, of which waited for: 5 -> 7; matrix products, arithmetic and copies ran while one was open for 1% -> 2% of each run, Pallas kernels for 24% -> 22%
where the time goes in v2:
time: 100 us; the launch traced here: 98.8 us
  waiting for transfers between devices  38.3 us (38%)
  Pallas kernels  31.6 us (32%)
  starting transfers between devices  24.6 us (25%)
  local copies, waits for them, and re-layouts  2.37 us (2%)
  other arithmetic  1.16 us (1%)
    all_to_all x1, waiting for transfers between devices, local(): lax.all_to_all(back.reshape(sources, chunk_rows, quarter), ALL, split_axi...  12.1 us
    all_to_all x1, waiting for transfers between devices, local(): lax.all_to_all(send.reshape(ep_count, chunk_rows, half), EP, split_axis=0...  10.1 us
    all_to_all x1, starting transfers between devices, local(): lax.all_to_all(send.reshape(ep_count, chunk_rows, half), EP, split_axis=0...  8.35 us
    pallas_call x1, Pallas kernels, local(): pl.pallas_call(update_kernel, grid=(pair_rows // pairs,), in_specs=[flat,...  8.25 us
    pallas_call x1, Pallas kernels, local(): pl.pallas_call(front_kernel, in_specs=[SMEM] + [ANY] * 16, out_specs=[VME...  7.78 us
    ppermute x1, waiting for transfers between devices, local(): head_f = lax.ppermute(pack_l[:cut], 'x', right)  7.62 us
    pallas_call x1, Pallas kernels, local(): pl.pallas_call(ffn_kernel, in_specs=[VMEM] + [ANY] * 13, out_specs=ANY, o...  6.98 us
    ppermute x1, waiting for transfers between devices, local(): heads_l = lax.ppermute(heads, 'x', right)  5.89 us
  transfers between devices with their start and end apart: 14, of which 7 were waited for; matrix products, arithmetic and copies ran while one was open for 2% of the time, Pallas kernels for 22%

profile of v2, /device:TPU:0, one launch (start us, length us, event | category | flops | bytes accessed | tf_op | source)
XLA Modules:
  0.0 98.8 jit_solution(556092049622771328)
XLA Ops:
  0.6 1.2 %pad_maximum_fusion.rest_0_ = bf16[192,2048]{1,0:T(8,128)(2,1)S(1)} fusion(bf16[64,2048]{1,0:T(8,128)(2,1)} %param.47, bf16[64,2048]{1,0:T(8,128)(2,1)} %bitcast.24, bf16[64,2048]{1,0:T(8,128)(2,1)} %bitcast.25), kind=kLoop, calls=%fused_computation | loop fusion | flops 2359296 | bytes 1572864 | tf_op jit(solution)/shard_map/concatenate | solution.py:443
  1.8 0.0 copy-start
  1.8 1.7 %collective-permute-start.3 = (bf16[192,2048]{1,0:T(8,128)(2,1)S(1)}, bf16[192,2048]{1,0:T(8,128)(2,1)S(1)}, u32[]{:S(2)}, u32[]{:S(2)}) collective-permute-start(bf16[192,2048]{1,0:T(8,128)(2,1)S(1)} %pad_maximum_fusion.rest_0_), channel_id=1, source_target_pairs={{0,1},{1,2},{2,3},{3,0},{4,5},{5,6},{6,7},{7,4},{8,9},{9,10},{10,1... | collective-permute-start | bytes 2359304 | tf_op jit(solution)/shard_map/ppermute | solution.py:515
  3.5 1.6 %collective-permute-start.4 = (bf16[192,2048]{1,0:T(8,128)(2,1)S(1)}, bf16[192,2048]{1,0:T(8,128)(2,1)}, u32[]{:S(2)}, u32[]{:S(2)}) collective-permute-start(bf16[192,2048]{1,0:T(8,128)(2,1)S(1)} %pad_maximum_fusion.rest_0_), channel_id=1, source_target_pairs={{0,3},{1,0},{2,1},{3,2},{4,7},{5,4},{6,5},{7,6},{8,11},{9,8},{10,9... | collective-permute-start | bytes 2359304 | tf_op jit(solution)/shard_map/ppermute | solution.py:516
  5.1 7.8 %front.1 = (bf16[48,256]{1,0:T(8,128)(2,1)S(1)}, f32[96,128]{1,0:T(8,128)}, f32[96,128]{1,0:T(8,128)}, f32[96,128]{1,0:T(8,128)}, f32[96,128]{1,0:T(8,128)}, /*i...) custom-call(s32[1]{0:T(128)} %bitcast.place, ...), custom_call_target="tpu_custom_call" | custom-call | flops 201326592 | bytes 10485760 | tf_op jit(solution)/shard_map/front/pallas_call | solution.py:448
  12.9 0.5 collective-permute-start
  13.4 2.9 %collective-permute-start.1 = (bf16[48,256]{1,0:T(8,128)(2,1)S(1)}, bf16[48,256]{1,0:T(8,128)(2,1)S(1)}, u32[]{:S(2)}, u32[]{:S(2)}) collective-permute-start(bf16[48,256]{1,0:T(8,128)(2,1)S(1)} %get-tuple-element.21.heads), channel_id=1, source_target_pairs={{0,3},{1,0},{2,1},{3,2},{4,7},{5,4},{6,5},{7,6},{8,11},{9,8},{10,9... | collective-permute-start | bytes 73736 | tf_op jit(solution)/shard_map/ppermute | solution.py:513
  16.2 0.7 collective-permute-start.2
  16.9 5.9 %collective-permute-done.heads_l = bf16[48,256]{1,0:T(8,128)(2,1)S(1)} collective-permute-done((bf16[48,256]{1,0:T(8,128)(2,1)S(1)}, bf16[48,256]{1,0:T(8,128)(2,1)S(1)}, u32[]{:S(2)}, u32[]{:S(2)}) %collective-permute-start) | collective-permute-done | bytes 24608 | tf_op jit(solution)/shard_map/ppermute | solution.py:512
  22.8 0.5 collective-permute-done.1.heads_r
  23.3 1.2 %collective-permute-done.2.heads_f = bf16[48,256]{1,0:T(8,128)(2,1)S(1)} collective-permute-done((bf16[48,256]{1,0:T(8,128)(2,1)S(1)}, bf16[48,256]{1,0:T(8,128)(2,1)S(1)}, u32[]{:S(2)}, u32[]{:S(2)}) %collective-permute-start.2) | collective-permute-done | bytes 24608 | tf_op jit(solution)/shard_map/ppermute | solution.py:514
  24.5 3.0 %mix.1 = (bf16[768,1024]{1,0:T(8,128)(2,1)}, bf16[48,512]{1,0:T(8,128)(2,1)}, bf16[48,2048]{1,0:T(8,128)(2,1)}) custom-call(s32[1]{0:T(128)} %bitcast.place, bf16[48,256]{1,0:T(8,128)(2,1)S(1)} %get-tuple-element.21.heads, bf16[48,256]{1,0:T(8,128)(2,1)S(1)} %collective-permute-done.heads_l, bf16[48,256]{1,0:T(8,128)(2,1)S(1)} %collective-permute-done.1.heads_r, ...), custom_call_target="tpu_custom_call" | custom-call | flops 201326592 | bytes 4194304 | tf_op jit(solution)/shard_map/mix/pallas_call | solution.py:523
  27.6 8.3 %all-to-all-start = ((bf16[32,24,1024]{2,1,0:T(8,128)(2,1)}), bf16[32,24,1024]{2,1,0:T(8,128)(2,1)S(1)}, u32[]{:S(2)}, u32[]{:S(2)}) async-start(bf16[32,24,1024]{2,1,0:T(8,128)(2,1)} %bitcast.23), calls=%async_computation | async-start | bytes 3145728 | tf_op jit(solution)/shard_map/all_to_all | solution.py:542
  35.9 0.0 copy-done
  35.9 0.4 collective-permute-start.7
  36.3 0.0 collective-permute-done.3.rest_1_
  36.3 0.0 copy-start.1
  36.3 1.2 %collective-permute-start.5 = (bf16[96,2048]{1,0:T(8,128)(2,1)S(1)}, bf16[96,2048]{1,0:T(8,128)(2,1)S(1)}, u32[]{:S(2)}, u32[]{:S(2)}) collective-permute-start(bf16[96,2048]{1,0:T(8,128)(2,1)S(1)} %slice.8), channel_id=1, source_target_pairs={{0,1},{1,2},{2,3},{3,0},{4,5},{5,6},{6,7},{7,4},{8,9},{9,10},{10,1... | collective-permute-start | bytes 1179656 | tf_op jit(solution)/shard_map/ppermute | solution.py:518
  37.5 0.0 collective-permute-done.4.rest_2_
  37.5 1.0 %slice.9 = bf16[96,2048]{1,0:T(8,128)(2,1)S(1)} slice(bf16[192,2048]{1,0:T(8,128)(2,1)} %collective-permute-done.4.rest_2_), slice={[96:192], [0:2048]} | slice | bytes 786432 | tf_op jit(solution)/shard_map/slice | solution.py:519
  38.6 2.2 %collective-permute-start.6 = (bf16[96,2048]{1,0:T(8,128)(2,1)S(1)}, bf16[96,2048]{1,0:T(8,128)(2,1)}, u32[]{:S(2)}, u32[]{:S(2)}) collective-permute-start(bf16[96,2048]{1,0:T(8,128)(2,1)S(1)} %slice.9), channel_id=1, source_target_pairs={{0,3},{1,0},{2,1},{3,2},{4,7},{5,4},{6,5},{7,6},{8,11},{9,8},{10,9... | collective-permute-start | bytes 1179656 | tf_op jit(solution)/shard_map/ppermute | solution.py:519
  40.7 0.0 collective-permute-start.8
  40.7 0.5 collective-permute-start.9
  41.2 7.6 %collective-permute-done.5.rest_3_ = bf16[96,2048]{1,0:T(8,128)(2,1)S(1)} collective-permute-done((bf16[96,2048]{1,0:T(8,128)(2,1)S(1)}, bf16[96,2048]{1,0:T(8,128)(2,1)S(1)}, u32[]{:S(2)}, u32[]{:S(2)}) %collective-permute-start.5) | collective-permute-done | bytes 393248 | tf_op jit(solution)/shard_map/ppermute | solution.py:518
  48.9 0.0 copy-start.2
  48.9 0.0 collective-permute-start.10
  48.9 0.8 collective-permute-done.6.rest_4_
  49.7 0.0 collective-permute-start.11
  49.7 0.0 collective-permute-done.7.rest_5_
  49.7 10.1 %all-to-all-done = bf16[32,24,1024]{2,1,0:T(8,128)(2,1)S(1)} async-done(((bf16[32,24,1024]{2,1,0:T(8,128)(2,1)}), bf16[32,24,1024]{2,1,0:T(8,128)(2,1)S(1)}, u32[]{:S(2)}, u32[]{:S(2)}) %all-to-all-start) | async-done | bytes 1572896 | tf_op jit(solution)/shard_map/all_to_all | solution.py:542
  59.8 0.0 collective-permute-done.10.rest_8_
  59.8 0.0 collective-permute-done.11.rest_9_
  59.8 0.0 collective-permute-done.8.rest_6_
  59.8 0.0 collective-permute-done.9.rest_7_
  59.9 0.0 copy-done.1
  59.9 0.0 copy-done.2
  59.9 7.0 %ffn.1 = bf16[32,4,24,256]{3,2,1,0:T(8,128)(2,1)} custom-call(bf16[768,1024]{1,0:T(8,128)(2,1)S(1)} %bitcast.18, bf16[1,2048,256]{2,1,0:T(8,128)(2,1)} %e_gate.1, bf16[1,2048,256]{2,1,0:T(8,128)(2,1)} %e_up.1, bf16[1,256,2048]{2,1,0:T(8,128)(2,1)} %e_down.1, bf16[192,2048]{1,0:T(8,128)(2,1)} %copy-done, bf16[192,2048]{1,0:T(8,128)(2,1)} %copy-done.1, ...), custom_call_target="tpu_custom_call" | custom-call | flops 1811939328 | bytes 9437184 | tf_op jit(solution)/shard_map/ffn/pallas_call | solution.py:559
  66.9 0.0 copy-start.3
  66.9 0.0 copy-start.4
  66.9 4.7 %all-to-all-start.1 = ((bf16[128,24,256]{2,1,0:T(8,128)(2,1)}), bf16[128,24,256]{2,1,0:T(8,128)(2,1)S(1)}, u32[]{:S(2)}, u32[]{:S(2)}) async-start(bf16[128,24,256]{2,1,0:T(8,128)(2,1)} %bitcast.22), calls=%async_computation.1 | async-start | bytes 3145728 | tf_op jit(solution)/shard_map/all_to_all | solution.py:587
  71.5 0.0 copy-done.3
  71.6 0.6 reshape.49.branch
  72.2 0.0 copy-done.4
  72.2 0.7 copy.28.route_h
  72.9 8.3 %update.1 = f32[96,128,128]{2,1,0:T(8,128)} custom-call(f32[96,128]{1,0:T(8,128)} %get-tuple-element.31.carry, f32[96,128]{1,0:T(8,128)} %get-tuple-element.32.written, f32[96,128]{1,0:T(8,128)} %get-tuple-element.33.value, f32[96,128,128]{2,1,0:T(8,128)} %bitcast.20), custom_call_target="tpu_custom_call" | custom-call | flops 4718592 | bytes 12582912 | tf_op jit(solution)/shard_map/update/pallas_call | solution.py:593
  81.1 2.7 %plan.1 = (bf16[288,3072]{1,0:T(8,128)(2,1)}, f32[48,128]{1,0:T(8,128)}) custom-call(s32[48,128]{1,0:T(8,128)} %get-tuple-element.20.slots, bf16[48,2048]{1,0:T(8,128)(2,1)} %get-tuple-element.26.moe_in, bf16[1,2048]{1,0:T(2,128)(2,1)} %reshape.49.branch), custom_call_target="tpu_custom_call" | custom-call | tf_op jit(solution)/shard_map/plan/pallas_call | solution.py:547
  83.8 12.1 %all-to-all-done.1 = bf16[128,24,256]{2,1,0:T(8,128)(2,1)S(1)} async-done(((bf16[128,24,256]{2,1,0:T(8,128)(2,1)}), bf16[128,24,256]{2,1,0:T(8,128)(2,1)S(1)}, u32[]{:S(2)}, u32[]{:S(2)}) %all-to-all-start.1) | async-done | bytes 1572896 | tf_op jit(solution)/shard_map/all_to_all | solution.py:587
  96.0 2.8 %final.1 = bf16[48,512]{1,0:T(8,128)(2,1)} custom-call(bf16[288,3072]{1,0:T(8,128)(2,1)} %get-tuple-element.27.picks_h, bf16[3072,256]{1,0:T(8,128)(2,1)S(1)} %bitcast.19, bf16[48,512]{1,0:T(8,128)(2,1)} %get-tuple-element.29.own_h, f32[48,128]{1,0:T(8,128)} %get-tuple-element.30.weight_h, f32[48,2]{1,0:T(8,128)} %copy.28.route_h), custom_call_target="tpu_custom_call" | custom-call | tf_op jit(solution)/shard_map/final/pallas_call | solution.py:605
  (1 shorter events, 0.0 us)
Async XLA Ops:
  1.8 34.1 %copy-start = (bf16[192,2048]{1,0:T(8,128)(2,1)}, bf16[192,2048]{1,0:T(8,128)(2,1)S(1)}, u32[]{:S(2)}) copy-start(bf16[192,2048]{1,0:T(8,128)(2,1)S(1)} %pad_maximum_fusion.rest_0_) | copy-start | bytes 2359300
  1.8 34.5 %collective-permute-start.3 = (bf16[192,2048]{1,0:T(8,128)(2,1)S(1)}, bf16[192,2048]{1,0:T(8,128)(2,1)S(1)}, u32[]{:S(2)}, u32[]{:S(2)}) collective-permute-start(bf16[192,2048]{1,0:T(8,128)(2,1)S(1)} %pad_maximum_fusion.rest_0_), channel_id=1, source_target_pairs={{0,1},{1,2},{2,3},{3,0},{4,5},{5,6},{6,7},{7,4},{8,9},{9,10},{10,1... | collective-permute-start | bytes 2359304 | tf_op jit(solution)/shard_map/ppermute | solution.py:515
  3.5 34.1 %collective-permute-start.4 = (bf16[192,2048]{1,0:T(8,128)(2,1)S(1)}, bf16[192,2048]{1,0:T(8,128)(2,1)}, u32[]{:S(2)}, u32[]{:S(2)}) collective-permute-start(bf16[192,2048]{1,0:T(8,128)(2,1)S(1)} %pad_maximum_fusion.rest_0_), channel_id=1, source_target_pairs={{0,3},{1,0},{2,1},{3,2},{4,7},{5,4},{6,5},{7,6},{8,11},{9,8},{10,9... | collective-permute-start | bytes 2359304 | tf_op jit(solution)/shard_map/ppermute | solution.py:516
  12.9 9.9 %collective-permute-start = (bf16[48,256]{1,0:T(8,128)(2,1)S(1)}, bf16[48,256]{1,0:T(8,128)(2,1)S(1)}, u32[]{:S(2)}, u32[]{:S(2)}) collective-permute-start(bf16[48,256]{1,0:T(8,128)(2,1)S(1)} %get-tuple-element.21.heads), channel_id=1, source_target_pairs={{0,1},{1,2},{2,3},{3,0},{4,5},{5,6},{6,7},{7,4},{8,9},{9,10},{10,1... | collective-permute-start | bytes 73736 | tf_op jit(solution)/shard_map/ppermute | solution.py:512
  13.4 9.9 %collective-permute-start.1 = (bf16[48,256]{1,0:T(8,128)(2,1)S(1)}, bf16[48,256]{1,0:T(8,128)(2,1)S(1)}, u32[]{:S(2)}, u32[]{:S(2)}) collective-permute-start(bf16[48,256]{1,0:T(8,128)(2,1)S(1)} %get-tuple-element.21.heads), channel_id=1, source_target_pairs={{0,3},{1,0},{2,1},{3,2},{4,7},{5,4},{6,5},{7,6},{8,11},{9,8},{10,9... | collective-permute-start | bytes 73736 | tf_op jit(solution)/shard_map/ppermute | solution.py:513
  16.2 8.3 %collective-permute-start.2 = (bf16[48,256]{1,0:T(8,128)(2,1)S(1)}, bf16[48,256]{1,0:T(8,128)(2,1)S(1)}, u32[]{:S(2)}, u32[]{:S(2)}) collective-permute-start(bf16[48,256]{1,0:T(8,128)(2,1)S(1)} %get-tuple-element.21.heads), channel_id=1, source_target_pairs={{0,2},{1,3},{2,0},{3,1},{4,6},{5,7},{6,4},{7,5},{8,10},{9,11},{10,... | collective-permute-start | bytes 73736 | tf_op jit(solution)/shard_map/ppermute | solution.py:514
  27.6 32.3 %all-to-all-start = ((bf16[32,24,1024]{2,1,0:T(8,128)(2,1)}), bf16[32,24,1024]{2,1,0:T(8,128)(2,1)S(1)}, u32[]{:S(2)}, u32[]{:S(2)}) async-start(bf16[32,24,1024]{2,1,0:T(8,128)(2,1)} %bitcast.23), calls=%async_computation | async-start | bytes 3145728 | tf_op jit(solution)/shard_map/all_to_all | solution.py:542
  35.9 13.8 %collective-permute-start.7 = (bf16[192,2048]{1,0:T(8,128)(2,1)S(1)}, bf16[192,2048]{1,0:T(8,128)(2,1)}, u32[]{:S(2)}, u32[]{:S(2)}) collective-permute-start(bf16[192,2048]{1,0:T(8,128)(2,1)S(1)} %pad_maximum_fusion.rest_0_), channel_id=1, source_target_pairs={{0,4},{4,0},{1,5},{5,1},{2,6},{6,2},{3,7},{7,3},{8,12},{12,8},{9,1... | collective-permute-start | bytes 2359304 | tf_op jit(solution)/shard_map/ppermute | solution.py:521
  36.3 23.6 %copy-start.1 = (bf16[192,2048]{1,0:T(8,128)(2,1)}, bf16[192,2048]{1,0:T(8,128)(2,1)S(1)}, u32[]{:S(2)}) copy-start(bf16[192,2048]{1,0:T(8,128)(2,1)S(1)} %collective-permute-done.3.rest_1_) | copy-start | bytes 2359300
  36.3 12.5 %collective-permute-start.5 = (bf16[96,2048]{1,0:T(8,128)(2,1)S(1)}, bf16[96,2048]{1,0:T(8,128)(2,1)S(1)}, u32[]{:S(2)}, u32[]{:S(2)}) collective-permute-start(bf16[96,2048]{1,0:T(8,128)(2,1)S(1)} %slice.8), channel_id=1, source_target_pairs={{0,1},{1,2},{2,3},{3,0},{4,5},{5,6},{6,7},{7,4},{8,9},{9,10},{10,1... | collective-permute-start | bytes 1179656 | tf_op jit(solution)/shard_map/ppermute | solution.py:518
  38.6 11.2 %collective-permute-start.6 = (bf16[96,2048]{1,0:T(8,128)(2,1)S(1)}, bf16[96,2048]{1,0:T(8,128)(2,1)}, u32[]{:S(2)}, u32[]{:S(2)}) collective-permute-start(bf16[96,2048]{1,0:T(8,128)(2,1)S(1)} %slice.9), channel_id=1, source_target_pairs={{0,3},{1,0},{2,1},{3,2},{4,7},{5,4},{6,5},{7,6},{8,11},{9,8},{10,9... | collective-permute-start | bytes 1179656 | tf_op jit(solution)/shard_map/ppermute | solution.py:519
  40.7 19.1 %collective-permute-start.8 = (bf16[192,2048]{1,0:T(8,128)(2,1)S(1)}, bf16[192,2048]{1,0:T(8,128)(2,1)}, u32[]{:S(2)}, u32[]{:S(2)}) collective-permute-start(bf16[192,2048]{1,0:T(8,128)(2,1)S(1)} %collective-permute-done.3.rest_1_), channel_id=1, source_target_pairs={{0,4},{4,0},{1,5},{5,1},{2,6},{6,2},{3,7},{7,3},{8,12},{12,8},{9,1... | collective-permute-start | bytes 2359304 | tf_op jit(solution)/shard_map/ppermute | solution.py:521
  40.7 19.1 %collective-permute-start.9 = (bf16[192,2048]{1,0:T(8,128)(2,1)}, bf16[192,2048]{1,0:T(8,128)(2,1)}, u32[]{:S(2)}, u32[]{:S(2)}) collective-permute-start(bf16[192,2048]{1,0:T(8,128)(2,1)} %collective-permute-done.4.rest_2_), channel_id=1, source_target_pairs={{0,4},{4,0},{1,5},{5,1},{2,6},{6,2},{3,7},{7,3},{8,12},{12,8},{9,1... | collective-permute-start | bytes 2359304 | tf_op jit(solution)/shard_map/ppermute | solution.py:521
  48.9 11.0 %copy-start.2 = (bf16[96,2048]{1,0:T(8,128)(2,1)}, bf16[96,2048]{1,0:T(8,128)(2,1)S(1)}, u32[]{:S(2)}) copy-start(bf16[96,2048]{1,0:T(8,128)(2,1)S(1)} %collective-permute-done.5.rest_3_) | copy-start | bytes 1179652
  48.9 11.0 %collective-permute-start.10 = (bf16[96,2048]{1,0:T(8,128)(2,1)S(1)}, bf16[96,2048]{1,0:T(8,128)(2,1)}, u32[]{:S(2)}, u32[]{:S(2)}) collective-permute-start(bf16[96,2048]{1,0:T(8,128)(2,1)S(1)} %collective-permute-done.5.rest_3_), channel_id=1, source_target_pairs={{0,4},{4,0},{1,5},{5,1},{2,6},{6,2},{3,7},{7,3},{8,12},{12,8},{9,1... | collective-permute-start | bytes 1179656 | tf_op jit(solution)/shard_map/ppermute | solution.py:521
  49.7 10.1 %collective-permute-start.11 = (bf16[96,2048]{1,0:T(8,128)(2,1)}, bf16[96,2048]{1,0:T(8,128)(2,1)}, u32[]{:S(2)}, u32[]{:S(2)}) collective-permute-start(bf16[96,2048]{1,0:T(8,128)(2,1)} %collective-permute-done.6.rest_4_), channel_id=1, source_target_pairs={{0,4},{4,0},{1,5},{5,1},{2,6},{6,2},{3,7},{7,3},{8,12},{12,8},{9,1... | collective-permute-start | bytes 1179656 | tf_op jit(solution)/shard_map/ppermute | solution.py:521
  66.9 4.7 %copy-start.3 = (bf16[2048]{0:T(1024)(128)(2,1)S(1)}, bf16[2048]{0:T(1024)(128)(2,1)}, u32[]{:S(2)}) copy-start(bf16[2048]{0:T(1024)(128)(2,1)} %param.44) | copy-start | bytes 12292
  66.9 5.3 %copy-start.4 = (f32[48,2]{0,1:T(2,128)S(1)}, f32[48,2]{0,1:T(2,128)}, u32[]{:S(2)}) copy-start(f32[48,2]{0,1:T(2,128)} %param.40) | copy-start | bytes 1156
  66.9 29.1 %all-to-all-start.1 = ((bf16[128,24,256]{2,1,0:T(8,128)(2,1)}), bf16[128,24,256]{2,1,0:T(8,128)(2,1)S(1)}, u32[]{:S(2)}, u32[]{:S(2)}) async-start(bf16[128,24,256]{2,1,0:T(8,128)(2,1)} %bitcast.22), calls=%async_computation.1 | async-start | bytes 3145728 | tf_op jit(solution)/shard_map/all_to_all | solution.py:587

commit v3 on v2

--- a/solution.py
+++ b/solution.py
@@ -303,22 +303,16 @@
 
 
 def ffn_kernel(abuf, e_gate, e_up, e_down, *rest):
-    packs, rest = rest[:10], rest[10:]
+    packs, rest = rest[:8], rest[8:]
     out, egbuf, eubuf, edbuf, gbuf, ubuf, dbuf, xbuf, obuf, sems, osems = rest
     units = packs[0].shape[0] // 3
-    mid = units // 2
-    pairs = [(e_gate, egbuf), (e_up, eubuf), (e_down, edbuf)]
-    for side in range(2):
-        for b in range(3):
-            pack, rows = packs[5 * side + b], pl.ds((4 * side + b) * units, units)
-            pairs.append((pack.at[pl.ds(0, units)], gbuf.at[rows]))
-            pairs.append((pack.at[pl.ds(units, units)], ubuf.at[rows]))
-            pairs.append((pack.at[pl.ds(2 * units, units)], dbuf.at[rows]))
-        head, tail, last = packs[5 * side + 3], packs[5 * side + 4], (4 * side + 3) * units
-        pairs.append((head.at[pl.ds(0, units)], gbuf.at[pl.ds(last, units)]))
-        pairs.append((head.at[pl.ds(units, mid)], ubuf.at[pl.ds(last, mid)]))
-        pairs.append((tail.at[pl.ds(0, mid)], ubuf.at[pl.ds(last + mid, mid)]))
-        pairs.append((tail.at[pl.ds(mid, units)], dbuf.at[pl.ds(last, units)]))
+    pairs = []
+    for b, pack in enumerate(packs):
+        rows = pl.ds(b * units, units)
+        pairs.append((pack.at[pl.ds(0, units)], gbuf.at[rows]))
+        pairs.append((pack.at[pl.ds(units, units)], ubuf.at[rows]))
+        pairs.append((pack.at[pl.ds(2 * units, units)], dbuf.at[rows]))
+    pairs += [(e_gate, egbuf), (e_up, eubuf), (e_down, edbuf)]
     loads = start_all(pairs, sems)
     size, half = abuf.shape
     block = 192
@@ -338,24 +332,24 @@
                 g * lines : (g + 1) * lines,
                 (part // 2) * half : (part // 2 + 1) * half,
             ] = sorted_rows[part * lines : (part + 1) * lines]
-    tok = xbuf[1]
-    loads[0].wait()
-    loads[1].wait()
-    gate_proj = jnp.dot(tok, egbuf[0], preferred_element_type=F32)
-    up_proj = jnp.dot(tok, eubuf[0], preferred_element_type=F32)
-    hidden = (jax.nn.silu(gate_proj) * up_proj).astype(BF)
-    loads[2].wait()
-    expert_out = jnp.dot(hidden, edbuf[0], preferred_element_type=F32).astype(BF)
     tok = xbuf[0]
     total = None
     for side in range(2):
-        for copy in loads[3 + 13 * side : 16 + 13 * side]:
+        for copy in loads[12 * side : 12 + 12 * side]:
             copy.wait()
         rows = slice(side * 4 * units, (side + 1) * 4 * units)
         hidden = (jax.nn.silu(nt_dot(tok, gbuf[rows])) * nt_dot(tok, ubuf[rows])).astype(BF)
         part = jnp.dot(hidden, dbuf[rows], preferred_element_type=F32)
         total = part if total is None else total + part
     total = total.astype(BF)
+    tok = xbuf[1]
+    loads[24].wait()
+    loads[25].wait()
+    gate_proj = jnp.dot(tok, egbuf[0], preferred_element_type=F32)
+    up_proj = jnp.dot(tok, eubuf[0], preferred_element_type=F32)
+    hidden = (jax.nn.silu(gate_proj) * up_proj).astype(BF)
+    loads[26].wait()
+    expert_out = jnp.dot(hidden, edbuf[0], preferred_element_type=F32).astype(BF)
     peers, quarter = obuf.shape[0], obuf.shape[3]
     held = obuf.shape[1] // groups
     stores = []
@@ -512,12 +506,12 @@
     heads_l = lax.ppermute(heads, "x", right)
     heads_r = lax.ppermute(heads, "x", left)
     heads_f = lax.ppermute(heads, "x", across)
-    pack_l = lax.ppermute(pack, "x", right)
-    pack_r = lax.ppermute(pack, "x", left)
-    cut = pack.shape[0] // 2
-    head_f = lax.ppermute(pack_l[:cut], "x", right)
-    tail_f = lax.ppermute(pack_r[cut:], "x", left)
-    packs = [pack, pack_l, pack_r, head_f, tail_f]
+    out_way = right + [(tp_count + i, tp_count + j) for i, j in left]
+    back_way = left + [(tp_count + i, tp_count + j) for i, j in right]
+    pack_1 = lax.ppermute(pack, ("c", "x"), out_way)
+    pack_2 = lax.ppermute(pack, ("c", "x"), back_way)
+    pack_3 = lax.ppermute(pack_1, ("c", "x"), out_way)
+    packs = [pack, pack_1, pack_2, pack_3]
     packs += [lax.ppermute(w, "c", swap) for w in packs]
 
     send, own, moe_in = pl.pallas_call(
@@ -558,7 +552,7 @@
     many = ep_count * share
     back = pl.pallas_call(
         ffn_kernel,
-        in_specs=[VMEM] + [ANY] * 13,
+        in_specs=[VMEM] + [ANY] * 11,
         out_specs=ANY,
         out_shape=pltpu.HBM((ep_count, tp_count, chunk_rows, quarter), BF),
         scratch_shapes=[
@@ -570,7 +564,7 @@
             pltpu.VMEM((8 * units, width), BF),
             pltpu.VMEM((2, many, width), BF),
             pltpu.VMEM((tp_count, ep_count, chunk_rows, quarter), BF),
-            pltpu.SemaphoreType.DMA((29,)),
+            pltpu.SemaphoreType.DMA((27,)),
             pltpu.SemaphoreType.DMA((tp_count,)),
         ],
         compiler_params=params(46),

time: 100 us -> 116 us (1.16)
  waiting for transfers between devices: 38.3 us -> 56.1 us
    all_to_all x1, waiting for transfers between devices: 10.1 us -> 21.4 us  [local(): lax.all_to_all(send.reshape(ep_count, chunk_rows, half), EP, split_axis=0...]
    ppermute x4 -> x3, waiting for transfers between devices: 8.48 us -> 16.9 us  [the longest x1 16.9 us: local(): pack_1 = lax.ppermute(pack, ('c', 'x'), out_way)]
    ppermute x1, waiting for transfers between devices: 5.89 us -> 0.73 us  [local(): heads_l = lax.ppermute(heads, 'x', right)]
    ppermute x1, waiting for transfers between devices: 1.25 us -> 3.53 us  [local(): heads_f = lax.ppermute(heads, 'x', across)]
    ppermute x4 -> x3, starting transfers between devices: 6.68 us -> 5.02 us  [the longest x1 1.71 us: local(): pack_3 = lax.ppermute(pack_1, ('c', 'x'), out_way)]
    ppermute x5 -> x4, waiting for transfers between devices: 0.01 us -> 1.39 us  [local(): packs += [lax.ppermute(w, 'c', swap) for w in packs]]
  transfers between devices with their start and end apart: 14 -> 12, of which waited for: 7 -> 6; matrix products, arithmetic and copies ran while one was open for 2% -> 1% of each run, Pallas kernels for 22% -> 19%
where the time goes in v3:
time: 116 us; the launch traced here: 114 us
  waiting for transfers between devices  56.1 us (48%)
  Pallas kernels  31.6 us (27%)
  starting transfers between devices  23.5 us (20%)
  local copies, waits for them, and re-layouts  1.31 us (1%)
  other arithmetic  1.16 us (1%)
    all_to_all x1, waiting for transfers between devices, local(): lax.all_to_all(send.reshape(ep_count, chunk_rows, half), EP, split_axis=0...  21.4 us
    ppermute x1, waiting for transfers between devices, local(): pack_1 = lax.ppermute(pack, ('c', 'x'), out_way)  16.9 us
    all_to_all x1, waiting for transfers between devices, local(): lax.all_to_all(back.reshape(sources, chunk_rows, quarter), ALL, split_axi...  12.1 us
    all_to_all x1, starting transfers between devices, local(): lax.all_to_all(send.reshape(ep_count, chunk_rows, half), EP, split_axis=0...  8.34 us
    pallas_call x1, Pallas kernels, local(): pl.pallas_call(update_kernel, grid=(pair_rows // pairs,), in_specs=[flat,...  8.25 us
    pallas_call x1, Pallas kernels, local(): pl.pallas_call(front_kernel, in_specs=[SMEM] + [ANY] * 16, out_specs=[VME...  7.78 us
    pallas_call x1, Pallas kernels, local(): pl.pallas_call(ffn_kernel, in_specs=[VMEM] + [ANY] * 11, out_specs=ANY, o...  7.01 us
    all_to_all x1, starting transfers between devices, local(): lax.all_to_all(back.reshape(sources, chunk_rows, quarter), ALL, split_axi...  4.66 us
  transfers between devices with their start and end apart: 12, of which 6 were waited for; matrix products, arithmetic and copies ran while one was open for 1% of the time, Pallas kernels for 19%

profile of v3, /device:TPU:0, one launch (start us, length us, event | category | flops | bytes accessed | tf_op | source)
XLA Modules:
  0.0 114.4 jit_solution(2312379257568513770)
XLA Ops:
  0.6 1.2 %pad_maximum_fusion.rest_0_ = bf16[192,2048]{1,0:T(8,128)(2,1)S(1)} fusion(bf16[64,2048]{1,0:T(8,128)(2,1)} %param.47, bf16[64,2048]{1,0:T(8,128)(2,1)} %bitcast.24, bf16[64,2048]{1,0:T(8,128)(2,1)} %bitcast.25), kind=kLoop, calls=%fused_computation | loop fusion | flops 2359296 | bytes 1572864 | tf_op jit(solution)/shard_map/concatenate | solution.py:437
  1.8 0.0 copy-start
  1.8 1.7 %collective-permute-start.3 = (bf16[192,2048]{1,0:T(8,128)(2,1)S(1)}, bf16[192,2048]{1,0:T(8,128)(2,1)S(1)}, u32[]{:S(2)}, u32[]{:S(2)}) collective-permute-start(bf16[192,2048]{1,0:T(8,128)(2,1)S(1)} %pad_maximum_fusion.rest_0_), channel_id=1, source_target_pairs={{0,1},{1,2},{2,3},{3,0},{4,7},{5,4},{6,5},{7,6},{8,9},{9,10},{10,1... | collective-permute-start | bytes 2359304 | tf_op jit(solution)/shard_map/ppermute | solution.py:511
  3.5 1.6 %collective-permute-start.4 = (bf16[192,2048]{1,0:T(8,128)(2,1)S(1)}, bf16[192,2048]{1,0:T(8,128)(2,1)}, u32[]{:S(2)}, u32[]{:S(2)}) collective-permute-start(bf16[192,2048]{1,0:T(8,128)(2,1)S(1)} %pad_maximum_fusion.rest_0_), channel_id=1, source_target_pairs={{0,3},{1,0},{2,1},{3,2},{4,5},{5,6},{6,7},{7,4},{8,11},{9,8},{10,9... | collective-permute-start | bytes 2359304 | tf_op jit(solution)/shard_map/ppermute | solution.py:512
  5.1 16.9 %collective-permute-done.3.rest_1_ = bf16[192,2048]{1,0:T(8,128)(2,1)S(1)} collective-permute-done((bf16[192,2048]{1,0:T(8,128)(2,1)S(1)}, bf16[192,2048]{1,0:T(8,128)(2,1)S(1)}, u32[]{:S(2)}, u32[]{:S(2)}) %collective-permute-start.3) | collective-permute-done | bytes 786464 | tf_op jit(solution)/shard_map/ppermute | solution.py:511
  22.0 0.0 copy-start.1
  22.0 1.7 %collective-permute-start.5 = (bf16[192,2048]{1,0:T(8,128)(2,1)S(1)}, bf16[192,2048]{1,0:T(8,128)(2,1)}, u32[]{:S(2)}, u32[]{:S(2)}) collective-permute-start(bf16[192,2048]{1,0:T(8,128)(2,1)S(1)} %collective-permute-done.3.rest_1_), channel_id=1, source_target_pairs={{0,1},{1,2},{2,3},{3,0},{4,7},{5,4},{6,5},{7,6},{8,9},{9,10},{10,1... | collective-permute-start | bytes 2359304 | tf_op jit(solution)/shard_map/ppermute | solution.py:513
  23.8 7.8 %front.1 = (bf16[48,256]{1,0:T(8,128)(2,1)S(1)}, f32[96,128]{1,0:T(8,128)}, f32[96,128]{1,0:T(8,128)}, f32[96,128]{1,0:T(8,128)}, f32[96,128]{1,0:T(8,128)}, /*i...) custom-call(s32[1]{0:T(128)} %bitcast.place, ...), custom_call_target="tpu_custom_call" | custom-call | flops 201326592 | bytes 10485760 | tf_op jit(solution)/shard_map/front/pallas_call | solution.py:442
  31.5 0.8 collective-permute-start
  32.4 2.5 %collective-permute-start.1 = (bf16[48,256]{1,0:T(8,128)(2,1)S(1)}, bf16[48,256]{1,0:T(8,128)(2,1)S(1)}, u32[]{:S(2)}, u32[]{:S(2)}) collective-permute-start(bf16[48,256]{1,0:T(8,128)(2,1)S(1)} %get-tuple-element.21.heads), channel_id=1, source_target_pairs={{0,3},{1,0},{2,1},{3,2},{4,7},{5,4},{6,5},{7,6},{8,11},{9,8},{10,9... | collective-permute-start | bytes 73736 | tf_op jit(solution)/shard_map/ppermute | solution.py:507
  34.8 1.1 collective-permute-start.2
  35.9 0.7 collective-permute-done.heads_l
  36.6 0.0 collective-permute-done.1.heads_r
  36.7 3.5 %collective-permute-done.2.heads_f = bf16[48,256]{1,0:T(8,128)(2,1)S(1)} collective-permute-done((bf16[48,256]{1,0:T(8,128)(2,1)S(1)}, bf16[48,256]{1,0:T(8,128)(2,1)S(1)}, u32[]{:S(2)}, u32[]{:S(2)}) %collective-permute-start.2) | collective-permute-done | bytes 24608 | tf_op jit(solution)/shard_map/ppermute | solution.py:508
  40.2 3.0 %mix.1 = (bf16[768,1024]{1,0:T(8,128)(2,1)}, bf16[48,512]{1,0:T(8,128)(2,1)}, bf16[48,2048]{1,0:T(8,128)(2,1)}) custom-call(s32[1]{0:T(128)} %bitcast.place, bf16[48,256]{1,0:T(8,128)(2,1)S(1)} %get-tuple-element.21.heads, bf16[48,256]{1,0:T(8,128)(2,1)S(1)} %collective-permute-done.heads_l, bf16[48,256]{1,0:T(8,128)(2,1)S(1)} %collective-permute-done.1.heads_r, ...), custom_call_target="tpu_custom_call" | custom-call | flops 201326592 | bytes 4194304 | tf_op jit(solution)/shard_map/mix/pallas_call | solution.py:517
  43.2 8.3 %all-to-all-start = ((bf16[32,24,1024]{2,1,0:T(8,128)(2,1)}), bf16[32,24,1024]{2,1,0:T(8,128)(2,1)S(1)}, u32[]{:S(2)}, u32[]{:S(2)}) async-start(bf16[32,24,1024]{2,1,0:T(8,128)(2,1)} %bitcast.23), calls=%async_computation | async-start | bytes 3145728 | tf_op jit(solution)/shard_map/all_to_all | solution.py:536
  51.6 0.0 copy-done
  51.6 0.4 collective-permute-start.6
  51.9 0.0 copy-done.1
  51.9 0.2 collective-permute-start.7
  52.2 0.0 collective-permute-done.4.rest_2_
  52.2 0.3 collective-permute-start.8
  52.5 0.0 collective-permute-done.5.rest_3_
  52.5 0.2 collective-permute-start.9
  52.7 1.4 %collective-permute-done.6.rest_4_ = bf16[192,2048]{1,0:T(8,128)(2,1)} collective-permute-done((bf16[192,2048]{1,0:T(8,128)(2,1)S(1)}, bf16[192,2048]{1,0:T(8,128)(2,1)}, u32[]{:S(2)}, u32[]{:S(2)}) %collective-permute-start.6) | collective-permute-done | bytes 786464 | tf_op jit(solution)/shard_map/ppermute | solution.py:515
  54.1 21.4 %all-to-all-done = bf16[32,24,1024]{2,1,0:T(8,128)(2,1)S(1)} async-done(((bf16[32,24,1024]{2,1,0:T(8,128)(2,1)}), bf16[32,24,1024]{2,1,0:T(8,128)(2,1)S(1)}, u32[]{:S(2)}, u32[]{:S(2)}) %all-to-all-start) | async-done | bytes 1572896 | tf_op jit(solution)/shard_map/all_to_all | solution.py:536
  75.5 0.0 collective-permute-done.7.rest_5_
  75.5 0.0 collective-permute-done.8.rest_6_
  75.5 0.0 collective-permute-done.9.rest_7_
  75.5 7.0 %ffn.1 = bf16[32,4,24,256]{3,2,1,0:T(8,128)(2,1)} custom-call(bf16[768,1024]{1,0:T(8,128)(2,1)S(1)} %bitcast.18, bf16[1,2048,256]{2,1,0:T(8,128)(2,1)} %e_gate.1, bf16[1,2048,256]{2,1,0:T(8,128)(2,1)} %e_up.1, bf16[1,256,2048]{2,1,0:T(8,128)(2,1)} %e_down.1, bf16[192,2048]{1,0:T(8,128)(2,1)} %copy-done, bf16[192,2048]{1,0:T(8,128)(2,1)} %copy-done.1, ...), custom_call_target="tpu_custom_call" | custom-call | flops 1811939328 | bytes 9437184 | tf_op jit(solution)/shard_map/ffn/pallas_call | solution.py:553
  82.5 0.0 copy-start.2
  82.5 0.0 copy-start.3
  82.5 4.7 %all-to-all-start.1 = ((bf16[128,24,256]{2,1,0:T(8,128)(2,1)}), bf16[128,24,256]{2,1,0:T(8,128)(2,1)S(1)}, u32[]{:S(2)}, u32[]{:S(2)}) async-start(bf16[128,24,256]{2,1,0:T(8,128)(2,1)} %bitcast.22), calls=%async_computation.1 | async-start | bytes 3145728 | tf_op jit(solution)/shard_map/all_to_all | solution.py:581
  87.2 0.0 copy-done.2
  87.2 0.6 reshape.49.branch
  87.8 0.0 copy-done.3
  87.8 0.7 copy.28.route_h
  88.5 8.3 %update.1 = f32[96,128,128]{2,1,0:T(8,128)} custom-call(f32[96,128]{1,0:T(8,128)} %get-tuple-element.31.carry, f32[96,128]{1,0:T(8,128)} %get-tuple-element.32.written, f32[96,128]{1,0:T(8,128)} %get-tuple-element.33.value, f32[96,128,128]{2,1,0:T(8,128)} %bitcast.20), custom_call_target="tpu_custom_call" | custom-call | flops 4718592 | bytes 12582912 | tf_op jit(solution)/shard_map/update/pallas_call | solution.py:587
  96.8 2.7 %plan.1 = (bf16[288,3072]{1,0:T(8,128)(2,1)}, f32[48,128]{1,0:T(8,128)}) custom-call(s32[48,128]{1,0:T(8,128)} %get-tuple-element.20.slots, bf16[48,2048]{1,0:T(8,128)(2,1)} %get-tuple-element.26.moe_in, bf16[1,2048]{1,0:T(2,128)(2,1)} %reshape.49.branch), custom_call_target="tpu_custom_call" | custom-call | tf_op jit(solution)/shard_map/plan/pallas_call | solution.py:541
  99.5 12.1 %all-to-all-done.1 = bf16[128,24,256]{2,1,0:T(8,128)(2,1)S(1)} async-done(((bf16[128,24,256]{2,1,0:T(8,128)(2,1)}), bf16[128,24,256]{2,1,0:T(8,128)(2,1)S(1)}, u32[]{:S(2)}, u32[]{:S(2)}) %all-to-all-start.1) | async-done | bytes 1572896 | tf_op jit(solution)/shard_map/all_to_all | solution.py:581
  111.6 2.8 %final.1 = bf16[48,512]{1,0:T(8,128)(2,1)} custom-call(bf16[288,3072]{1,0:T(8,128)(2,1)} %get-tuple-element.27.picks_h, bf16[3072,256]{1,0:T(8,128)(2,1)S(1)} %bitcast.19, bf16[48,512]{1,0:T(8,128)(2,1)} %get-tuple-element.29.own_h, f32[48,128]{1,0:T(8,128)} %get-tuple-element.30.weight_h, f32[48,2]{1,0:T(8,128)} %copy.28.route_h), custom_call_target="tpu_custom_call" | custom-call | tf_op jit(solution)/shard_map/final/pallas_call | solution.py:599
Async XLA Ops:
  1.8 49.8 %copy-start = (bf16[192,2048]{1,0:T(8,128)(2,1)}, bf16[192,2048]{1,0:T(8,128)(2,1)S(1)}, u32[]{:S(2)}) copy-start(bf16[192,2048]{1,0:T(8,128)(2,1)S(1)} %pad_maximum_fusion.rest_0_) | copy-start | bytes 2359300
  1.8 20.2 %collective-permute-start.3 = (bf16[192,2048]{1,0:T(8,128)(2,1)S(1)}, bf16[192,2048]{1,0:T(8,128)(2,1)S(1)}, u32[]{:S(2)}, u32[]{:S(2)}) collective-permute-start(bf16[192,2048]{1,0:T(8,128)(2,1)S(1)} %pad_maximum_fusion.rest_0_), channel_id=1, source_target_pairs={{0,1},{1,2},{2,3},{3,0},{4,7},{5,4},{6,5},{7,6},{8,9},{9,10},{10,1... | collective-permute-start | bytes 2359304 | tf_op jit(solution)/shard_map/ppermute | solution.py:511
  3.5 48.7 %collective-permute-start.4 = (bf16[192,2048]{1,0:T(8,128)(2,1)S(1)}, bf16[192,2048]{1,0:T(8,128)(2,1)}, u32[]{:S(2)}, u32[]{:S(2)}) collective-permute-start(bf16[192,2048]{1,0:T(8,128)(2,1)S(1)} %pad_maximum_fusion.rest_0_), channel_id=1, source_target_pairs={{0,3},{1,0},{2,1},{3,2},{4,5},{5,6},{6,7},{7,4},{8,11},{9,8},{10,9... | collective-permute-start | bytes 2359304 | tf_op jit(solution)/shard_map/ppermute | solution.py:512
  22.0 29.9 %copy-start.1 = (bf16[192,2048]{1,0:T(8,128)(2,1)}, bf16[192,2048]{1,0:T(8,128)(2,1)S(1)}, u32[]{:S(2)}) copy-start(bf16[192,2048]{1,0:T(8,128)(2,1)S(1)} %collective-permute-done.3.rest_1_) | copy-start | bytes 2359300
  22.0 30.4 %collective-permute-start.5 = (bf16[192,2048]{1,0:T(8,128)(2,1)S(1)}, bf16[192,2048]{1,0:T(8,128)(2,1)}, u32[]{:S(2)}, u32[]{:S(2)}) collective-permute-start(bf16[192,2048]{1,0:T(8,128)(2,1)S(1)} %collective-permute-done.3.rest_1_), channel_id=1, source_target_pairs={{0,1},{1,2},{2,3},{3,0},{4,7},{5,4},{6,5},{7,6},{8,9},{9,10},{10,1... | collective-permute-start | bytes 2359304 | tf_op jit(solution)/shard_map/ppermute | solution.py:513
  31.5 5.1 %collective-permute-start = (bf16[48,256]{1,0:T(8,128)(2,1)S(1)}, bf16[48,256]{1,0:T(8,128)(2,1)S(1)}, u32[]{:S(2)}, u32[]{:S(2)}) collective-permute-start(bf16[48,256]{1,0:T(8,128)(2,1)S(1)} %get-tuple-element.21.heads), channel_id=1, source_target_pairs={{0,1},{1,2},{2,3},{3,0},{4,5},{5,6},{6,7},{7,4},{8,9},{9,10},{10,1... | collective-permute-start | bytes 73736 | tf_op jit(solution)/shard_map/ppermute | solution.py:506
  32.4 4.3 %collective-permute-start.1 = (bf16[48,256]{1,0:T(8,128)(2,1)S(1)}, bf16[48,256]{1,0:T(8,128)(2,1)S(1)}, u32[]{:S(2)}, u32[]{:S(2)}) collective-permute-start(bf16[48,256]{1,0:T(8,128)(2,1)S(1)} %get-tuple-element.21.heads), channel_id=1, source_target_pairs={{0,3},{1,0},{2,1},{3,2},{4,7},{5,4},{6,5},{7,6},{8,11},{9,8},{10,9... | collective-permute-start | bytes 73736 | tf_op jit(solution)/shard_map/ppermute | solution.py:507
  34.8 5.3 %collective-permute-start.2 = (bf16[48,256]{1,0:T(8,128)(2,1)S(1)}, bf16[48,256]{1,0:T(8,128)(2,1)S(1)}, u32[]{:S(2)}, u32[]{:S(2)}) collective-permute-start(bf16[48,256]{1,0:T(8,128)(2,1)S(1)} %get-tuple-element.21.heads), channel_id=1, source_target_pairs={{0,2},{1,3},{2,0},{3,1},{4,6},{5,7},{6,4},{7,5},{8,10},{9,11},{10,... | collective-permute-start | bytes 73736 | tf_op jit(solution)/shard_map/ppermute | solution.py:508
  43.2 32.3 %all-to-all-start = ((bf16[32,24,1024]{2,1,0:T(8,128)(2,1)}), bf16[32,24,1024]{2,1,0:T(8,128)(2,1)S(1)}, u32[]{:S(2)}, u32[]{:S(2)}) async-start(bf16[32,24,1024]{2,1,0:T(8,128)(2,1)} %bitcast.23), calls=%async_computation | async-start | bytes 3145728 | tf_op jit(solution)/shard_map/all_to_all | solution.py:536
  51.6 2.5 %collective-permute-start.6 = (bf16[192,2048]{1,0:T(8,128)(2,1)S(1)}, bf16[192,2048]{1,0:T(8,128)(2,1)}, u32[]{:S(2)}, u32[]{:S(2)}) collective-permute-start(bf16[192,2048]{1,0:T(8,128)(2,1)S(1)} %pad_maximum_fusion.rest_0_), channel_id=1, source_target_pairs={{0,4},{4,0},{1,5},{5,1},{2,6},{6,2},{3,7},{7,3},{8,12},{12,8},{9,1... | collective-permute-start | bytes 2359304 | tf_op jit(solution)/shard_map/ppermute | solution.py:515
  51.9 23.5 %collective-permute-start.7 = (bf16[192,2048]{1,0:T(8,128)(2,1)S(1)}, bf16[192,2048]{1,0:T(8,128)(2,1)}, u32[]{:S(2)}, u32[]{:S(2)}) collective-permute-start(bf16[192,2048]{1,0:T(8,128)(2,1)S(1)} %collective-permute-done.3.rest_1_), channel_id=1, source_target_pairs={{0,4},{4,0},{1,5},{5,1},{2,6},{6,2},{3,7},{7,3},{8,12},{12,8},{9,1... | collective-permute-start | bytes 2359304 | tf_op jit(solution)/shard_map/ppermute | solution.py:515
  52.2 23.3 %collective-permute-start.8 = (bf16[192,2048]{1,0:T(8,128)(2,1)}, bf16[192,2048]{1,0:T(8,128)(2,1)}, u32[]{:S(2)}, u32[]{:S(2)}) collective-permute-start(bf16[192,2048]{1,0:T(8,128)(2,1)} %collective-permute-done.4.rest_2_), channel_id=1, source_target_pairs={{0,4},{4,0},{1,5},{5,1},{2,6},{6,2},{3,7},{7,3},{8,12},{12,8},{9,1... | collective-permute-start | bytes 2359304 | tf_op jit(solution)/shard_map/ppermute | solution.py:515
  52.5 23.0 %collective-permute-start.9 = (bf16[192,2048]{1,0:T(8,128)(2,1)}, bf16[192,2048]{1,0:T(8,128)(2,1)}, u32[]{:S(2)}, u32[]{:S(2)}) collective-permute-start(bf16[192,2048]{1,0:T(8,128)(2,1)} %collective-permute-done.5.rest_3_), channel_id=1, source_target_pairs={{0,4},{4,0},{1,5},{5,1},{2,6},{6,2},{3,7},{7,3},{8,12},{12,8},{9,1... | collective-permute-start | bytes 2359304 | tf_op jit(solution)/shard_map/ppermute | solution.py:515
  82.5 4.7 %copy-start.2 = (bf16[2048]{0:T(1024)(128)(2,1)S(1)}, bf16[2048]{0:T(1024)(128)(2,1)}, u32[]{:S(2)}) copy-start(bf16[2048]{0:T(1024)(128)(2,1)} %param.44) | copy-start | bytes 12292
  82.5 5.3 %copy-start.3 = (f32[48,2]{0,1:T(2,128)S(1)}, f32[48,2]{0,1:T(2,128)}, u32[]{:S(2)}) copy-start(f32[48,2]{0,1:T(2,128)} %param.40) | copy-start | bytes 1156
  82.5 29.1 %all-to-all-start.1 = ((bf16[128,24,256]{2,1,0:T(8,128)(2,1)}), bf16[128,24,256]{2,1,0:T(8,128)(2,1)S(1)}, u32[]{:S(2)}, u32[]{:S(2)}) async-start(bf16[128,24,256]{2,1,0:T(8,128)(2,1)} %bitcast.22), calls=%async_computation.1 | async-start | bytes 3145728 | tf_op jit(solution)/shard_map/all_to_all | solution.py:581

commit v4 on v3

--- a/solution.py
+++ b/solution.py
@@ -134,7 +134,7 @@
         for j in range(chunks)
     ]
     later = pltpu.make_async_copy(w_mix_h, w_mix, wsem.at[4])
-    for copy in (loads[0], *parts, *loads[1:], later):
+    for copy in (*loads[:3], *parts, loads[3], later):
         copy.start()
     small[8].wait()
     route_tables(place[0], ids, select_o, slots)
@@ -150,23 +150,21 @@
     high = queries.astype(BF).astype(F32)
     gap = jnp.zeros((64 - rows, head_count * hd), F32)
     stacked = jnp.concatenate([high, gap, queries - high, gap], axis=0)
-    turned = jnp.concatenate(
-        [stacked[:, h * hd : (h + 1) * hd].T for h in range(head_count)], axis=0
-    ).astype(BF)
+    turned = stacked[:, hd:].T.astype(BF)
+    plain = padded_transpose(queries[:, :hd])
 
     def read_out(j):
         parts[j].wait()
         for b in range(j * per, (j + 1) * per, 2):
             spread = jnp.dot(turned, hot[:, b * hd : (b + 2) * hd], preferred_element_type=F32)
             for k in range(2):
-                for h in range(head_count):
-                    num[h, b + k : b + k + 1] = jnp.sum(
-                        spread[h * hd : (h + 1) * hd, k * hd : (k + 1) * hd] * cbuf[b + k, h],
-                        axis=0,
-                        keepdims=True,
-                    )
-
-    read_out(0)
+                num[1, b + k : b + k + 1] = jnp.sum(
+                    spread[:, k * hd : (k + 1) * hd] * cbuf[b + k, 1], axis=0, keepdims=True
+                )
+                num[0, b + k : b + k + 1] = jnp.sum(
+                    plain[:, b + k : b + k + 1] * cbuf[b + k, 0], axis=0, keepdims=True
+                )
+
     in_row = nt_dot(w_in[...], normed)
     fg_row = nt_dot(w_fg[...], normed)
     factors = []
@@ -187,9 +185,6 @@
         preferred_element_type=F32,
         precision=lax.Precision.HIGHEST,
     )
-
-    for j in range(1, chunks):
-        read_out(j)
 
     def project(i):
         loads[i].wait()
@@ -220,6 +215,8 @@
         ],
         osem,
     )
+    for j in range(chunks):
+        read_out(j)
     opened = jax.nn.sigmoid(project(3))
     for h in range(head_count):
         cols = slice(h * hd, (h + 1) * hd)
@@ -371,12 +368,20 @@
 def final_kernel(
     picks_h, returned, own_h, weight_h, route_h, out, picks, own, weight, route_w, sems
 ):
+    lanes = picks.shape[1] // 3
+    thirds = [pl.ds(k * lanes, lanes) for k in range(3)]
     loads = start_all(
-        [(own_h, own), (weight_h, weight), (route_h, route_w), (picks_h, picks)], sems
-    )
-    for copy in loads:
+        [(picks_h.at[:, at], picks.at[:, at]) for at in thirds]
+        + [(own_h, own), (weight_h, weight), (route_h, route_w)],
+        sems,
+    )
+    sums = None
+    for k, at in enumerate(thirds):
+        loads[k].wait()
+        part = jnp.dot(picks[:, at], returned[at], preferred_element_type=F32)
+        sums = part if sums is None else sums + part
+    for copy in loads[3:]:
         copy.wait()
-    sums = jnp.dot(picks[...], returned[...], preferred_element_type=F32)
     seqs, quarter = own.shape[0], returned.shape[1]
     for h in range(2):
         dense, first, second = (
@@ -606,7 +611,7 @@
             pltpu.VMEM((seqs, cols), BF),
             pltpu.VMEM((seqs, 128), F32),
             pltpu.VMEM(route_weights.shape, F32),
-            pltpu.SemaphoreType.DMA((4,)),
+            pltpu.SemaphoreType.DMA((6,)),
         ],
         compiler_params=params(40),
         name="final",

time: 116 us -> 115 us (level)
  transfers between devices with their start and end apart: 12 -> 12, of which waited for: 6 -> 6; matrix products, arithmetic and copies ran while one was open for 1% -> 1% of each run, Pallas kernels for 19% -> 18%
where the time goes in v4:
time: 115 us; the launch traced here: 114 us
  waiting for transfers between devices  56.1 us (49%)
  Pallas kernels  31 us (27%)
  starting transfers between devices  23.5 us (20%)
  local copies, waits for them, and re-layouts  1.31 us (1%)
  other arithmetic  1.16 us (1%)
    all_to_all x1, waiting for transfers between devices, local(): lax.all_to_all(send.reshape(ep_count, chunk_rows, half), EP, split_axis=0...  21.4 us
    ppermute x1, waiting for transfers between devices, local(): pack_1 = lax.ppermute(pack, ('c', 'x'), out_way)  16.9 us
    all_to_all x1, waiting for transfers between devices, local(): lax.all_to_all(back.reshape(sources, chunk_rows, quarter), ALL, split_axi...  12.1 us
    all_to_all x1, starting transfers between devices, local(): lax.all_to_all(send.reshape(ep_count, chunk_rows, half), EP, split_axis=0...  8.36 us
    pallas_call x1, Pallas kernels, local(): pl.pallas_call(update_kernel, grid=(pair_rows // pairs,), in_specs=[flat,...  8.25 us
    pallas_call x1, Pallas kernels, local(): pl.pallas_call(ffn_kernel, in_specs=[VMEM] + [ANY] * 11, out_specs=ANY, o...  7.01 us
    pallas_call x1, Pallas kernels, local(): pl.pallas_call(front_kernel, in_specs=[SMEM] + [ANY] * 16, out_specs=[VME...  6.92 us
    all_to_all x1, starting transfers between devices, local(): lax.all_to_all(back.reshape(sources, chunk_rows, quarter), ALL, split_axi...  4.66 us
  transfers between devices with their start and end apart: 12, of which 6 were waited for; matrix products, arithmetic and copies ran while one was open for 1% of the time, Pallas kernels for 18%

profile of v4, /device:TPU:0, one launch (start us, length us, event | category | flops | bytes accessed | tf_op | source)
XLA Modules:
  0.0 113.9 jit_solution(11373248322543842331)
XLA Ops:
  0.6 1.2 %pad_maximum_fusion.rest_0_ = bf16[192,2048]{1,0:T(8,128)(2,1)S(1)} fusion(bf16[64,2048]{1,0:T(8,128)(2,1)} %param.47, bf16[64,2048]{1,0:T(8,128)(2,1)} %bitcast.24, bf16[64,2048]{1,0:T(8,128)(2,1)} %bitcast.25), kind=kLoop, calls=%fused_computation | loop fusion | flops 2359296 | bytes 1572864 | tf_op jit(solution)/shard_map/concatenate | solution.py:442
  1.8 0.0 copy-start
  1.8 1.7 %collective-permute-start.3 = (bf16[192,2048]{1,0:T(8,128)(2,1)S(1)}, bf16[192,2048]{1,0:T(8,128)(2,1)S(1)}, u32[]{:S(2)}, u32[]{:S(2)}) collective-permute-start(bf16[192,2048]{1,0:T(8,128)(2,1)S(1)} %pad_maximum_fusion.rest_0_), channel_id=1, source_target_pairs={{0,1},{1,2},{2,3},{3,0},{4,7},{5,4},{6,5},{7,6},{8,9},{9,10},{10,1... | collective-permute-start | bytes 2359304 | tf_op jit(solution)/shard_map/ppermute | solution.py:516
  3.5 1.6 %collective-permute-start.4 = (bf16[192,2048]{1,0:T(8,128)(2,1)S(1)}, bf16[192,2048]{1,0:T(8,128)(2,1)}, u32[]{:S(2)}, u32[]{:S(2)}) collective-permute-start(bf16[192,2048]{1,0:T(8,128)(2,1)S(1)} %pad_maximum_fusion.rest_0_), channel_id=1, source_target_pairs={{0,3},{1,0},{2,1},{3,2},{4,5},{5,6},{6,7},{7,4},{8,11},{9,8},{10,9... | collective-permute-start | bytes 2359304 | tf_op jit(solution)/shard_map/ppermute | solution.py:517
  5.1 16.9 %collective-permute-done.3.rest_1_ = bf16[192,2048]{1,0:T(8,128)(2,1)S(1)} collective-permute-done((bf16[192,2048]{1,0:T(8,128)(2,1)S(1)}, bf16[192,2048]{1,0:T(8,128)(2,1)S(1)}, u32[]{:S(2)}, u32[]{:S(2)}) %collective-permute-start.3) | collective-permute-done | bytes 786464 | tf_op jit(solution)/shard_map/ppermute | solution.py:516
  22.0 0.0 copy-start.1
  22.0 1.7 %collective-permute-start.5 = (bf16[192,2048]{1,0:T(8,128)(2,1)S(1)}, bf16[192,2048]{1,0:T(8,128)(2,1)}, u32[]{:S(2)}, u32[]{:S(2)}) collective-permute-start(bf16[192,2048]{1,0:T(8,128)(2,1)S(1)} %collective-permute-done.3.rest_1_), channel_id=1, source_target_pairs={{0,1},{1,2},{2,3},{3,0},{4,7},{5,4},{6,5},{7,6},{8,9},{9,10},{10,1... | collective-permute-start | bytes 2359304 | tf_op jit(solution)/shard_map/ppermute | solution.py:518
  23.8 6.9 %front.1 = (bf16[48,256]{1,0:T(8,128)(2,1)S(1)}, f32[96,128]{1,0:T(8,128)}, f32[96,128]{1,0:T(8,128)}, f32[96,128]{1,0:T(8,128)}, f32[96,128]{1,0:T(8,128)}, /*i...) custom-call(s32[1]{0:T(128)} %bitcast.place, ...), custom_call_target="tpu_custom_call" | custom-call | flops 201326592 | bytes 10485760 | tf_op jit(solution)/shard_map/front/pallas_call | solution.py:447
  30.7 0.8 collective-permute-start
  31.5 2.5 %collective-permute-start.1 = (bf16[48,256]{1,0:T(8,128)(2,1)S(1)}, bf16[48,256]{1,0:T(8,128)(2,1)S(1)}, u32[]{:S(2)}, u32[]{:S(2)}) collective-permute-start(bf16[48,256]{1,0:T(8,128)(2,1)S(1)} %get-tuple-element.21.heads), channel_id=1, source_target_pairs={{0,3},{1,0},{2,1},{3,2},{4,7},{5,4},{6,5},{7,6},{8,11},{9,8},{10,9... | collective-permute-start | bytes 73736 | tf_op jit(solution)/shard_map/ppermute | solution.py:512
  34.0 1.1 collective-permute-start.2
  35.1 0.7 collective-permute-done.heads_l
  35.8 0.0 collective-permute-done.1.heads_r
  35.8 3.5 %collective-permute-done.2.heads_f = bf16[48,256]{1,0:T(8,128)(2,1)S(1)} collective-permute-done((bf16[48,256]{1,0:T(8,128)(2,1)S(1)}, bf16[48,256]{1,0:T(8,128)(2,1)S(1)}, u32[]{:S(2)}, u32[]{:S(2)}) %collective-permute-start.2) | collective-permute-done | bytes 24608 | tf_op jit(solution)/shard_map/ppermute | solution.py:513
  39.3 3.0 %mix.1 = (bf16[768,1024]{1,0:T(8,128)(2,1)}, bf16[48,512]{1,0:T(8,128)(2,1)}, bf16[48,2048]{1,0:T(8,128)(2,1)}) custom-call(s32[1]{0:T(128)} %bitcast.place, bf16[48,256]{1,0:T(8,128)(2,1)S(1)} %get-tuple-element.21.heads, bf16[48,256]{1,0:T(8,128)(2,1)S(1)} %collective-permute-done.heads_l, bf16[48,256]{1,0:T(8,128)(2,1)S(1)} %collective-permute-done.1.heads_r, ...), custom_call_target="tpu_custom_call" | custom-call | flops 201326592 | bytes 4194304 | tf_op jit(solution)/shard_map/mix/pallas_call | solution.py:522
  42.4 8.4 %all-to-all-start = ((bf16[32,24,1024]{2,1,0:T(8,128)(2,1)}), bf16[32,24,1024]{2,1,0:T(8,128)(2,1)S(1)}, u32[]{:S(2)}, u32[]{:S(2)}) async-start(bf16[32,24,1024]{2,1,0:T(8,128)(2,1)} %bitcast.23), calls=%async_computation | async-start | bytes 3145728 | tf_op jit(solution)/shard_map/all_to_all | solution.py:541
  50.7 0.0 copy-done
  50.8 0.4 collective-permute-start.6
  51.1 0.0 copy-done.1
  51.1 0.2 collective-permute-start.7
  51.3 0.0 collective-permute-done.4.rest_2_
  51.3 0.3 collective-permute-start.8
  51.6 0.0 collective-permute-done.5.rest_3_
  51.6 0.2 collective-permute-start.9
  51.9 1.4 %collective-permute-done.6.rest_4_ = bf16[192,2048]{1,0:T(8,128)(2,1)} collective-permute-done((bf16[192,2048]{1,0:T(8,128)(2,1)S(1)}, bf16[192,2048]{1,0:T(8,128)(2,1)}, u32[]{:S(2)}, u32[]{:S(2)}) %collective-permute-start.6) | collective-permute-done | bytes 786464 | tf_op jit(solution)/shard_map/ppermute | solution.py:520
  53.2 21.4 %all-to-all-done = bf16[32,24,1024]{2,1,0:T(8,128)(2,1)S(1)} async-done(((bf16[32,24,1024]{2,1,0:T(8,128)(2,1)}), bf16[32,24,1024]{2,1,0:T(8,128)(2,1)S(1)}, u32[]{:S(2)}, u32[]{:S(2)}) %all-to-all-start) | async-done | bytes 1572896 | tf_op jit(solution)/shard_map/all_to_all | solution.py:541
  74.7 0.0 collective-permute-done.7.rest_5_
  74.7 0.0 collective-permute-done.8.rest_6_
  74.7 0.0 collective-permute-done.9.rest_7_
  74.7 7.0 %ffn.1 = bf16[32,4,24,256]{3,2,1,0:T(8,128)(2,1)} custom-call(bf16[768,1024]{1,0:T(8,128)(2,1)S(1)} %bitcast.18, bf16[1,2048,256]{2,1,0:T(8,128)(2,1)} %e_gate.1, bf16[1,2048,256]{2,1,0:T(8,128)(2,1)} %e_up.1, bf16[1,256,2048]{2,1,0:T(8,128)(2,1)} %e_down.1, bf16[192,2048]{1,0:T(8,128)(2,1)} %copy-done, bf16[192,2048]{1,0:T(8,128)(2,1)} %copy-done.1, ...), custom_call_target="tpu_custom_call" | custom-call | flops 1811939328 | bytes 9437184 | tf_op jit(solution)/shard_map/ffn/pallas_call | solution.py:558
  81.7 0.0 copy-start.2
  81.7 0.0 copy-start.3
  81.7 4.7 %all-to-all-start.1 = ((bf16[128,24,256]{2,1,0:T(8,128)(2,1)}), bf16[128,24,256]{2,1,0:T(8,128)(2,1)S(1)}, u32[]{:S(2)}, u32[]{:S(2)}) async-start(bf16[128,24,256]{2,1,0:T(8,128)(2,1)} %bitcast.22), calls=%async_computation.1 | async-start | bytes 3145728 | tf_op jit(solution)/shard_map/all_to_all | solution.py:586
  86.4 0.0 copy-done.2
  86.4 0.6 reshape.49.branch
  87.0 0.0 copy-done.3
  87.0 0.7 copy.28.route_h
  87.7 8.3 %update.1 = f32[96,128,128]{2,1,0:T(8,128)} custom-call(f32[96,128]{1,0:T(8,128)} %get-tuple-element.31.carry, f32[96,128]{1,0:T(8,128)} %get-tuple-element.32.written, f32[96,128]{1,0:T(8,128)} %get-tuple-element.33.value, f32[96,128,128]{2,1,0:T(8,128)} %bitcast.20), custom_call_target="tpu_custom_call" | custom-call | flops 4718592 | bytes 12582912 | tf_op jit(solution)/shard_map/update/pallas_call | solution.py:592
  95.9 2.7 %plan.1 = (bf16[288,3072]{1,0:T(8,128)(2,1)}, f32[48,128]{1,0:T(8,128)}) custom-call(s32[48,128]{1,0:T(8,128)} %get-tuple-element.20.slots, bf16[48,2048]{1,0:T(8,128)(2,1)} %get-tuple-element.26.moe_in, bf16[1,2048]{1,0:T(2,128)(2,1)} %reshape.49.branch), custom_call_target="tpu_custom_call" | custom-call | tf_op jit(solution)/shard_map/plan/pallas_call | solution.py:546
  98.6 12.1 %all-to-all-done.1 = bf16[128,24,256]{2,1,0:T(8,128)(2,1)S(1)} async-done(((bf16[128,24,256]{2,1,0:T(8,128)(2,1)}), bf16[128,24,256]{2,1,0:T(8,128)(2,1)S(1)}, u32[]{:S(2)}, u32[]{:S(2)}) %all-to-all-start.1) | async-done | bytes 1572896 | tf_op jit(solution)/shard_map/all_to_all | solution.py:586
  110.8 3.1 %final.1 = bf16[48,512]{1,0:T(8,128)(2,1)} custom-call(bf16[288,3072]{1,0:T(8,128)(2,1)} %get-tuple-element.27.picks_h, bf16[3072,256]{1,0:T(8,128)(2,1)S(1)} %bitcast.19, bf16[48,512]{1,0:T(8,128)(2,1)} %get-tuple-element.29.own_h, f32[48,128]{1,0:T(8,128)} %get-tuple-element.30.weight_h, f32[48,2]{1,0:T(8,128)} %copy.28.route_h), custom_call_target="tpu_custom_call" | custom-call | tf_op jit(solution)/shard_map/final/pallas_call | solution.py:604
Async XLA Ops:
  1.8 48.9 %copy-start = (bf16[192,2048]{1,0:T(8,128)(2,1)}, bf16[192,2048]{1,0:T(8,128)(2,1)S(1)}, u32[]{:S(2)}) copy-start(bf16[192,2048]{1,0:T(8,128)(2,1)S(1)} %pad_maximum_fusion.rest_0_) | copy-start | bytes 2359300
  1.8 20.2 %collective-permute-start.3 = (bf16[192,2048]{1,0:T(8,128)(2,1)S(1)}, bf16[192,2048]{1,0:T(8,128)(2,1)S(1)}, u32[]{:S(2)}, u32[]{:S(2)}) collective-permute-start(bf16[192,2048]{1,0:T(8,128)(2,1)S(1)} %pad_maximum_fusion.rest_0_), channel_id=1, source_target_pairs={{0,1},{1,2},{2,3},{3,0},{4,7},{5,4},{6,5},{7,6},{8,9},{9,10},{10,1... | collective-permute-start | bytes 2359304 | tf_op jit(solution)/shard_map/ppermute | solution.py:516
  3.5 47.9 %collective-permute-start.4 = (bf16[192,2048]{1,0:T(8,128)(2,1)S(1)}, bf16[192,2048]{1,0:T(8,128)(2,1)}, u32[]{:S(2)}, u32[]{:S(2)}) collective-permute-start(bf16[192,2048]{1,0:T(8,128)(2,1)S(1)} %pad_maximum_fusion.rest_0_), channel_id=1, source_target_pairs={{0,3},{1,0},{2,1},{3,2},{4,5},{5,6},{6,7},{7,4},{8,11},{9,8},{10,9... | collective-permute-start | bytes 2359304 | tf_op jit(solution)/shard_map/ppermute | solution.py:517
  22.0 29.1 %copy-start.1 = (bf16[192,2048]{1,0:T(8,128)(2,1)}, bf16[192,2048]{1,0:T(8,128)(2,1)S(1)}, u32[]{:S(2)}) copy-start(bf16[192,2048]{1,0:T(8,128)(2,1)S(1)} %collective-permute-done.3.rest_1_) | copy-start | bytes 2359300
  22.0 29.6 %collective-permute-start.5 = (bf16[192,2048]{1,0:T(8,128)(2,1)S(1)}, bf16[192,2048]{1,0:T(8,128)(2,1)}, u32[]{:S(2)}, u32[]{:S(2)}) collective-permute-start(bf16[192,2048]{1,0:T(8,128)(2,1)S(1)} %collective-permute-done.3.rest_1_), channel_id=1, source_target_pairs={{0,1},{1,2},{2,3},{3,0},{4,7},{5,4},{6,5},{7,6},{8,9},{9,10},{10,1... | collective-permute-start | bytes 2359304 | tf_op jit(solution)/shard_map/ppermute | solution.py:518
  30.7 5.1 %collective-permute-start = (bf16[48,256]{1,0:T(8,128)(2,1)S(1)}, bf16[48,256]{1,0:T(8,128)(2,1)S(1)}, u32[]{:S(2)}, u32[]{:S(2)}) collective-permute-start(bf16[48,256]{1,0:T(8,128)(2,1)S(1)} %get-tuple-element.21.heads), channel_id=1, source_target_pairs={{0,1},{1,2},{2,3},{3,0},{4,5},{5,6},{6,7},{7,4},{8,9},{9,10},{10,1... | collective-permute-start | bytes 73736 | tf_op jit(solution)/shard_map/ppermute | solution.py:511
  31.5 4.3 %collective-permute-start.1 = (bf16[48,256]{1,0:T(8,128)(2,1)S(1)}, bf16[48,256]{1,0:T(8,128)(2,1)S(1)}, u32[]{:S(2)}, u32[]{:S(2)}) collective-permute-start(bf16[48,256]{1,0:T(8,128)(2,1)S(1)} %get-tuple-element.21.heads), channel_id=1, source_target_pairs={{0,3},{1,0},{2,1},{3,2},{4,7},{5,4},{6,5},{7,6},{8,11},{9,8},{10,9... | collective-permute-start | bytes 73736 | tf_op jit(solution)/shard_map/ppermute | solution.py:512
  34.0 5.3 %collective-permute-start.2 = (bf16[48,256]{1,0:T(8,128)(2,1)S(1)}, bf16[48,256]{1,0:T(8,128)(2,1)S(1)}, u32[]{:S(2)}, u32[]{:S(2)}) collective-permute-start(bf16[48,256]{1,0:T(8,128)(2,1)S(1)} %get-tuple-element.21.heads), channel_id=1, source_target_pairs={{0,2},{1,3},{2,0},{3,1},{4,6},{5,7},{6,4},{7,5},{8,10},{9,11},{10,... | collective-permute-start | bytes 73736 | tf_op jit(solution)/shard_map/ppermute | solution.py:513
  42.4 32.3 %all-to-all-start = ((bf16[32,24,1024]{2,1,0:T(8,128)(2,1)}), bf16[32,24,1024]{2,1,0:T(8,128)(2,1)S(1)}, u32[]{:S(2)}, u32[]{:S(2)}) async-start(bf16[32,24,1024]{2,1,0:T(8,128)(2,1)} %bitcast.23), calls=%async_computation | async-start | bytes 3145728 | tf_op jit(solution)/shard_map/all_to_all | solution.py:541
  50.8 2.5 %collective-permute-start.6 = (bf16[192,2048]{1,0:T(8,128)(2,1)S(1)}, bf16[192,2048]{1,0:T(8,128)(2,1)}, u32[]{:S(2)}, u32[]{:S(2)}) collective-permute-start(bf16[192,2048]{1,0:T(8,128)(2,1)S(1)} %pad_maximum_fusion.rest_0_), channel_id=1, source_target_pairs={{0,4},{4,0},{1,5},{5,1},{2,6},{6,2},{3,7},{7,3},{8,12},{12,8},{9,1... | collective-permute-start | bytes 2359304 | tf_op jit(solution)/shard_map/ppermute | solution.py:520
  51.1 23.5 %collective-permute-start.7 = (bf16[192,2048]{1,0:T(8,128)(2,1)S(1)}, bf16[192,2048]{1,0:T(8,128)(2,1)}, u32[]{:S(2)}, u32[]{:S(2)}) collective-permute-start(bf16[192,2048]{1,0:T(8,128)(2,1)S(1)} %collective-permute-done.3.rest_1_), channel_id=1, source_target_pairs={{0,4},{4,0},{1,5},{5,1},{2,6},{6,2},{3,7},{7,3},{8,12},{12,8},{9,1... | collective-permute-start | bytes 2359304 | tf_op jit(solution)/shard_map/ppermute | solution.py:520
  51.3 23.3 %collective-permute-start.8 = (bf16[192,2048]{1,0:T(8,128)(2,1)}, bf16[192,2048]{1,0:T(8,128)(2,1)}, u32[]{:S(2)}, u32[]{:S(2)}) collective-permute-start(bf16[192,2048]{1,0:T(8,128)(2,1)} %collective-permute-done.4.rest_2_), channel_id=1, source_target_pairs={{0,4},{4,0},{1,5},{5,1},{2,6},{6,2},{3,7},{7,3},{8,12},{12,8},{9,1... | collective-permute-start | bytes 2359304 | tf_op jit(solution)/shard_map/ppermute | solution.py:520
  51.6 23.0 %collective-permute-start.9 = (bf16[192,2048]{1,0:T(8,128)(2,1)}, bf16[192,2048]{1,0:T(8,128)(2,1)}, u32[]{:S(2)}, u32[]{:S(2)}) collective-permute-start(bf16[192,2048]{1,0:T(8,128)(2,1)} %collective-permute-done.5.rest_3_), channel_id=1, source_target_pairs={{0,4},{4,0},{1,5},{5,1},{2,6},{6,2},{3,7},{7,3},{8,12},{12,8},{9,1... | collective-permute-start | bytes 2359304 | tf_op jit(solution)/shard_map/ppermute | solution.py:520
  81.7 4.7 %copy-start.2 = (bf16[2048]{0:T(1024)(128)(2,1)S(1)}, bf16[2048]{0:T(1024)(128)(2,1)}, u32[]{:S(2)}) copy-start(bf16[2048]{0:T(1024)(128)(2,1)} %param.44) | copy-start | bytes 12292
  81.7 5.3 %copy-start.3 = (f32[48,2]{0,1:T(2,128)S(1)}, f32[48,2]{0,1:T(2,128)}, u32[]{:S(2)}) copy-start(f32[48,2]{0,1:T(2,128)} %param.40) | copy-start | bytes 1156
  81.7 29.1 %all-to-all-start.1 = ((bf16[128,24,256]{2,1,0:T(8,128)(2,1)}), bf16[128,24,256]{2,1,0:T(8,128)(2,1)S(1)}, u32[]{:S(2)}, u32[]{:S(2)}) async-start(bf16[128,24,256]{2,1,0:T(8,128)(2,1)} %bitcast.22), calls=%async_computation.1 | async-start | bytes 3145728 | tf_op jit(solution)/shard_map/all_to_all | solution.py:586

commit v5 on v4

--- a/solution.py
+++ b/solution.py
@@ -260,8 +260,8 @@
 
 def mix_kernel(
     place, heads, heads_l, heads_r, heads_f, w_mix, tok, gain, select,
-    send_h, own_o, moe_o,
-    send, sems,
+    send_h, own_h, moe_h,
+    send, own_o, moe_o, sems,
 ):
     width = heads.shape[1]
     mixed_proj = None
@@ -274,20 +274,25 @@
     half = send.shape[1]
     gap = jnp.zeros((select.shape[1] // 2 - moe_in.shape[0], half), BF)
     stacked = jnp.concatenate([moe_in[:, :half], gap, moe_in[:, half:], gap], axis=0)
-    chunks = sems.shape[0]
-    lines = send.shape[0] // chunks
-    stores = []
-    for j in range(chunks):
-        at = pl.ds(j * lines, lines)
-        send[at] = jnp.dot(select[at], stacked, preferred_element_type=F32).astype(BF)
-        stores.append(pltpu.make_async_copy(send.at[at], send_h.at[at], sems.at[j]))
-        stores[j].start()
     moe_o[...] = moe_in
     cols = own_o.shape[1]
     own = residual[:, :cols]
     for k in range(1, residual.shape[1] // cols):
         own = jnp.where(place[0] == k, residual[:, k * cols : (k + 1) * cols], own)
     own_o[...] = own
+    chunks = sems.shape[0] - 2
+    lines = send.shape[0] // chunks
+    stores = [
+        pltpu.make_async_copy(own_o, own_h, sems.at[chunks]),
+        pltpu.make_async_copy(moe_o, moe_h, sems.at[chunks + 1]),
+    ]
+    for copy in stores:
+        copy.start()
+    for j in range(chunks):
+        at = pl.ds(j * lines, lines)
+        send[at] = jnp.dot(select[at], stacked, preferred_element_type=F32).astype(BF)
+        stores.append(pltpu.make_async_copy(send.at[at], send_h.at[at], sems.at[j]))
+        stores[-1].start()
     for copy in stores:
         copy.wait()
 
@@ -368,20 +373,12 @@
 def final_kernel(
     picks_h, returned, own_h, weight_h, route_h, out, picks, own, weight, route_w, sems
 ):
-    lanes = picks.shape[1] // 3
-    thirds = [pl.ds(k * lanes, lanes) for k in range(3)]
     loads = start_all(
-        [(picks_h.at[:, at], picks.at[:, at]) for at in thirds]
-        + [(own_h, own), (weight_h, weight), (route_h, route_w)],
-        sems,
-    )
-    sums = None
-    for k, at in enumerate(thirds):
-        loads[k].wait()
-        part = jnp.dot(picks[:, at], returned[at], preferred_element_type=F32)
-        sums = part if sums is None else sums + part
-    for copy in loads[3:]:
+        [(own_h, own), (weight_h, weight), (route_h, route_w), (picks_h, picks)], sems
+    )
+    for copy in loads:
         copy.wait()
+    sums = jnp.dot(picks[...], returned[...], preferred_element_type=F32)
     seqs, quarter = own.shape[0], returned.shape[1]
     for h in range(2):
         dense, first, second = (
@@ -522,13 +519,18 @@
     send, own, moe_in = pl.pallas_call(
         mix_kernel,
         in_specs=[SMEM] + [VMEM] * 8,
-        out_specs=[ANY, VMEM, VMEM],
+        out_specs=[ANY] * 3,
         out_shape=[
             pltpu.HBM((total_rows, half), BF),
             pltpu.HBM((seqs, cols), BF),
             pltpu.HBM((seqs, width), BF),
         ],
-        scratch_shapes=[pltpu.VMEM((total_rows, half), BF), pltpu.SemaphoreType.DMA((4,))],
+        scratch_shapes=[
+            pltpu.VMEM((total_rows, half), BF),
+            pltpu.VMEM((seqs, cols), BF),
+            pltpu.VMEM((seqs, width), BF),
+            pltpu.SemaphoreType.DMA((6,)),
+        ],
         compiler_params=params(30),
         cost_estimate=pl.CostEstimate(
             flops=2 * seqs * width * w_mix_out.shape[0], transcendentals=0, bytes_accessed=w_mix_out.size * 2
@@ -611,7 +613,7 @@
             pltpu.VMEM((seqs, cols), BF),
             pltpu.VMEM((seqs, 128), F32),
             pltpu.VMEM(route_weights.shape, F32),
-            pltpu.SemaphoreType.DMA((6,)),
+            pltpu.SemaphoreType.DMA((4,)),
         ],
         compiler_params=params(40),
         name="final",

time: 115 us -> 114 us (level)
  no operation moved by 1% of the time
where the time goes in v5:
time: 114 us; the launch traced here: 113 us
  waiting for transfers between devices  56.1 us (49%)
  Pallas kernels  30.1 us (26%)
  starting transfers between devices  23.5 us (21%)
  local copies, waits for them, and re-layouts  1.31 us (1%)
  other arithmetic  1.16 us (1%)
    all_to_all x1, waiting for transfers between devices, local(): lax.all_to_all(send.reshape(ep_count, chunk_rows, half), EP, split_axis=0...  21.4 us
    ppermute x1, waiting for transfers between devices, local(): pack_1 = lax.ppermute(pack, ('c', 'x'), out_way)  16.9 us
    all_to_all x1, waiting for transfers between devices, local(): lax.all_to_all(back.reshape(sources, chunk_rows, quarter), ALL, split_axi...  12.1 us
    all_to_all x1, starting transfers between devices, local(): lax.all_to_all(send.reshape(ep_count, chunk_rows, half), EP, split_axis=0...  8.36 us
    pallas_call x1, Pallas kernels, local(): pl.pallas_call(update_kernel, grid=(pair_rows // pairs,), in_specs=[flat,...  8.25 us
    pallas_call x1, Pallas kernels, local(): pl.pallas_call(ffn_kernel, in_specs=[VMEM] + [ANY] * 11, out_specs=ANY, o...  7.01 us
    pallas_call x1, Pallas kernels, local(): pl.pallas_call(front_kernel, in_specs=[SMEM] + [ANY] * 16, out_specs=[VME...  6.92 us
    all_to_all x1, starting transfers between devices, local(): lax.all_to_all(back.reshape(sources, chunk_rows, quarter), ALL, split_axi...  4.66 us
  transfers between devices with their start and end apart: 12, of which 6 were waited for; matrix products, arithmetic and copies ran while one was open for 1% of the time, Pallas kernels for 18%

profile of v5, /device:TPU:0, one launch (start us, length us, event | category | flops | bytes accessed | tf_op | source)
XLA Modules:
  0.0 112.9 jit_solution(16788319561011985031)
XLA Ops:
  0.6 1.2 %pad_maximum_fusion.rest_0_ = bf16[192,2048]{1,0:T(8,128)(2,1)S(1)} fusion(bf16[64,2048]{1,0:T(8,128)(2,1)} %param.47, bf16[64,2048]{1,0:T(8,128)(2,1)} %bitcast.24, bf16[64,2048]{1,0:T(8,128)(2,1)} %bitcast.25), kind=kLoop, calls=%fused_computation | loop fusion | flops 2359296 | bytes 1572864 | tf_op jit(solution)/shard_map/concatenate | solution.py:439
  1.8 0.0 copy-start
  1.8 1.7 %collective-permute-start.3 = (bf16[192,2048]{1,0:T(8,128)(2,1)S(1)}, bf16[192,2048]{1,0:T(8,128)(2,1)S(1)}, u32[]{:S(2)}, u32[]{:S(2)}) collective-permute-start(bf16[192,2048]{1,0:T(8,128)(2,1)S(1)} %pad_maximum_fusion.rest_0_), channel_id=1, source_target_pairs={{0,1},{1,2},{2,3},{3,0},{4,7},{5,4},{6,5},{7,6},{8,9},{9,10},{10,1... | collective-permute-start | bytes 2359304 | tf_op jit(solution)/shard_map/ppermute | solution.py:513
  3.5 1.6 %collective-permute-start.4 = (bf16[192,2048]{1,0:T(8,128)(2,1)S(1)}, bf16[192,2048]{1,0:T(8,128)(2,1)}, u32[]{:S(2)}, u32[]{:S(2)}) collective-permute-start(bf16[192,2048]{1,0:T(8,128)(2,1)S(1)} %pad_maximum_fusion.rest_0_), channel_id=1, source_target_pairs={{0,3},{1,0},{2,1},{3,2},{4,5},{5,6},{6,7},{7,4},{8,11},{9,8},{10,9... | collective-permute-start | bytes 2359304 | tf_op jit(solution)/shard_map/ppermute | solution.py:514
  5.1 16.9 %collective-permute-done.3.rest_1_ = bf16[192,2048]{1,0:T(8,128)(2,1)S(1)} collective-permute-done((bf16[192,2048]{1,0:T(8,128)(2,1)S(1)}, bf16[192,2048]{1,0:T(8,128)(2,1)S(1)}, u32[]{:S(2)}, u32[]{:S(2)}) %collective-permute-start.3) | collective-permute-done | bytes 786464 | tf_op jit(solution)/shard_map/ppermute | solution.py:513
  22.0 0.0 copy-start.1
  22.0 1.7 %collective-permute-start.5 = (bf16[192,2048]{1,0:T(8,128)(2,1)S(1)}, bf16[192,2048]{1,0:T(8,128)(2,1)}, u32[]{:S(2)}, u32[]{:S(2)}) collective-permute-start(bf16[192,2048]{1,0:T(8,128)(2,1)S(1)} %collective-permute-done.3.rest_1_), channel_id=1, source_target_pairs={{0,1},{1,2},{2,3},{3,0},{4,7},{5,4},{6,5},{7,6},{8,9},{9,10},{10,1... | collective-permute-start | bytes 2359304 | tf_op jit(solution)/shard_map/ppermute | solution.py:515
  23.8 6.9 %front.1 = (bf16[48,256]{1,0:T(8,128)(2,1)S(1)}, f32[96,128]{1,0:T(8,128)}, f32[96,128]{1,0:T(8,128)}, f32[96,128]{1,0:T(8,128)}, f32[96,128]{1,0:T(8,128)}, /*i...) custom-call(s32[1]{0:T(128)} %bitcast.place, ...), custom_call_target="tpu_custom_call" | custom-call | flops 201326592 | bytes 10485760 | tf_op jit(solution)/shard_map/front/pallas_call | solution.py:444
  30.7 0.8 collective-permute-start
  31.5 2.5 %collective-permute-start.1 = (bf16[48,256]{1,0:T(8,128)(2,1)S(1)}, bf16[48,256]{1,0:T(8,128)(2,1)S(1)}, u32[]{:S(2)}, u32[]{:S(2)}) collective-permute-start(bf16[48,256]{1,0:T(8,128)(2,1)S(1)} %get-tuple-element.21.heads), channel_id=1, source_target_pairs={{0,3},{1,0},{2,1},{3,2},{4,7},{5,4},{6,5},{7,6},{8,11},{9,8},{10,9... | collective-permute-start | bytes 73736 | tf_op jit(solution)/shard_map/ppermute | solution.py:509
  34.0 1.1 collective-permute-start.2
  35.1 0.7 collective-permute-done.heads_l
  35.8 0.0 collective-permute-done.1.heads_r
  35.8 3.5 %collective-permute-done.2.heads_f = bf16[48,256]{1,0:T(8,128)(2,1)S(1)} collective-permute-done((bf16[48,256]{1,0:T(8,128)(2,1)S(1)}, bf16[48,256]{1,0:T(8,128)(2,1)S(1)}, u32[]{:S(2)}, u32[]{:S(2)}) %collective-permute-start.2) | collective-permute-done | bytes 24608 | tf_op jit(solution)/shard_map/ppermute | solution.py:510
  39.3 2.4 %mix.1 = (bf16[768,1024]{1,0:T(8,128)(2,1)}, bf16[48,512]{1,0:T(8,128)(2,1)}, bf16[48,2048]{1,0:T(8,128)(2,1)}) custom-call(s32[1]{0:T(128)} %bitcast.place, bf16[48,256]{1,0:T(8,128)(2,1)S(1)} %get-tuple-element.21.heads, bf16[48,256]{1,0:T(8,128)(2,1)S(1)} %collective-permute-done.heads_l, bf16[48,256]{1,0:T(8,128)(2,1)S(1)} %collective-permute-done.1.heads_r, ...), custom_call_target="tpu_custom_call" | custom-call | flops 201326592 | bytes 4194304 | tf_op jit(solution)/shard_map/mix/pallas_call | solution.py:519
  41.7 8.4 %all-to-all-start = ((bf16[32,24,1024]{2,1,0:T(8,128)(2,1)}), bf16[32,24,1024]{2,1,0:T(8,128)(2,1)S(1)}, u32[]{:S(2)}, u32[]{:S(2)}) async-start(bf16[32,24,1024]{2,1,0:T(8,128)(2,1)} %bitcast.23), calls=%async_computation | async-start | bytes 3145728 | tf_op jit(solution)/shard_map/all_to_all | solution.py:543
  50.1 0.0 copy-done
  50.1 0.4 collective-permute-start.6
  50.4 0.0 copy-done.1
  50.4 0.2 collective-permute-start.7
  50.7 0.0 collective-permute-done.4.rest_2_
  50.7 0.3 collective-permute-start.8
  51.0 0.0 collective-permute-done.5.rest_3_
  51.0 0.2 collective-permute-start.9
  51.2 1.4 %collective-permute-done.6.rest_4_ = bf16[192,2048]{1,0:T(8,128)(2,1)} collective-permute-done((bf16[192,2048]{1,0:T(8,128)(2,1)S(1)}, bf16[192,2048]{1,0:T(8,128)(2,1)}, u32[]{:S(2)}, u32[]{:S(2)}) %collective-permute-start.6) | collective-permute-done | bytes 786464 | tf_op jit(solution)/shard_map/ppermute | solution.py:517
  52.6 21.4 %all-to-all-done = bf16[32,24,1024]{2,1,0:T(8,128)(2,1)S(1)} async-done(((bf16[32,24,1024]{2,1,0:T(8,128)(2,1)}), bf16[32,24,1024]{2,1,0:T(8,128)(2,1)S(1)}, u32[]{:S(2)}, u32[]{:S(2)}) %all-to-all-start) | async-done | bytes 1572896 | tf_op jit(solution)/shard_map/all_to_all | solution.py:543
  74.0 0.0 collective-permute-done.7.rest_5_
  74.0 0.0 collective-permute-done.8.rest_6_
  74.0 0.0 collective-permute-done.9.rest_7_
  74.0 7.0 %ffn.1 = bf16[32,4,24,256]{3,2,1,0:T(8,128)(2,1)} custom-call(bf16[768,1024]{1,0:T(8,128)(2,1)S(1)} %bitcast.18, bf16[1,2048,256]{2,1,0:T(8,128)(2,1)} %e_gate.1, bf16[1,2048,256]{2,1,0:T(8,128)(2,1)} %e_up.1, bf16[1,256,2048]{2,1,0:T(8,128)(2,1)} %e_down.1, bf16[192,2048]{1,0:T(8,128)(2,1)} %copy-done, bf16[192,2048]{1,0:T(8,128)(2,1)} %copy-done.1, ...), custom_call_target="tpu_custom_call" | custom-call | flops 1811939328 | bytes 9437184 | tf_op jit(solution)/shard_map/ffn/pallas_call | solution.py:560
  81.0 0.0 copy-start.2
  81.0 0.0 copy-start.3
  81.0 4.7 %all-to-all-start.1 = ((bf16[128,24,256]{2,1,0:T(8,128)(2,1)}), bf16[128,24,256]{2,1,0:T(8,128)(2,1)S(1)}, u32[]{:S(2)}, u32[]{:S(2)}) async-start(bf16[128,24,256]{2,1,0:T(8,128)(2,1)} %bitcast.22), calls=%async_computation.1 | async-start | bytes 3145728 | tf_op jit(solution)/shard_map/all_to_all | solution.py:588
  85.7 0.0 copy-done.2
  85.7 0.6 reshape.49.branch
  86.3 0.0 copy-done.3
  86.3 0.7 copy.28.route_h
  87.0 8.3 %update.1 = f32[96,128,128]{2,1,0:T(8,128)} custom-call(f32[96,128]{1,0:T(8,128)} %get-tuple-element.31.carry, f32[96,128]{1,0:T(8,128)} %get-tuple-element.32.written, f32[96,128]{1,0:T(8,128)} %get-tuple-element.33.value, f32[96,128,128]{2,1,0:T(8,128)} %bitcast.20), custom_call_target="tpu_custom_call" | custom-call | flops 4718592 | bytes 12582912 | tf_op jit(solution)/shard_map/update/pallas_call | solution.py:594
  95.3 2.7 %plan.1 = (bf16[288,3072]{1,0:T(8,128)(2,1)}, f32[48,128]{1,0:T(8,128)}) custom-call(s32[48,128]{1,0:T(8,128)} %get-tuple-element.20.slots, bf16[48,2048]{1,0:T(8,128)(2,1)} %get-tuple-element.26.moe_in, bf16[1,2048]{1,0:T(2,128)(2,1)} %reshape.49.branch), custom_call_target="tpu_custom_call" | custom-call | tf_op jit(solution)/shard_map/plan/pallas_call | solution.py:548
  98.0 12.1 %all-to-all-done.1 = bf16[128,24,256]{2,1,0:T(8,128)(2,1)S(1)} async-done(((bf16[128,24,256]{2,1,0:T(8,128)(2,1)}), bf16[128,24,256]{2,1,0:T(8,128)(2,1)S(1)}, u32[]{:S(2)}, u32[]{:S(2)}) %all-to-all-start.1) | async-done | bytes 1572896 | tf_op jit(solution)/shard_map/all_to_all | solution.py:588
  110.1 2.8 %final.1 = bf16[48,512]{1,0:T(8,128)(2,1)} custom-call(bf16[288,3072]{1,0:T(8,128)(2,1)} %get-tuple-element.27.picks_h, bf16[3072,256]{1,0:T(8,128)(2,1)S(1)} %bitcast.19, bf16[48,512]{1,0:T(8,128)(2,1)} %get-tuple-element.29.own_h, f32[48,128]{1,0:T(8,128)} %get-tuple-element.30.weight_h, f32[48,2]{1,0:T(8,128)} %copy.28.route_h), custom_call_target="tpu_custom_call" | custom-call | tf_op jit(solution)/shard_map/final/pallas_call | solution.py:606
Async XLA Ops:
  1.8 48.3 %copy-start = (bf16[192,2048]{1,0:T(8,128)(2,1)}, bf16[192,2048]{1,0:T(8,128)(2,1)S(1)}, u32[]{:S(2)}) copy-start(bf16[192,2048]{1,0:T(8,128)(2,1)S(1)} %pad_maximum_fusion.rest_0_) | copy-start | bytes 2359300
  1.8 20.2 %collective-permute-start.3 = (bf16[192,2048]{1,0:T(8,128)(2,1)S(1)}, bf16[192,2048]{1,0:T(8,128)(2,1)S(1)}, u32[]{:S(2)}, u32[]{:S(2)}) collective-permute-start(bf16[192,2048]{1,0:T(8,128)(2,1)S(1)} %pad_maximum_fusion.rest_0_), channel_id=1, source_target_pairs={{0,1},{1,2},{2,3},{3,0},{4,7},{5,4},{6,5},{7,6},{8,9},{9,10},{10,1... | collective-permute-start | bytes 2359304 | tf_op jit(solution)/shard_map/ppermute | solution.py:513
  3.5 47.2 %collective-permute-start.4 = (bf16[192,2048]{1,0:T(8,128)(2,1)S(1)}, bf16[192,2048]{1,0:T(8,128)(2,1)}, u32[]{:S(2)}, u32[]{:S(2)}) collective-permute-start(bf16[192,2048]{1,0:T(8,128)(2,1)S(1)} %pad_maximum_fusion.rest_0_), channel_id=1, source_target_pairs={{0,3},{1,0},{2,1},{3,2},{4,5},{5,6},{6,7},{7,4},{8,11},{9,8},{10,9... | collective-permute-start | bytes 2359304 | tf_op jit(solution)/shard_map/ppermute | solution.py:514
  22.0 28.4 %copy-start.1 = (bf16[192,2048]{1,0:T(8,128)(2,1)}, bf16[192,2048]{1,0:T(8,128)(2,1)S(1)}, u32[]{:S(2)}) copy-start(bf16[192,2048]{1,0:T(8,128)(2,1)S(1)} %collective-permute-done.3.rest_1_) | copy-start | bytes 2359300
  22.0 28.9 %collective-permute-start.5 = (bf16[192,2048]{1,0:T(8,128)(2,1)S(1)}, bf16[192,2048]{1,0:T(8,128)(2,1)}, u32[]{:S(2)}, u32[]{:S(2)}) collective-permute-start(bf16[192,2048]{1,0:T(8,128)(2,1)S(1)} %collective-permute-done.3.rest_1_), channel_id=1, source_target_pairs={{0,1},{1,2},{2,3},{3,0},{4,7},{5,4},{6,5},{7,6},{8,9},{9,10},{10,1... | collective-permute-start | bytes 2359304 | tf_op jit(solution)/shard_map/ppermute | solution.py:515
  30.7 5.1 %collective-permute-start = (bf16[48,256]{1,0:T(8,128)(2,1)S(1)}, bf16[48,256]{1,0:T(8,128)(2,1)S(1)}, u32[]{:S(2)}, u32[]{:S(2)}) collective-permute-start(bf16[48,256]{1,0:T(8,128)(2,1)S(1)} %get-tuple-element.21.heads), channel_id=1, source_target_pairs={{0,1},{1,2},{2,3},{3,0},{4,5},{5,6},{6,7},{7,4},{8,9},{9,10},{10,1... | collective-permute-start | bytes 73736 | tf_op jit(solution)/shard_map/ppermute | solution.py:508
  31.5 4.3 %collective-permute-start.1 = (bf16[48,256]{1,0:T(8,128)(2,1)S(1)}, bf16[48,256]{1,0:T(8,128)(2,1)S(1)}, u32[]{:S(2)}, u32[]{:S(2)}) collective-permute-start(bf16[48,256]{1,0:T(8,128)(2,1)S(1)} %get-tuple-element.21.heads), channel_id=1, source_target_pairs={{0,3},{1,0},{2,1},{3,2},{4,7},{5,4},{6,5},{7,6},{8,11},{9,8},{10,9... | collective-permute-start | bytes 73736 | tf_op jit(solution)/shard_map/ppermute | solution.py:509
  34.0 5.3 %collective-permute-start.2 = (bf16[48,256]{1,0:T(8,128)(2,1)S(1)}, bf16[48,256]{1,0:T(8,128)(2,1)S(1)}, u32[]{:S(2)}, u32[]{:S(2)}) collective-permute-start(bf16[48,256]{1,0:T(8,128)(2,1)S(1)} %get-tuple-element.21.heads), channel_id=1, source_target_pairs={{0,2},{1,3},{2,0},{3,1},{4,6},{5,7},{6,4},{7,5},{8,10},{9,11},{10,... | collective-permute-start | bytes 73736 | tf_op jit(solution)/shard_map/ppermute | solution.py:510
  41.7 32.3 %all-to-all-start = ((bf16[32,24,1024]{2,1,0:T(8,128)(2,1)}), bf16[32,24,1024]{2,1,0:T(8,128)(2,1)S(1)}, u32[]{:S(2)}, u32[]{:S(2)}) async-start(bf16[32,24,1024]{2,1,0:T(8,128)(2,1)} %bitcast.23), calls=%async_computation | async-start | bytes 3145728 | tf_op jit(solution)/shard_map/all_to_all | solution.py:543
  50.1 2.5 %collective-permute-start.6 = (bf16[192,2048]{1,0:T(8,128)(2,1)S(1)}, bf16[192,2048]{1,0:T(8,128)(2,1)}, u32[]{:S(2)}, u32[]{:S(2)}) collective-permute-start(bf16[192,2048]{1,0:T(8,128)(2,1)S(1)} %pad_maximum_fusion.rest_0_), channel_id=1, source_target_pairs={{0,4},{4,0},{1,5},{5,1},{2,6},{6,2},{3,7},{7,3},{8,12},{12,8},{9,1... | collective-permute-start | bytes 2359304 | tf_op jit(solution)/shard_map/ppermute | solution.py:517
  50.4 23.5 %collective-permute-start.7 = (bf16[192,2048]{1,0:T(8,128)(2,1)S(1)}, bf16[192,2048]{1,0:T(8,128)(2,1)}, u32[]{:S(2)}, u32[]{:S(2)}) collective-permute-start(bf16[192,2048]{1,0:T(8,128)(2,1)S(1)} %collective-permute-done.3.rest_1_), channel_id=1, source_target_pairs={{0,4},{4,0},{1,5},{5,1},{2,6},{6,2},{3,7},{7,3},{8,12},{12,8},{9,1... | collective-permute-start | bytes 2359304 | tf_op jit(solution)/shard_map/ppermute | solution.py:517
  50.7 23.3 %collective-permute-start.8 = (bf16[192,2048]{1,0:T(8,128)(2,1)}, bf16[192,2048]{1,0:T(8,128)(2,1)}, u32[]{:S(2)}, u32[]{:S(2)}) collective-permute-start(bf16[192,2048]{1,0:T(8,128)(2,1)} %collective-permute-done.4.rest_2_), channel_id=1, source_target_pairs={{0,4},{4,0},{1,5},{5,1},{2,6},{6,2},{3,7},{7,3},{8,12},{12,8},{9,1... | collective-permute-start | bytes 2359304 | tf_op jit(solution)/shard_map/ppermute | solution.py:517
  51.0 23.0 %collective-permute-start.9 = (bf16[192,2048]{1,0:T(8,128)(2,1)}, bf16[192,2048]{1,0:T(8,128)(2,1)}, u32[]{:S(2)}, u32[]{:S(2)}) collective-permute-start(bf16[192,2048]{1,0:T(8,128)(2,1)} %collective-permute-done.5.rest_3_), channel_id=1, source_target_pairs={{0,4},{4,0},{1,5},{5,1},{2,6},{6,2},{3,7},{7,3},{8,12},{12,8},{9,1... | collective-permute-start | bytes 2359304 | tf_op jit(solution)/shard_map/ppermute | solution.py:517
  81.0 4.7 %copy-start.2 = (bf16[2048]{0:T(1024)(128)(2,1)S(1)}, bf16[2048]{0:T(1024)(128)(2,1)}, u32[]{:S(2)}) copy-start(bf16[2048]{0:T(1024)(128)(2,1)} %param.44) | copy-start | bytes 12292
  81.0 5.3 %copy-start.3 = (f32[48,2]{0,1:T(2,128)S(1)}, f32[48,2]{0,1:T(2,128)}, u32[]{:S(2)}) copy-start(f32[48,2]{0,1:T(2,128)} %param.40) | copy-start | bytes 1156
  81.0 29.1 %all-to-all-start.1 = ((bf16[128,24,256]{2,1,0:T(8,128)(2,1)}), bf16[128,24,256]{2,1,0:T(8,128)(2,1)S(1)}, u32[]{:S(2)}, u32[]{:S(2)}) async-start(bf16[128,24,256]{2,1,0:T(8,128)(2,1)} %bitcast.22), calls=%async_computation.1 | async-start | bytes 3145728 | tf_op jit(solution)/shard_map/all_to_all | solution.py:588
